TPU v7x, 512 devices: a whole 4x8x8 slice. The times are simulated.
512 devices in a mesh: sp: 64 (over z, y), tp: 8 (over x, core).
Axes of the slice: x: 4, y: 8, z: 8, core: 2. Of those that a mesh axis runs over, the one named last changes fastest.
Arguments:
- queries: bfloat16 [32768, 2048], P('sp', 'tp'), may hold values from -14 to 14
- key_states: bfloat16 [32768, 512], P('sp', 'tp'), may hold values from -14 to 14
- value_states: bfloat16 [32768, 512], P('sp', 'tp'), may hold values from -6 to 6
- sink_logits: float32 [32], P('tp'), may hold values from 0 to 5
- out_weight: bfloat16 [2048, 2048], P('tp'), may hold values from -0.125 to 0.125
- residual: bfloat16 [32768, 2048], P(('sp', 'tp')), may hold values from -6 to 6
- gain_attn: float32 [2048], replicated, may hold values from 0.1 to 1.9
- gain_before: float32 [2048], replicated, may hold values from 0.1 to 1.9
- gain_after: float32 [2048], replicated, may hold values from 0.1 to 1.9
- gate_weight: bfloat16 [2048, 5632], P('sp', 'tp'), may hold values from -0.125 to 0.125
- value_weight: bfloat16 [2048, 5632], P('sp', 'tp'), may hold values from -0.125 to 0.125
- gate_taps: float32 [3, 5632], P(None, 'tp'), may hold values from -3 to 3
- value_taps: float32 [3, 5632], P(None, 'tp'), may hold values from -3 to 3
- down_weight: bfloat16 [5632, 2048], P('tp', 'sp'), may hold values from -0.078125 to 0.078125
Outputs:
- layer_out: bfloat16 [32768, 2048], P(('sp', 'tp'))
All inputs are finite; a program needn't handle non-finite values.
Results may differ from a plain program's by a relative error of at most 0.018.
Values may be sent and summed in bfloat16 or wider, within the bound.
No kernel may reach another device: no remote copies, remote signals or barrier semaphores. Data moves between devices by JAX's collectives and lax.ppermute only.
A program may use at most 64 MiB of HBM per device.

v0:
```python
import jax
import jax.numpy as jnp
from jax import lax
from jax.sharding import PartitionSpec as P

HD = 64
WINDOW = 128


NEG_FILL = -1e30


def passed_along(block, axis, distance):
    devices = range(lax.axis_size(axis))
    route = [(i - distance, i) for i in devices if i - distance in devices]
    return lax.ppermute(block, axis, route)


def in_blocks(shard, dim, peers):
    before, after = (shard.shape[:dim], shard.shape[dim + 1 :])
    return jnp.moveaxis(shard.reshape(*before, peers, -1, *after), dim, 0)


def sum_at_owner(shard, axis, dim):
    peers = lax.axis_size(axis)
    pieces = lax.all_to_all(in_blocks(shard, dim, peers), axis, 0, 0, tiled=True)
    return jnp.sum(pieces.astype(jnp.float32), axis=0)


def in_order(pieces, dim):
    pieces = jnp.moveaxis(pieces, 0, dim)
    lengths = pieces.shape
    return pieces.reshape(*lengths[:dim], lengths[dim] * lengths[dim + 1], *lengths[dim + 2 :])


def sent_to_all(shard, axis):
    copies = jnp.broadcast_to(shard, (lax.axis_size(axis), *shard.shape))
    return lax.all_to_all(copies, axis, split_axis=0, concat_axis=0, tiled=True)


def gather_directly(shard, axis, dim):
    return in_order(sent_to_all(shard, axis), dim)


def in_one_piece(arrays, axis, dim, along):
    widths = [a.shape[along] for a in arrays]
    both = jnp.concatenate(arrays, axis=along)
    filled = lax.all_gather(both, axis, axis=dim, tiled=True)
    return tuple(jnp.split(filled, [sum(widths[:k]) for k in range(1, len(widths))], axis=along))


def rms_scale(matrix):
    return matrix * lax.rsqrt(jnp.mean(matrix * matrix, axis=-1, keepdims=True) + 1e-06)


def attention_local(queries, key_states, value_states, sink_logits):
    length = queries.shape[0]
    blocks = length // WINDOW
    kv_local = key_states.shape[1] // HD
    grouping = queries.shape[1] // key_states.shape[1]
    earlier_keys, earlier_values = passed_along(
        (key_states[length - WINDOW :], value_states[length - WINDOW :]), "sp", 1
    )
    keys_ext = jnp.concatenate([earlier_keys, key_states], axis=0).reshape(
        blocks + 1, WINDOW, kv_local, HD
    )
    values_ext = jnp.concatenate([earlier_values, value_states], axis=0).reshape(
        blocks + 1, WINDOW, kv_local, HD
    )
    key_blocks = jnp.concatenate([keys_ext[:-1], keys_ext[1:]], axis=1)
    value_blocks = jnp.concatenate([values_ext[:-1], values_ext[1:]], axis=1)
    query_blocks = queries.reshape(blocks, WINDOW, kv_local, grouping, HD)
    offset = lax.axis_index("sp") * length
    qpos = (offset + jnp.arange(length, dtype=jnp.int32)).reshape(blocks, WINDOW)
    kpos = jnp.concatenate([qpos - WINDOW, qpos], axis=1)
    visible = (
        (kpos[:, None, :] <= qpos[:, :, None])
        & (qpos[:, :, None] - kpos[:, None, :] < WINDOW)
        & (kpos[:, None, :] >= 0)
    )
    scores = jnp.einsum(
        "nqhgd,nkhd->nhgqk", query_blocks, key_blocks, preferred_element_type=jnp.float32
    ) * HD ** (-0.5)
    scores = jnp.where(visible[:, None, None], scores, NEG_FILL)
    sink_col = sink_logits.reshape(kv_local, grouping)[None, :, :, None]
    top = jnp.maximum(jnp.max(scores, axis=-1), sink_col)
    expo = jnp.exp(scores - top[..., None])
    total = jnp.sum(expo, axis=-1) + jnp.exp(sink_col - top)
    probs = (expo / total[..., None]).astype(jnp.bfloat16)
    result = jnp.einsum(
        "nhgqk,nkhd->nqhgd", probs, value_blocks, preferred_element_type=jnp.float32
    )
    return result.astype(jnp.bfloat16).reshape(length, queries.shape[1])


def causal_local(upward, earlier, kernel):
    length = upward.shape[0]
    padded = jnp.concatenate([earlier, upward], axis=0).astype(jnp.float32)
    result = jnp.zeros(upward.shape, jnp.float32)
    for tap_index in range(kernel.shape[0]):
        result = result + kernel[tap_index][None, :] * padded[tap_index : tap_index + length]
    return result


def on_device(
    queries,
    key_states,
    value_states,
    sink_logits,
    out_weight,
    residual,
    gain_attn,
    gain_before,
    gain_after,
    gate_weight,
    value_weight,
    gate_taps,
    value_taps,
    down_weight,
):
    length = queries.shape[0]
    attended = attention_local(queries, key_states, value_states, sink_logits)
    selected = attended
    attn_proj = sum_at_owner(
        jnp.dot(selected, out_weight, preferred_element_type=jnp.float32).astype(jnp.bfloat16),
        "tp",
        0,
    )
    middle = residual.astype(jnp.float32) + rms_scale(attn_proj) * gain_attn
    normed = (rms_scale(middle) * gain_before).astype(jnp.bfloat16)
    whole_rows = gather_directly(normed, "tp", 0)
    gate_full, value_full = in_one_piece((gate_weight, value_weight), "sp", 0, 1)
    gate_up = jnp.dot(whole_rows, gate_full, preferred_element_type=jnp.float32).astype(
        jnp.bfloat16
    )
    value_up = jnp.dot(whole_rows, value_full, preferred_element_type=jnp.float32).astype(
        jnp.bfloat16
    )
    reach = gate_taps.shape[0] - 1
    gate_before, value_before = passed_along(
        (gate_up[length - reach :], value_up[length - reach :]), "sp", 1
    )
    gate_conv = causal_local(gate_up, gate_before, gate_taps)
    value_conv = causal_local(value_up, value_before, value_taps)
    hidden = (jax.nn.silu(gate_conv) * value_conv).astype(jnp.bfloat16)
    down_whole = lax.all_gather(down_weight, "sp", axis=1, tiled=True)
    selected = hidden
    down = sum_at_owner(
        jnp.dot(selected, down_whole, preferred_element_type=jnp.float32).astype(jnp.bfloat16),
        "tp",
        0,
    )
    return (middle + rms_scale(down) * gain_after).astype(jnp.bfloat16)


def solution(mesh):
    in_specs = (
        P("sp", "tp"),
        P("sp", "tp"),
        P("sp", "tp"),
        P("tp"),
        P("tp", None),
        P(("sp", "tp"), None),
        P(),
        P(),
        P(),
        P("sp", "tp"),
        P("sp", "tp"),
        P(None, "tp"),
        P(None, "tp"),
        P("tp", "sp"),
    )
    out_specs = P(("sp", "tp"), None)
    return jax.shard_map(
        on_device, mesh=mesh, in_specs=in_specs, out_specs=out_specs, check_vma=False
    )
```

profile of v0, /device:TPU:1, one launch (start us, length us, event | category | flops | bytes accessed | tf_op | source)
XLA Modules:
  0.0 238.2 jit_solution(13050096968348563992)
XLA Ops:
  6.5 0.0 copy-start
  6.5 0.0 copy-start.2
  6.5 0.0 all-gather.3.cloned.1.call-start
  6.5 1.6 pad_maximum_fusion
  8.2 0.0 all-gather.3.cloned.1.call-update
  8.2 0.7 slice.72
  8.9 4.0 %collective-permute-start.1 = (bf16[128,64]{0,1:T(8,128)(2,1)S(1)}, bf16[128,64]{0,1:T(8,128)(2,1)S(1)}, u32[]{:S(2)}, u32[]{:S(2)}) collective-permute-start(bf16[128,64]{0,1:T(8,128)(2,1)S(1)} %slice.72), channel_id=1, source_target_pairs={{0,8},{8,16},{16,24},{24,32},{32,40},{40,48},{48,56},{56,64},{64,7... | collective-permute-start | bytes 49160 | tf_op jit(solution)/shard_map/ppermute | solution.py:16
  13.0 0.7 slice.68
  13.7 3.2 %collective-permute-start = (bf16[128,64]{0,1:T(8,128)(2,1)S(1)}, bf16[128,64]{0,1:T(8,128)(2,1)S(1)}, u32[]{:S(2)}, u32[]{:S(2)}) collective-permute-start(bf16[128,64]{0,1:T(8,128)(2,1)S(1)} %slice.68), channel_id=1, source_target_pairs={{0,8},{8,16},{16,24},{24,32},{32,40},{40,48},{48,56},{56,64},{64,7... | collective-permute-start | bytes 49160 | tf_op jit(solution)/shard_map/ppermute | solution.py:16
  16.9 0.3 fusion.29
  17.3 0.9 slice.75
  18.1 0.9 slice.71
  19.0 1.2 reshape.136
  20.2 0.0 copy-start.8
  20.3 0.0 collective-permute-done.1
  20.3 0.8 pad_maximum_fusion.1
  21.2 0.0 collective-permute-done
  21.2 0.0 copy-done.2
  21.2 0.5 fusion.39
  21.8 0.0 copy-done.8
  21.8 0.1 broadcast_maximum_fusion
  21.9 0.3 fusion.4
  22.2 0.1 exponential_add_fusion
  22.3 0.5 fusion.17
  22.8 0.2 copy.24
  23.0 0.0 copy-done
  23.0 2.1 convolution_convert_fusion
  25.1 6.4 %all-to-all-start = ((bf16[8,64,2048]{2,1,0:T(8,128)(2,1)}), bf16[8,64,2048]{2,1,0:T(8,128)(2,1)}, u32[]{:S(2)}, u32[]{:S(2)}) async-start(bf16[8,64,2048]{2,1,0:T(8,128)(2,1)} %bitcast.11), calls=%async_computation | async-start | bytes 4194304 | tf_op jit(solution)/shard_map/all_to_all | solution.py:26
  31.5 0.0 copy-start.1
  31.5 0.0 all-gather.5.cloned.1.call-start
  31.6 0.7 all-gather.5.cloned.1.call-update
  32.3 25.6 %all-to-all-done = bf16[8,64,2048]{2,1,0:T(8,128)(2,1)} async-done(((bf16[8,64,2048]{2,1,0:T(8,128)(2,1)}), bf16[8,64,2048]{2,1,0:T(8,128)(2,1)}, u32[]{:S(2)}, u32[]{:S(2)}) %all-to-all-start) | async-done | bytes 2097184 | tf_op jit(solution)/shard_map/all_to_all | solution.py:26
  57.9 2.0 convert_reduce_fusion.1
  59.9 0.1 multiply_reduce_fusion.2
  60.0 0.0 copy-done.1
  60.0 0.0 copy-done.3
  60.0 0.3 multiply_reduce_fusion.1
  60.3 0.0 copy-done.4
  60.3 0.2 multiply_convert_fusion
  60.5 1.6 broadcast_in_dim.16
  62.1 5.3 %all-to-all-start.1 = ((bf16[8,64,2048]{2,1,0:T(8,128)(2,1)}), bf16[8,64,2048]{2,1,0:T(8,128)(2,1)}, u32[]{:S(2)}, u32[]{:S(2)}) async-start(bf16[8,64,2048]{2,1,0:T(8,128)(2,1)} %broadcast_in_dim.16), calls=%async_computation.1 | async-start | bytes 4194304 | tf_op jit(solution)/shard_map/all_to_all | solution.py:38
  67.5 0.0 copy-done.6
  67.5 0.0 copy-done.7
  67.5 0.1 slice_reduce_fusion.2
  67.6 26.3 %all-to-all-done.1 = bf16[8,64,2048]{2,1,0:T(8,128)(2,1)} async-done(((bf16[8,64,2048]{2,1,0:T(8,128)(2,1)}), bf16[8,64,2048]{2,1,0:T(8,128)(2,1)}, u32[]{:S(2)}, u32[]{:S(2)}) %all-to-all-start.1) | async-done | bytes 2097184 | tf_op jit(solution)/shard_map/all_to_all | solution.py:38
  93.8 8.4 %all-gather.3.cloned.1.call-done = bf16[2048,1408]{1,0:T(8,128)(2,1)} async-done(((bf16[32,1408]{1,0:T(8,128)(2,1)}), bf16[2048,1408]{1,0:T(8,128)(2,1)}) %all-gather.3.cloned.1.call-update) | async-done | bytes 5767184 | tf_op jit(solution)/shard_map/all_gather | solution.py:48
  102.2 4.4 %fusion.11 = bf16[512,704]{0,1:T(8,128)(2,1)S(1)} fusion(bf16[512,2048]{1,0:T(8,128)(2,1)} %bitcast.12, bf16[2048,1408]{1,0:T(8,128)(2,1)} %all-gather.3.cloned.1.call-done), kind=kOutput, calls=%fused_computation.24 | convolution fusion | flops 1476755456 | bytes 5963776 | tf_op jit(solution)/shard_map/dot_general | solution.py:133
  106.6 0.1 slice.90
  106.7 2.7 %collective-permute-start.2 = (bf16[2,704]{0,1:T(8,128)(2,1)S(1)}, bf16[2,704]{0,1:T(8,128)(2,1)S(1)}, u32[]{:S(2)}, u32[]{:S(2)}) collective-permute-start(bf16[2,704]{0,1:T(8,128)(2,1)S(1)} %slice.90), channel_id=1, source_target_pairs={{0,8},{8,16},{16,24},{24,32},{32,40},{40,48},{48,56},{56,64},{64,7... | collective-permute-start | bytes 8456 | tf_op jit(solution)/shard_map/ppermute | solution.py:16
  109.4 0.0 copy-done.9
  109.4 4.5 %fusion.14 = bf16[512,704]{0,1:T(8,128)(2,1)S(1)} fusion(bf16[512,2048]{1,0:T(8,128)(2,1)} %bitcast.12, bf16[2048,1408]{1,0:T(8,128)(2,1)S(1)} %copy-done.9), kind=kOutput, calls=%fused_computation.25 | convolution fusion | flops 1476755456 | bytes 5963776 | tf_op jit(solution)/shard_map/dot_general | solution.py:136
  113.9 0.1 slice.94
  114.0 3.7 %collective-permute-start.3 = (bf16[2,704]{0,1:T(8,128)(2,1)S(1)}, bf16[2,704]{0,1:T(8,128)(2,1)S(1)}, u32[]{:S(2)}, u32[]{:S(2)}) collective-permute-start(bf16[2,704]{0,1:T(8,128)(2,1)S(1)} %slice.94), channel_id=1, source_target_pairs={{0,8},{8,16},{16,24},{24,32},{32,40},{40,48},{48,56},{56,64},{64,7... | collective-permute-start | bytes 8456 | tf_op jit(solution)/shard_map/ppermute | solution.py:16
  117.7 0.0 collective-permute-done.2
  117.7 1.6 maximum_convert_fusion
  119.3 0.6 collective-permute-done.3
  119.9 1.6 maximum_convert_fusion.1
  121.5 64.6 %all-gather.5.cloned.1.call-done = bf16[704,2048]{0,1:T(8,128)(2,1)} async-done(((bf16[704,32]{0,1:T(8,128)(2,1)}), bf16[704,2048]{0,1:T(8,128)(2,1)}) %all-gather.5.cloned.1.call-update) | async-done | bytes 2883600 | tf_op jit(solution)/shard_map/all_gather | solution.py:146
  186.1 9.1 %convolution_convert_fusion.1 = bf16[512,2048]{1,0:T(8,128)(2,1)S(1)} fusion(bf16[704,2048]{0,1:T(8,128)(2,1)} %all-gather.5.cloned.1.call-done, f32[514,704]{0,1:T(8,128)} %maximum_convert_fusion.1, f32[514,704]{0,1:T(8,128)} %maximum_convert_fusion, f32[704]{0:T(1024)S(1)} %get-tuple-element.9, f32[704]{0:T(1024)S(1)} %get-tuple-element.10, ...), kind=kOutput, calls=%fused_computation.7 | convolution fusion | flops 1483210752 | bytes 13910528 | tf_op jit(solution)/shard_map/dot_general | solution.py:149
  195.2 34.6 %all_to_all.15 = bf16[8,64,2048]{2,1,0:T(8,128)(2,1)S(1)} all-to-all(bf16[8,64,2048]{2,1,0:T(8,128)(2,1)S(1)} %bitcast.47), channel_id=1, replica_groups=mesh['sp'=64,'tp'=8] {'tp'}, dimensions={0} | all-to-all | bytes 4194304 | tf_op jit(solution)/shard_map/all_to_all | solution.py:26
  229.8 0.4 convert_reduce_fusion
  230.1 0.1 multiply_reduce_fusion
  230.3 0.2 copy-done.5
  230.5 0.9 add_convert_fusion
  (20 shorter events, 0.2 us)
Async XLA Ops:
  6.5 16.4 %copy-start = (bf16[256,2048]{1,0:T(8,128)(2,1)S(1)}, bf16[256,2048]{1,0:T(8,128)(2,1)}, u32[]{:S(2)}) copy-start(bf16[256,2048]{1,0:T(8,128)(2,1)} %param.18) | copy-start | bytes 3145732
  6.5 14.6 %copy-start.2 = (bf16[512,64]{0,1:T(8,128)(2,1)S(1)}, bf16[512,64]{0,1:T(8,128)(2,1)}, u32[]{:S(2)}) copy-start(bf16[512,64]{0,1:T(8,128)(2,1)} %param.16) | copy-start | bytes 196612
  6.5 95.7 %all-gather.3.cloned.1.call-start = ((), (), s32[]{:S(2)}) async-start(), calls=%async_computation.3 | async-start | bytes 5857280 | tf_op jit(solution)/shard_map/all_gather | solution.py:48
  8.9 11.4 %collective-permute-start.1 = (bf16[128,64]{0,1:T(8,128)(2,1)S(1)}, bf16[128,64]{0,1:T(8,128)(2,1)S(1)}, u32[]{:S(2)}, u32[]{:S(2)}) collective-permute-start(bf16[128,64]{0,1:T(8,128)(2,1)S(1)} %slice.72), channel_id=1, source_target_pairs={{0,8},{8,16},{16,24},{24,32},{32,40},{40,48},{48,56},{56,64},{64,7... | collective-permute-start | bytes 49160 | tf_op jit(solution)/shard_map/ppermute | solution.py:16
  13.7 7.5 %collective-permute-start = (bf16[128,64]{0,1:T(8,128)(2,1)S(1)}, bf16[128,64]{0,1:T(8,128)(2,1)S(1)}, u32[]{:S(2)}, u32[]{:S(2)}) collective-permute-start(bf16[128,64]{0,1:T(8,128)(2,1)S(1)} %slice.68), channel_id=1, source_target_pairs={{0,8},{8,16},{16,24},{24,32},{32,40},{40,48},{48,56},{56,64},{64,7... | collective-permute-start | bytes 49160 | tf_op jit(solution)/shard_map/ppermute | solution.py:16
  20.2 1.5 copy-start.8
  25.1 32.8 %all-to-all-start = ((bf16[8,64,2048]{2,1,0:T(8,128)(2,1)}), bf16[8,64,2048]{2,1,0:T(8,128)(2,1)}, u32[]{:S(2)}, u32[]{:S(2)}) async-start(bf16[8,64,2048]{2,1,0:T(8,128)(2,1)} %bitcast.11), calls=%async_computation | async-start | bytes 4194304 | tf_op jit(solution)/shard_map/all_to_all | solution.py:26
  31.5 28.5 %copy-start.1 = (bf16[64,2048]{1,0:T(8,128)(2,1)S(1)}, bf16[64,2048]{1,0:T(8,128)(2,1)}, u32[]{:S(2)}) copy-start(bf16[64,2048]{1,0:T(8,128)(2,1)} %param.19) | copy-start | bytes 786436
  31.5 28.5 %copy-start.3 = (f32[2048]{0:T(1024)S(1)}, f32[2048]{0:T(1024)}, u32[]{:S(2)}) copy-start(f32[2048]{0:T(1024)} %param.20) | copy-start | bytes 24580
  31.5 28.8 %copy-start.4 = (f32[2048]{0:T(1024)S(1)}, f32[2048]{0:T(1024)}, u32[]{:S(2)}) copy-start(f32[2048]{0:T(1024)} %param.21) | copy-start | bytes 24580
  31.5 154.6 %all-gather.5.cloned.1.call-start = ((), (), s32[]{:S(2)}) async-start(), calls=%async_computation.4 | async-start | bytes 3194880 | tf_op jit(solution)/shard_map/all_gather | solution.py:146
  62.1 5.3 %copy-start.6 = (f32[3,704]{1,0:T(4,128)S(1)}, f32[3,704]{1,0:T(4,128)}, u32[]{:S(2)}) copy-start(f32[3,704]{1,0:T(4,128)} %param.26) | copy-start | bytes 25348
  62.1 5.3 %copy-start.7 = (f32[3,704]{1,0:T(4,128)S(1)}, f32[3,704]{1,0:T(4,128)}, u32[]{:S(2)}) copy-start(f32[3,704]{1,0:T(4,128)} %param.25) | copy-start | bytes 25348
  62.1 31.7 %all-to-all-start.1 = ((bf16[8,64,2048]{2,1,0:T(8,128)(2,1)}), bf16[8,64,2048]{2,1,0:T(8,128)(2,1)}, u32[]{:S(2)}, u32[]{:S(2)}) async-start(bf16[8,64,2048]{2,1,0:T(8,128)(2,1)} %broadcast_in_dim.16), calls=%async_computation.1 | async-start | bytes 4194304 | tf_op jit(solution)/shard_map/all_to_all | solution.py:38
  102.2 7.2 %copy-start.9 = (bf16[2048,1408]{1,0:T(8,128)(2,1)S(1)}, bf16[2048,1408]{1,0:T(8,128)(2,1)}, u32[]{:S(2)}) copy-start(bf16[2048,1408]{1,0:T(8,128)(2,1)} %all-gather.3.cloned.1.call-done) | copy-start | bytes 17301508
  106.7 11.0 %collective-permute-start.2 = (bf16[2,704]{0,1:T(8,128)(2,1)S(1)}, bf16[2,704]{0,1:T(8,128)(2,1)S(1)}, u32[]{:S(2)}, u32[]{:S(2)}) collective-permute-start(bf16[2,704]{0,1:T(8,128)(2,1)S(1)} %slice.90), channel_id=1, source_target_pairs={{0,8},{8,16},{16,24},{24,32},{32,40},{40,48},{48,56},{56,64},{64,7... | collective-permute-start | bytes 8456 | tf_op jit(solution)/shard_map/ppermute | solution.py:16
  114.0 5.9 %collective-permute-start.3 = (bf16[2,704]{0,1:T(8,128)(2,1)S(1)}, bf16[2,704]{0,1:T(8,128)(2,1)S(1)}, u32[]{:S(2)}, u32[]{:S(2)}) collective-permute-start(bf16[2,704]{0,1:T(8,128)(2,1)S(1)} %slice.94), channel_id=1, source_target_pairs={{0,8},{8,16},{16,24},{24,32},{32,40},{40,48},{48,56},{56,64},{64,7... | collective-permute-start | bytes 8456 | tf_op jit(solution)/shard_map/ppermute | solution.py:16
  229.8 0.7 copy-start.5
Sparse Core Ops, SparseCore 0:
  10.3 91.8 all-gather.2
  105.2 80.8 all-gather.4
where the time goes:
time: 239 us; the launch traced here: 238 us
  waiting for transfers between devices  126 us (53%)
  blocking collectives  34.6 us (14%)
  starting transfers between devices  25.4 us (11%)
  matrix products  21 us (9%)
  between operations  13.7 us (6%)
  other arithmetic  10.6 us (4%)
  local copies, waits for them, and re-layouts  6.82 us (3%)
    all_gather x1, waiting for transfers between devices, on_device(): down_whole = lax.all_gather(down_weight, 'sp', axis=1, tiled=True)  64.6 us
    all_to_all x1, blocking collectives, sum_at_owner(): lax.all_to_all(in_blocks(shard, dim, peers), axis, 0, 0, tiled=True)  34.6 us
    all_to_all x1, waiting for transfers between devices, sent_to_all(): return lax.all_to_all(copies, axis, split_axis=0, concat_axis=0, tiled=True)  26.3 us
    all_to_all x1, waiting for transfers between devices, sum_at_owner(): lax.all_to_all(in_blocks(shard, dim, peers), axis, 0, 0, tiled=True)  25.6 us
    ppermute x4, starting transfers between devices, passed_along(): return lax.ppermute(block, axis, route)  13.5 us
    dot_general x1, matrix products, on_device(): jnp.dot(selected, down_whole, preferred_element_type=jnp.float32)  9.1 us
    all_gather x1, waiting for transfers between devices, in_one_piece(): filled = lax.all_gather(both, axis, axis=dim, tiled=True)  8.4 us
    all_to_all x1, starting transfers between devices, sum_at_owner(): lax.all_to_all(in_blocks(shard, dim, peers), axis, 0, 0, tiled=True)  6.45 us
  transfers between devices with their start and end apart: 8, of which 5 were waited for; matrix products, arithmetic and copies ran while one was open for 11% of the time, Pallas kernels for 0%

commit v1 on v0

v1 whole, which is shorter than its diff:
```python
import functools

import jax
import jax.numpy as jnp
from jax import lax
from jax.experimental import pallas as pl
from jax.experimental.pallas import tpu as pltpu
from jax.sharding import Mesh
from jax.sharding import PartitionSpec as P

HD = 64
WINDOW = 128
D = 2048
UNITS = 704
PADDED = 768
UP_AT = PADDED
WIDE = PADDED + 2 * UNITS
HALO = 16
LOCAL = 512
OWN = 64
SP = ("z", "y")
TP = ("x", "c")

NEG_FILL = -1e30
BLOCKS = tuple((at, min(256, WIDE - at)) for at in range(UP_AT, WIDE, 256))


def passed_along(block, axis, distance):
    devices = range(lax.axis_size(axis))
    route = [(i - distance, i) for i in devices if i - distance in devices]
    return lax.ppermute(block, axis, route)


def in_blocks(shard, dim, peers):
    before, after = (shard.shape[:dim], shard.shape[dim + 1 :])
    return jnp.moveaxis(shard.reshape(*before, peers, -1, *after), dim, 0)


def sum_at_owner(shard, axis, dim):
    peers = lax.axis_size(axis)
    pieces = lax.all_to_all(in_blocks(shard, dim, peers), axis, 0, 0, tiled=True)
    return jnp.sum(pieces.astype(jnp.float32), axis=0)


def sent_to_all(shard, axis):
    copies = jnp.broadcast_to(shard, (lax.axis_size(axis), *shard.shape))
    return lax.all_to_all(copies, axis, split_axis=0, concat_axis=0, tiled=True)


def rms_scale(matrix):
    return matrix * lax.rsqrt(jnp.mean(matrix * matrix, axis=-1, keepdims=True) + 1e-06)


def attention_local(queries, key_states, value_states, sink_logits):
    length = queries.shape[0]
    blocks = length // WINDOW
    kv_local = key_states.shape[1] // HD
    grouping = queries.shape[1] // key_states.shape[1]
    earlier_keys, earlier_values = passed_along(
        (key_states[length - WINDOW :], value_states[length - WINDOW :]), SP, 1
    )
    keys_ext = jnp.concatenate([earlier_keys, key_states], axis=0).reshape(
        blocks + 1, WINDOW, kv_local, HD
    )
    values_ext = jnp.concatenate([earlier_values, value_states], axis=0).reshape(
        blocks + 1, WINDOW, kv_local, HD
    )
    key_blocks = jnp.concatenate([keys_ext[:-1], keys_ext[1:]], axis=1)
    value_blocks = jnp.concatenate([values_ext[:-1], values_ext[1:]], axis=1)
    query_blocks = queries.reshape(blocks, WINDOW, kv_local, grouping, HD)
    offset = lax.axis_index(SP) * length
    qpos = (offset + jnp.arange(length, dtype=jnp.int32)).reshape(blocks, WINDOW)
    kpos = jnp.concatenate([qpos - WINDOW, qpos], axis=1)
    visible = (
        (kpos[:, None, :] <= qpos[:, :, None])
        & (qpos[:, :, None] - kpos[:, None, :] < WINDOW)
        & (kpos[:, None, :] >= 0)
    )
    scores = jnp.einsum(
        "nqhgd,nkhd->nhgqk", query_blocks, key_blocks, preferred_element_type=jnp.float32
    ) * HD ** (-0.5)
    scores = jnp.where(visible[:, None, None], scores, NEG_FILL)
    sink_col = sink_logits.reshape(kv_local, grouping)[None, :, :, None]
    top = jnp.maximum(jnp.max(scores, axis=-1), sink_col)
    expo = jnp.exp(scores - top[..., None])
    total = jnp.sum(expo, axis=-1) + jnp.exp(sink_col - top)
    probs = (expo / total[..., None]).astype(jnp.bfloat16)
    result = jnp.einsum(
        "nhgqk,nkhd->nqhgd", probs, value_blocks, preferred_element_type=jnp.float32
    )
    return result.astype(jnp.bfloat16).reshape(length, queries.shape[1])


def feed_forward_kernel(x_ref, taps_ref, w_hbm, out_ref, w_up, w_down, up, hidden, sems):
    copies = []
    for k, (at, width) in enumerate(BLOCKS):
        copies.append(
            pltpu.make_async_copy(
                w_hbm.at[:, pl.ds(at, width)],
                w_up.at[:, pl.ds(at - UP_AT, width)],
                sems.at[k],
            )
        )
    down_copy = pltpu.make_async_copy(w_hbm.at[:, pl.ds(0, PADDED)], w_down, sems.at[len(BLOCKS)])
    for copy in copies:
        copy.start()
    down_copy.start()
    for (at, width), copy in zip(BLOCKS, copies):
        copy.wait()
        cols = pl.ds(at - UP_AT, width)
        part = jnp.dot(x_ref[...], w_up[:, cols], preferred_element_type=jnp.float32)
        up[:, cols] = part.astype(jnp.bfloat16).astype(jnp.float32)
    rows = 64
    lane = lax.broadcasted_iota(jnp.int32, (rows, PADDED), 1)

    def conv(start, first):
        cols = pl.ds(first, PADDED)
        total = taps_ref[0:1, cols] * up[pl.ds(start + HALO - 2, rows), cols]
        total = total + taps_ref[1:2, cols] * up[pl.ds(start + HALO - 1, rows), cols]
        return total + taps_ref[2:3, cols] * up[pl.ds(start + HALO, rows), cols]

    for start in range(0, LOCAL, rows):
        gate = conv(start, 0)
        value = pltpu.roll(conv(start, 2 * UNITS - PADDED), UNITS, 1)
        both = gate / (1.0 + jnp.exp(-gate)) * value
        both = jnp.where(lane < UNITS, both, 0.0)
        hidden[pl.ds(start, rows), :] = both.astype(jnp.bfloat16)
    down_copy.wait()
    width = 512
    for at in range(0, D, width):
        part = lax.dot_general(
            hidden[...],
            w_down[pl.ds(at, width), :],
            (((1,), (1,)), ((), ())),
            preferred_element_type=jnp.float32,
        ).astype(jnp.bfloat16)
        for block in range(LOCAL // OWN):
            out_ref[block % 2, block // 2, :, pl.ds(at, width)] = part[
                block * OWN : (block + 1) * OWN
            ]


def feed_forward(rows, taps, weights):
    return pl.pallas_call(
        feed_forward_kernel,
        out_shape=jax.ShapeDtypeStruct((2, LOCAL // OWN // 2, OWN, D), jnp.bfloat16),
        in_specs=[
            pl.BlockSpec(memory_space=pltpu.VMEM),
            pl.BlockSpec(memory_space=pltpu.VMEM),
            pl.BlockSpec(memory_space=pltpu.HBM),
        ],
        out_specs=pl.BlockSpec(memory_space=pltpu.VMEM),
        scratch_shapes=[
            pltpu.VMEM((D, 2 * UNITS), jnp.bfloat16),
            pltpu.VMEM((D, PADDED), jnp.bfloat16),
            pltpu.VMEM((HALO + LOCAL, 2 * UNITS), jnp.float32),
            pltpu.VMEM((LOCAL, PADDED), jnp.bfloat16),
            pltpu.SemaphoreType.DMA((len(BLOCKS) + 1,)),
        ],
        compiler_params=pltpu.CompilerParams(vmem_limit_bytes=40 * 1024 * 1024),
        cost_estimate=pl.CostEstimate(
            flops=6 * LOCAL * D * UNITS,
            bytes_accessed=2 * D * WIDE + 4 * LOCAL * D,
            transcendentals=LOCAL * UNITS,
        ),
        name="feed_forward",
    )(rows, taps, weights)


def on_device(
    queries,
    key_states,
    value_states,
    sink_logits,
    out_weight,
    residual,
    gain_attn,
    gain_before,
    gain_after,
    gate_weight,
    value_weight,
    gate_taps,
    value_taps,
    down_weight,
):
    packed = jnp.concatenate(
        [
            jnp.pad(down_weight.T, ((0, 0), (0, PADDED - UNITS))),
            gate_weight,
            value_weight,
        ],
        axis=1,
    )
    weights = lax.all_gather(packed, SP, axis=0, tiled=True)
    taps = jnp.concatenate([gate_taps, value_taps], axis=1)
    attended = attention_local(queries, key_states, value_states, sink_logits)
    attn_proj = sum_at_owner(
        jnp.dot(attended, out_weight, preferred_element_type=jnp.float32).astype(jnp.bfloat16),
        TP,
        0,
    )
    middle = residual.astype(jnp.float32) + rms_scale(attn_proj) * gain_attn
    normed = (rms_scale(middle) * gain_before).astype(jnp.bfloat16)
    whole_rows = sent_to_all(normed, TP).reshape(LOCAL, D)
    earlier = passed_along(whole_rows[LOCAL - HALO :], SP, 1)
    rows = jnp.concatenate([earlier, whole_rows], axis=0)
    shares = feed_forward(rows, taps, weights)
    pair = jnp.sum(
        lax.all_to_all(shares, "c", 0, 0, tiled=True).astype(jnp.float32), axis=0
    ).astype(jnp.bfloat16)
    down = jnp.sum(
        lax.all_to_all(pair, "x", 0, 0, tiled=True).astype(jnp.float32), axis=0
    )
    return (middle + rms_scale(down) * gain_after).astype(jnp.bfloat16)


def solution(mesh):
    mesh = Mesh(mesh.devices.reshape(8, 8, 4, 2), ("z", "y", "x", "c"))
    in_specs = (
        P(SP, TP),
        P(SP, TP),
        P(SP, TP),
        P(TP),
        P(TP, None),
        P((*SP, *TP), None),
        P(),
        P(),
        P(),
        P(SP, TP),
        P(SP, TP),
        P(None, TP),
        P(None, TP),
        P(TP, SP),
    )
    out_specs = P((*SP, *TP), None)
    return jax.shard_map(
        on_device, mesh=mesh, in_specs=in_specs, out_specs=out_specs, check_vma=False
    )
```

time: 239 us -> 168 us (0.70)
  waiting for transfers between devices: 126 us -> 27.7 us
  blocking collectives: 34.6 us -> 85.9 us
  matrix products: 21 us -> 1.77 us
  starting transfers between devices: 25.4 us -> 10.6 us
  Pallas kernels: 0 us -> 11.5 us
  other arithmetic: 10.6 us -> 5 us
  local copies, waits for them, and re-layouts: 6.82 us -> 11.4 us
    all_to_all x0 -> x3, blocking collectives: none -> 54.3 us  [the longest x1 29.7 us: sent_to_all(): return lax.all_to_all(copies, axis, split_axis=0, concat_axis=0, tiled=True)]
    all_to_all x2 -> x0, waiting for transfers between devices: 51.8 us -> none  [the longest x1 26.3 us: sent_to_all(): return lax.all_to_all(copies, axis, split_axis=0, concat_axis=0, tiled=True)]
    all_gather x2 -> x1, waiting for transfers between devices: 73 us -> 25.2 us  [on_device(): weights = lax.all_gather(packed, SP, axis=0, tiled=True)]
    dot_general x4 -> x1, matrix products: 20 us -> 0.74 us  [on_device(): jnp.dot(attended, out_weight, preferred_element_type=jnp.float32)]
    all_to_all x2 -> x0, starting transfers between devices: 11.8 us -> none  [the longest x1 6.45 us: sum_at_owner(): lax.all_to_all(in_blocks(shard, dim, peers), axis, 0, 0, tiled=True)]
    pallas_call x0 -> x1, Pallas kernels: none -> 11.5 us  [feed_forward(): pl.pallas_call(feed_forward_kernel, out_shape=jax.ShapeDtypeStruct((2, LO...]
    unnamed x20 -> x26, local copies, waits for them, and re-layouts: 0.23 us -> 4 us
    convert_element_type x2 -> x0, other arithmetic: 3.24 us -> none  [causal_local(): padded = jnp.concatenate([earlier, upward], axis=0).astype(jnp.float32)]
  transfers between devices with their start and end apart: 8 -> 4, of which waited for: 5 -> 2; matrix products, arithmetic and copies ran while one was open for 11% -> 5% of each run, Pallas kernels for 0% -> 0%
where the time goes in v1:
time: 168 us
  blocking collectives  85.9 us (51%)
  waiting for transfers between devices  27.7 us (16%)
  between operations  13.7 us (8%)
  Pallas kernels  11.5 us (7%)
  local copies, waits for them, and re-layouts  11.4 us (7%)
  starting transfers between devices  10.6 us (6%)
  other arithmetic  5 us (3%)
  matrix products  1.77 us (1%)
    all_to_all x1, blocking collectives, sum_at_owner(): lax.all_to_all(in_blocks(shard, dim, peers), axis, 0, 0, tiled=True)  31.6 us
    all_to_all x1, blocking collectives, sent_to_all(): return lax.all_to_all(copies, axis, split_axis=0, concat_axis=0, tiled=True)  29.7 us
    all_gather x1, waiting for transfers between devices, on_device(): weights = lax.all_gather(packed, SP, axis=0, tiled=True)  25.2 us
    all_to_all x1, blocking collectives, on_device(): lax.all_to_all(pair, 'x', 0, 0, tiled=True).astype(jnp.float32)  18.3 us
    pallas_call x1, Pallas kernels, feed_forward(): pl.pallas_call(feed_forward_kernel, out_shape=jax.ShapeDtypeStruct((2, LO...  11.5 us
    ppermute x3, starting transfers between devices, passed_along(): return lax.ppermute(block, axis, route)  10.6 us
    all_to_all x1, blocking collectives, on_device(): lax.all_to_all(shares, 'c', 0, 0, tiled=True).astype(jnp.float32)  6.29 us
    unnamed x26, local copies, waits for them, and re-layouts  4 us
  transfers between devices with their start and end apart: 4, of which 2 were waited for; matrix products, arithmetic and copies ran while one was open for 5% of the time, Pallas kernels for 0%

profile of v1, /device:TPU:1, one launch (start us, length us, event | category | flops | bytes accessed | tf_op | source)
XLA Modules:
  0.0 167.6 jit_solution(17017621263568666371)
XLA Ops:
  6.5 0.0 copy-start
  6.5 0.0 copy-start.5
  6.5 0.0 copy-start.6
  6.5 0.0 all-gather.2.cloned.1.call-start
  6.5 0.9 pad.4
  7.4 1.6 concatenate.35
  9.0 0.0 all-gather.2.cloned.1.call-update
  9.1 0.7 slice.33
  9.8 4.0 %collective-permute-start.1 = (bf16[128,64]{0,1:T(8,128)(2,1)S(1)}, bf16[128,64]{0,1:T(8,128)(2,1)S(1)}, u32[]{:S(2)}, u32[]{:S(2)}) collective-permute-start(bf16[128,64]{0,1:T(8,128)(2,1)S(1)} %slice.33), channel_id=1, source_target_pairs={{0,8},{8,16},{16,24},{24,32},{32,40},{40,48},{48,56},{56,64},{64,7... | collective-permute-start | bytes 49160 | tf_op jit(solution)/shard_map/ppermute | solution.py:31
  13.8 0.7 slice.29
  14.5 3.2 %collective-permute-start = (bf16[128,64]{0,1:T(8,128)(2,1)S(1)}, bf16[128,64]{0,1:T(8,128)(2,1)S(1)}, u32[]{:S(2)}, u32[]{:S(2)}) collective-permute-start(bf16[128,64]{0,1:T(8,128)(2,1)S(1)} %slice.29), channel_id=1, source_target_pairs={{0,8},{8,16},{16,24},{24,32},{32,40},{40,48},{48,56},{56,64},{64,7... | collective-permute-start | bytes 49160 | tf_op jit(solution)/shard_map/ppermute | solution.py:31
  17.8 0.3 fusion.5
  18.1 0.9 slice.36
  19.0 0.9 slice.32
  19.9 1.2 reshape.132
  21.1 0.0 copy-start.12
  21.1 0.0 collective-permute-done.1
  21.2 0.0 copy-done.5
  21.2 0.0 collective-permute-done
  21.2 0.0 copy-done.6
  21.3 0.5 fusion.14
  21.8 0.0 copy-done.12
  21.8 0.1 broadcast_maximum_fusion
  21.9 0.3 fusion
  22.2 0.1 exponential_add_fusion
  22.3 0.5 fusion.1
  22.8 0.2 copy.32
  23.0 0.0 copy-done
  23.0 0.7 convolution_convert_fusion
  23.8 31.6 %all_to_all.20 = bf16[8,64,2048]{2,1,0:T(8,128)(2,1)S(1)} all-to-all(bf16[8,64,2048]{2,1,0:T(8,128)(2,1)S(1)} %bitcast.46), channel_id=1, replica_groups=mesh['z'=8,'y'=8,'x'=4,'c'=2] {'x','c'}, dimensions={0} | all-to-all | bytes 4194304 | tf_op jit(solution)/shard_map/all_to_all | solution.py:41
  55.4 0.0 copy-start.4
  55.4 0.0 copy-start.7
  55.4 0.0 copy-start.10
  55.4 0.4 convert_reduce_fusion
  55.7 0.0 copy-start.2
  55.7 0.1 multiply_reduce_fusion.2
  55.9 0.4 copy-done.4
  56.3 0.0 copy-done.7
  56.3 0.3 multiply_reduce_fusion.1
  56.6 0.0 copy-done.10
  56.6 0.2 multiply_convert_fusion
  56.8 0.2 broadcast_in_dim.16
  57.1 0.0 copy-done.2
  57.1 0.0 copy-start.8
  57.1 0.0 copy-start.9
  57.1 29.7 %all_to_all.21 = bf16[8,64,2048]{2,1,0:T(8,128)(2,1)S(1)} all-to-all(bf16[8,64,2048]{2,1,0:T(8,128)(2,1)S(1)} %broadcast_in_dim.16), channel_id=1, replica_groups=mesh['z'=8,'y'=8,'x'=4,'c'=2] {'x','c'}, dimensions={0} | all-to-all | bytes 4194304 | tf_op jit(solution)/shard_map/all_to_all | solution.py:47
  86.8 3.4 %collective-permute-start.2 = (bf16[16,2048]{1,0:T(8,128)(2,1)S(1)}, bf16[16,2048]{1,0:T(8,128)(2,1)S(1)}, u32[]{:S(2)}, u32[]{:S(2)}) collective-permute-start(bf16[16,2048]{1,0:T(8,128)(2,1)S(1)} %slice.38), channel_id=1, source_target_pairs={{0,8},{8,16},{16,24},{24,32},{32,40},{40,48},{48,56},{56,64},{64,7... | collective-permute-start | bytes 196616 | tf_op jit(solution)/shard_map/ppermute | solution.py:31
  90.1 0.0 copy-done.8
  90.1 0.0 copy-done.9
  90.2 0.1 pad_maximum_fusion.3.taps_ref
  90.2 2.5 %collective-permute-done.2 = bf16[16,2048]{1,0:T(8,128)(2,1)S(1)} collective-permute-done((bf16[16,2048]{1,0:T(8,128)(2,1)S(1)}, bf16[16,2048]{1,0:T(8,128)(2,1)S(1)}, u32[]{:S(2)}, u32[]{:S(2)}) %collective-permute-start.2) | collective-permute-done | bytes 65568 | tf_op jit(solution)/shard_map/ppermute | solution.py:31
  92.7 0.1 pad_maximum_fusion.x_ref
  92.9 25.2 %all-gather.2.cloned.1.call-done.w_hbm = bf16[2048,2176]{1,0:T(8,128)(2,1)} async-done(((bf16[32,2176]{1,0:T(8,128)(2,1)}), bf16[2048,2176]{1,0:T(8,128)(2,1)}) %all-gather.2.cloned.1.call-update) | async-done | bytes 8912912 | tf_op jit(solution)/shard_map/all_gather | solution.py:194
  118.1 3.5 %copy-done.1 = bf16[2048,2176]{1,0:T(8,128)(2,1)S(1)} copy-done((bf16[2048,2176]{1,0:T(8,128)(2,1)S(1)}, bf16[2048,2176]{1,0:T(8,128)(2,1)}, u32[]{:S(2)}) %copy-start.1) | copy-done | bytes 8912920
  121.6 11.5 %feed_forward.1 = bf16[2,4,64,2048]{3,2,1,0:T(8,128)(2,1)S(1)} custom-call(bf16[528,2048]{1,0:T(8,128)(2,1)S(1)} %pad_maximum_fusion.x_ref, f32[3,1408]{1,0:T(4,128)S(1)} %pad_maximum_fusion.3.taps_ref, bf16[2048,2176]{1,0:T(8,128)(2,1)S(1)} %copy-done.1), custom_call_target="tpu_custom_call" | custom-call | flops 4429185024 | bytes 13107200 | tf_op jit(solution)/shard_map/feed_forward/pallas_call | solution.py:144
  133.2 6.3 %all_to_all.22 = bf16[2,4,64,2048]{3,2,1,0:T(8,128)(2,1)S(1)} all-to-all(bf16[2,4,64,2048]{3,2,1,0:T(8,128)(2,1)S(1)} %feed_forward.1), channel_id=1, replica_groups=mesh['z'=8,'y'=8,'x'=4,'c'=2] {'c'}, dimensions={0} | all-to-all | bytes 4194304 | tf_op jit(solution)/shard_map/all_to_all | solution.py:209
  139.5 1.7 %reduce_sum.70 = bf16[4,64,2048]{2,1,0:T(8,128)(2,1)} reduce(bf16[2,4,64,2048]{3,2,1,0:T(8,128)(2,1)S(1)} %all_to_all.22, bf16[]{:T(256)} %constant.40.clone.1), dimensions={0}, to_apply=%region_5.6 | reduce | flops 524288 | bytes 3145730 | tf_op jit(solution)/shard_map/reduce_sum | solution.py:208
  141.2 0.0 copy-start.3
  141.2 18.3 %all_to_all.23 = bf16[4,64,2048]{2,1,0:T(8,128)(2,1)S(1)} all-to-all(bf16[4,64,2048]{2,1,0:T(8,128)(2,1)} %reduce_sum.70), channel_id=1, replica_groups=mesh['z'=8,'y'=8,'x'=4,'c'=2] {'x'}, dimensions={0} | all-to-all | bytes 2097152 | tf_op jit(solution)/shard_map/all_to_all | solution.py:212
  159.5 0.2 convert_reduce_fusion.1
  159.7 0.1 multiply_reduce_fusion
  159.8 0.0 copy-done.3
  159.8 0.0 copy-done.11
  159.8 0.9 add_convert_fusion
  (18 shorter events, 0.2 us)
Async XLA Ops:
  6.5 16.5 %copy-start = (bf16[256,2048]{1,0:T(8,128)(2,1)S(1)}, bf16[256,2048]{1,0:T(8,128)(2,1)}, u32[]{:S(2)}) copy-start(bf16[256,2048]{1,0:T(8,128)(2,1)} %param.18) | copy-start | bytes 3145732
  6.5 14.6 %copy-start.5 = (bf16[512,64]{0,1:T(8,128)(2,1)S(1)}, bf16[512,64]{0,1:T(8,128)(2,1)}, u32[]{:S(2)}) copy-start(bf16[512,64]{0,1:T(8,128)(2,1)} %param.15) | copy-start | bytes 196612
  6.5 14.7 %copy-start.6 = (bf16[512,64]{0,1:T(8,128)(2,1)S(1)}, bf16[512,64]{0,1:T(8,128)(2,1)}, u32[]{:S(2)}) copy-start(bf16[512,64]{0,1:T(8,128)(2,1)} %param.16) | copy-start | bytes 196612
  6.5 111.5 %all-gather.2.cloned.1.call-start = ((), (), s32[]{:S(2)}) async-start(), calls=%async_computation.4 | async-start | bytes 9052160 | tf_op jit(solution)/shard_map/all_gather | solution.py:194
  9.8 11.4 %collective-permute-start.1 = (bf16[128,64]{0,1:T(8,128)(2,1)S(1)}, bf16[128,64]{0,1:T(8,128)(2,1)S(1)}, u32[]{:S(2)}, u32[]{:S(2)}) collective-permute-start(bf16[128,64]{0,1:T(8,128)(2,1)S(1)} %slice.33), channel_id=1, source_target_pairs={{0,8},{8,16},{16,24},{24,32},{32,40},{40,48},{48,56},{56,64},{64,7... | collective-permute-start | bytes 49160 | tf_op jit(solution)/shard_map/ppermute | solution.py:31
  14.5 6.7 %collective-permute-start = (bf16[128,64]{0,1:T(8,128)(2,1)S(1)}, bf16[128,64]{0,1:T(8,128)(2,1)S(1)}, u32[]{:S(2)}, u32[]{:S(2)}) collective-permute-start(bf16[128,64]{0,1:T(8,128)(2,1)S(1)} %slice.29), channel_id=1, source_target_pairs={{0,8},{8,16},{16,24},{24,32},{32,40},{40,48},{48,56},{56,64},{64,7... | collective-permute-start | bytes 49160 | tf_op jit(solution)/shard_map/ppermute | solution.py:31
  21.1 0.7 copy-start.12
  55.4 1.0 copy-start.4
  55.4 1.0 copy-start.7
  55.4 1.2 copy-start.10
  55.7 1.3 copy-start.2
  57.1 33.1 %copy-start.8 = (f32[3,704]{1,0:T(4,128)S(1)}, f32[3,704]{1,0:T(4,128)}, u32[]{:S(2)}) copy-start(f32[3,704]{1,0:T(4,128)} %param.26) | copy-start | bytes 25348
  57.1 33.1 %copy-start.9 = (f32[3,704]{1,0:T(4,128)S(1)}, f32[3,704]{1,0:T(4,128)}, u32[]{:S(2)}) copy-start(f32[3,704]{1,0:T(4,128)} %param.25) | copy-start | bytes 25348
  86.8 6.0 %collective-permute-start.2 = (bf16[16,2048]{1,0:T(8,128)(2,1)S(1)}, bf16[16,2048]{1,0:T(8,128)(2,1)S(1)}, u32[]{:S(2)}, u32[]{:S(2)}) collective-permute-start(bf16[16,2048]{1,0:T(8,128)(2,1)S(1)} %slice.38), channel_id=1, source_target_pairs={{0,8},{8,16},{16,24},{24,32},{32,40},{40,48},{48,56},{56,64},{64,7... | collective-permute-start | bytes 196616 | tf_op jit(solution)/shard_map/ppermute | solution.py:31
  118.1 3.5 %copy-start.1 = (bf16[2048,2176]{1,0:T(8,128)(2,1)S(1)}, bf16[2048,2176]{1,0:T(8,128)(2,1)}, u32[]{:S(2)}) copy-start(bf16[2048,2176]{1,0:T(8,128)(2,1)} %all-gather.2.cloned.1.call-done.w_hbm) | copy-start | bytes 26738692
  141.2 18.7 %copy-start.3 = (f32[64,2048]{1,0:T(8,128)S(1)}, f32[64,2048]{1,0:T(8,128)}, u32[]{:S(2)}) copy-start(f32[64,2048]{1,0:T(8,128)} %copy-done.2) | copy-start | bytes 1572868
  141.2 18.7 %copy-start.11 = (f32[2048]{0:T(1024)S(1)}, f32[2048]{0:T(1024)}, u32[]{:S(2)}) copy-start(f32[2048]{0:T(1024)} %param.22) | copy-start | bytes 24580
Sparse Core Ops, SparseCore 0:
  10.3 107.6 all-gather.1

commit v2 on v1

--- a/solution.py
+++ b/solution.py
@@ -22,7 +22,11 @@
 TP = ("x", "c")
 
 NEG_FILL = -1e30
-BLOCKS = tuple((at, min(256, WIDE - at)) for at in range(UP_AT, WIDE, 256))
+ALL = (*SP, *TP)
+RING = 8
+STEPS = (0, 1, -1, 2, -2, 3, -3, 4)
+CHUNKS = ((UP_AT, 512), (UP_AT + 512, 512), (UP_AT + 1024, 384), (0, PADDED))
+VMEM_LIMIT = 44 * 1024 * 1024
 
 
 def passed_along(block, axis, distance):
@@ -31,15 +35,11 @@
     return lax.ppermute(block, axis, route)
 
 
-def in_blocks(shard, dim, peers):
-    before, after = (shard.shape[:dim], shard.shape[dim + 1 :])
-    return jnp.moveaxis(shard.reshape(*before, peers, -1, *after), dim, 0)
-
-
-def sum_at_owner(shard, axis, dim):
-    peers = lax.axis_size(axis)
-    pieces = lax.all_to_all(in_blocks(shard, dim, peers), axis, 0, 0, tiled=True)
-    return jnp.sum(pieces.astype(jnp.float32), axis=0)
+def summed_at_owner(shares):
+    pair = jnp.sum(
+        lax.all_to_all(shares, "c", 0, 0, tiled=True).astype(jnp.float32), axis=0
+    ).astype(jnp.bfloat16)
+    return jnp.sum(lax.all_to_all(pair, "x", 0, 0, tiled=True).astype(jnp.float32), axis=0)
 
 
 def sent_to_all(shard, axis):
@@ -91,25 +91,48 @@
     return result.astype(jnp.bfloat16).reshape(length, queries.shape[1])
 
 
-def feed_forward_kernel(x_ref, taps_ref, w_hbm, out_ref, w_up, w_down, up, hidden, sems):
-    copies = []
-    for k, (at, width) in enumerate(BLOCKS):
-        copies.append(
-            pltpu.make_async_copy(
-                w_hbm.at[:, pl.ds(at, width)],
-                w_up.at[:, pl.ds(at - UP_AT, width)],
-                sems.at[k],
+def feed_forward_kernel(x_ref, taps_ref, *refs):
+    blocks = refs[:RING]
+    out_ref, weights, up, hidden, sems = refs[RING:]
+    core = lax.axis_index("c")
+    place = jnp.where(core == 1, lax.axis_index("z"), lax.axis_index("y"))
+
+    def on_copies(chunk, act):
+        cols = pl.ds(*CHUNKS[chunk])
+        for k, (block, step) in enumerate(zip(blocks, STEPS)):
+            source = lax.rem(place - step + RING, RING)
+            sem = sems.at[chunk, k]
+
+            @pl.when(core == 1)
+            def _():
+                act(
+                    pltpu.make_async_copy(
+                        block.at[:, :, cols], weights.at[source, :, :, cols], sem
+                    )
+                )
+
+            @pl.when(core == 0)
+            def _():
+                act(
+                    pltpu.make_async_copy(
+                        block.at[:, :, cols], weights.at[:, source, :, cols], sem
+                    )
+                )
+
+    for chunk in range(len(CHUNKS)):
+        on_copies(chunk, lambda copy: copy.start())
+    for chunk, (at, width) in enumerate(CHUNKS[:-1]):
+        on_copies(chunk, lambda copy: copy.wait())
+        for sub in range(at, at + width, 256):
+            wide = min(256, at + width - sub)
+            part = jnp.dot(
+                x_ref[...],
+                weights[:, :, :, sub : sub + wide].reshape(D, wide),
+                preferred_element_type=jnp.float32,
             )
-        )
-    down_copy = pltpu.make_async_copy(w_hbm.at[:, pl.ds(0, PADDED)], w_down, sems.at[len(BLOCKS)])
-    for copy in copies:
-        copy.start()
-    down_copy.start()
-    for (at, width), copy in zip(BLOCKS, copies):
-        copy.wait()
-        cols = pl.ds(at - UP_AT, width)
-        part = jnp.dot(x_ref[...], w_up[:, cols], preferred_element_type=jnp.float32)
-        up[:, cols] = part.astype(jnp.bfloat16).astype(jnp.float32)
+            up[:, sub - UP_AT : sub - UP_AT + wide] = part.astype(jnp.bfloat16).astype(
+                jnp.float32
+            )
     rows = 64
     lane = lax.broadcasted_iota(jnp.int32, (rows, PADDED), 1)
 
@@ -125,46 +148,81 @@
         both = gate / (1.0 + jnp.exp(-gate)) * value
         both = jnp.where(lane < UNITS, both, 0.0)
         hidden[pl.ds(start, rows), :] = both.astype(jnp.bfloat16)
-    down_copy.wait()
-    width = 512
-    for at in range(0, D, width):
+    on_copies(len(CHUNKS) - 1, lambda copy: copy.wait())
+    for z in range(0, RING, 2):
         part = lax.dot_general(
             hidden[...],
-            w_down[pl.ds(at, width), :],
+            weights[z : z + 2, :, :, 0:PADDED].reshape(2 * D // RING, PADDED),
             (((1,), (1,)), ((), ())),
             preferred_element_type=jnp.float32,
         ).astype(jnp.bfloat16)
+        cols = pl.ds(z * (D // RING), 2 * D // RING)
         for block in range(LOCAL // OWN):
-            out_ref[block % 2, block // 2, :, pl.ds(at, width)] = part[
-                block * OWN : (block + 1) * OWN
-            ]
-
-
-def feed_forward(rows, taps, weights):
+            out_ref[block % 2, block // 2, :, cols] = part[block * OWN : (block + 1) * OWN]
+
+
+def feed_forward(rows, taps, blocks):
     return pl.pallas_call(
         feed_forward_kernel,
         out_shape=jax.ShapeDtypeStruct((2, LOCAL // OWN // 2, OWN, D), jnp.bfloat16),
         in_specs=[
             pl.BlockSpec(memory_space=pltpu.VMEM),
             pl.BlockSpec(memory_space=pltpu.VMEM),
-            pl.BlockSpec(memory_space=pltpu.HBM),
-        ],
+        ]
+        + [pl.BlockSpec(memory_space=pl.ANY)] * RING,
         out_specs=pl.BlockSpec(memory_space=pltpu.VMEM),
         scratch_shapes=[
-            pltpu.VMEM((D, 2 * UNITS), jnp.bfloat16),
-            pltpu.VMEM((D, PADDED), jnp.bfloat16),
+            pltpu.VMEM((RING, RING, D // RING // RING, WIDE), jnp.bfloat16),
             pltpu.VMEM((HALO + LOCAL, 2 * UNITS), jnp.float32),
             pltpu.VMEM((LOCAL, PADDED), jnp.bfloat16),
-            pltpu.SemaphoreType.DMA((len(BLOCKS) + 1,)),
+            pltpu.SemaphoreType.DMA((len(CHUNKS), RING)),
         ],
-        compiler_params=pltpu.CompilerParams(vmem_limit_bytes=40 * 1024 * 1024),
+        compiler_params=pltpu.CompilerParams(vmem_limit_bytes=VMEM_LIMIT),
         cost_estimate=pl.CostEstimate(
             flops=6 * LOCAL * D * UNITS,
             bytes_accessed=2 * D * WIDE + 4 * LOCAL * D,
             transcendentals=LOCAL * UNITS,
         ),
         name="feed_forward",
-    )(rows, taps, weights)
+    )(rows, taps, *blocks)
+
+
+def device_at(z, y, x, c):
+    return ((z * RING + y) * 4 + x) * 2 + c
+
+
+def crossed_groups():
+    groups = []
+    for x in range(4):
+        for fixed in range(RING):
+            groups.append([device_at(fixed, k, x, 1) for k in range(RING)])
+            groups.append([device_at(k, fixed, x, 0) for k in range(RING)])
+    return groups
+
+
+def ring_step(block, distance):
+    route = []
+    for z in range(RING):
+        for y in range(RING):
+            for x in range(4):
+                route.append(
+                    (device_at(z, y, x, 1), device_at((z + distance) % RING, y, x, 1))
+                )
+                route.append(
+                    (device_at(z, y, x, 0), device_at(z, (y + distance) % RING, x, 0))
+                )
+    return lax.ppermute(block, ALL, route)
+
+
+def gathered_blocks(packed):
+    copies = jnp.broadcast_to(packed, (RING, *packed.shape))
+    own = lax.all_to_all(copies, ALL, 0, 0, tiled=True, axis_index_groups=crossed_groups())
+    held = {0: own}
+    for step in range(1, RING // 2 + 1):
+        held[step] = ring_step(held[step - 1], 1)
+        if step < RING // 2:
+            held[-step] = ring_step(held[1 - step], -1)
+    return [held[step] for step in STEPS]
 
 
 def on_device(
@@ -191,26 +249,20 @@
         ],
         axis=1,
     )
-    weights = lax.all_gather(packed, SP, axis=0, tiled=True)
+    weights = gathered_blocks(packed)
     taps = jnp.concatenate([gate_taps, value_taps], axis=1)
     attended = attention_local(queries, key_states, value_states, sink_logits)
-    attn_proj = sum_at_owner(
-        jnp.dot(attended, out_weight, preferred_element_type=jnp.float32).astype(jnp.bfloat16),
-        TP,
-        0,
-    )
+    shares = jnp.dot(attended, out_weight, preferred_element_type=jnp.float32)
+    shares = shares.astype(jnp.bfloat16).reshape(LOCAL // OWN // 2, 2, OWN, D)
+    attn_proj = summed_at_owner(jnp.moveaxis(shares, 1, 0))
     middle = residual.astype(jnp.float32) + rms_scale(attn_proj) * gain_attn
     normed = (rms_scale(middle) * gain_before).astype(jnp.bfloat16)
-    whole_rows = sent_to_all(normed, TP).reshape(LOCAL, D)
+    half = sent_to_all(normed, "x")
+    whole_rows = jnp.moveaxis(sent_to_all(half, "c"), 0, 1).reshape(LOCAL, D)
     earlier = passed_along(whole_rows[LOCAL - HALO :], SP, 1)
     rows = jnp.concatenate([earlier, whole_rows], axis=0)
     shares = feed_forward(rows, taps, weights)
-    pair = jnp.sum(
-        lax.all_to_all(shares, "c", 0, 0, tiled=True).astype(jnp.float32), axis=0
-    ).astype(jnp.bfloat16)
-    down = jnp.sum(
-        lax.all_to_all(pair, "x", 0, 0, tiled=True).astype(jnp.float32), axis=0
-    )
+    down = summed_at_owner(shares)
     return (middle + rms_scale(down) * gain_after).astype(jnp.bfloat16)
 
 

time: 168 us -> 172 us (1.024); the launches traced: 168 us -> 170 us
  starting transfers between devices: 10.6 us -> 48.2 us
  blocking collectives: 85.9 us -> 63.3 us
  between operations: 13.7 us -> 0.44 us
  other arithmetic: 5 us -> 11.2 us
  local copies, waits for them, and re-layouts: 11.4 us -> 6.78 us
  waiting for transfers between devices: 27.7 us -> 24.7 us
    ppermute x0 -> x7, starting transfers between devices: none -> 27.9 us  [ring_step(): return lax.ppermute(block, ALL, route)]
    all_gather x1 -> x0, waiting for transfers between devices: 25.2 us -> none  [on_device(): weights = lax.all_gather(packed, SP, axis=0, tiled=True)]
    all_to_all x1, blocking collectives: 29.7 us -> 8.9 us  [sent_to_all(): return lax.all_to_all(copies, axis, split_axis=0, concat_axis=0, tiled=True)]
    ppermute x0 -> x7, waiting for transfers between devices: none -> 13.2 us  [ring_step(): return lax.ppermute(block, ALL, route)]
    all_to_all x0 -> x2, starting transfers between devices: none -> 11.9 us  [the longest x1 7.64 us: gathered_blocks(): lax.all_to_all(copies, ALL, 0, 0, tiled=True, axis_index_groups=crossed_g...]
    all_to_all x0 -> x2, waiting for transfers between devices: none -> 5.45 us  [the longest x1 5.35 us: gathered_blocks(): lax.all_to_all(copies, ALL, 0, 0, tiled=True, axis_index_groups=crossed_g...]
    unnamed x26 -> x28, local copies, waits for them, and re-layouts: 4 us -> 0.06 us
    ppermute x3, waiting for transfers between devices: 2.49 us -> 6.12 us  [passed_along(): return lax.ppermute(block, axis, route)]
  transfers between devices with their start and end apart: 4 -> 12, of which waited for: 2 -> 6; matrix products, arithmetic and copies ran while one was open for 5% -> 9% of each run, Pallas kernels for 0% -> 0%
where the time goes in v2:
time: 172 us; the launch traced here: 170 us
  blocking collectives  63.3 us (37%)
  starting transfers between devices  48.2 us (28%)
  waiting for transfers between devices  24.7 us (14%)
  Pallas kernels  11.9 us (7%)
  other arithmetic  11.2 us (7%)
  local copies, waits for them, and re-layouts  6.78 us (4%)
  matrix products  3.1 us (2%)
    all_to_all x2, blocking collectives, summed_at_owner(): lax.all_to_all(pair, 'x', 0, 0, tiled=True).astype(jnp.float32)  36.8 us
    ppermute x7, starting transfers between devices, ring_step(): return lax.ppermute(block, ALL, route)  27.9 us
    all_to_all x2, blocking collectives, summed_at_owner(): lax.all_to_all(shares, 'c', 0, 0, tiled=True).astype(jnp.float32)  17.6 us
    ppermute x7, waiting for transfers between devices, ring_step(): return lax.ppermute(block, ALL, route)  13.2 us
    pallas_call x1, Pallas kernels, feed_forward(): pl.pallas_call(feed_forward_kernel, out_shape=jax.ShapeDtypeStruct((2, LO...  11.9 us
    all_to_all x1, blocking collectives, sent_to_all(): return lax.all_to_all(copies, axis, split_axis=0, concat_axis=0, tiled=True)  8.9 us
    ppermute x3, starting transfers between devices, passed_along(): return lax.ppermute(block, axis, route)  8.42 us
    all_to_all x1, starting transfers between devices, gathered_blocks(): lax.all_to_all(copies, ALL, 0, 0, tiled=True, axis_index_groups=crossed_g...  7.64 us
  transfers between devices with their start and end apart: 12, of which 6 were waited for; matrix products, arithmetic and copies ran while one was open for 9% of the time, Pallas kernels for 0%

profile of v2, /device:TPU:1, one launch (start us, length us, event | category | flops | bytes accessed | tf_op | source)
XLA Modules:
  0.0 169.7 jit_solution(1068083203794722999)
XLA Ops:
  0.0 0.0 copy-start
  0.0 0.9 pad.4
  0.9 1.0 concatenate.35
  1.9 1.1 broadcast_in_dim.22
  3.0 7.6 %all-to-all-start.4 = ((bf16[8,32,2176]{2,1,0:T(8,128)(2,1)}), bf16[8,32,2176]{2,1,0:T(8,128)(2,1)S(1)}, u32[]{:S(2)}, u32[]{:S(2)}) async-start(bf16[8,32,2176]{2,1,0:T(8,128)(2,1)} %broadcast_in_dim.22), calls=%async_computation.4 | async-start | bytes 2228224 | tf_op jit(solution)/shard_map/all_to_all | solution.py:219
  10.6 0.0 copy-done.5
  10.7 3.4 %collective-permute-start.1 = (bf16[128,64]{0,1:T(8,128)(2,1)S(1)}, bf16[128,64]{0,1:T(8,128)(2,1)S(1)}, u32[]{:S(2)}, u32[]{:S(2)}) collective-permute-start(bf16[128,64]{0,1:T(8,128)(2,1)S(1)} %slice.33), channel_id=1, source_target_pairs={{0,8},{8,16},{16,24},{24,32},{32,40},{40,48},{48,56},{56,64},{64,7... | collective-permute-start | bytes 49160 | tf_op jit(solution)/shard_map/ppermute | solution.py:35
  14.0 3.1 %collective-permute-start = (bf16[128,64]{0,1:T(8,128)(2,1)S(1)}, bf16[128,64]{0,1:T(8,128)(2,1)S(1)}, u32[]{:S(2)}, u32[]{:S(2)}) collective-permute-start(bf16[128,64]{0,1:T(8,128)(2,1)S(1)} %slice.29), channel_id=1, source_target_pairs={{0,8},{8,16},{16,24},{24,32},{32,40},{40,48},{48,56},{56,64},{64,7... | collective-permute-start | bytes 49160 | tf_op jit(solution)/shard_map/ppermute | solution.py:35
  17.2 0.3 fusion.5
  17.6 0.0 copy-done.7
  17.6 0.2 reshape.132
  17.9 0.0 copy-start.13
  17.9 4.3 %collective-permute-done.1 = bf16[128,64]{0,1:T(8,128)(2,1)S(1)} collective-permute-done((bf16[128,64]{0,1:T(8,128)(2,1)S(1)}, bf16[128,64]{0,1:T(8,128)(2,1)S(1)}, u32[]{:S(2)}, u32[]{:S(2)}) %collective-permute-start.1) | collective-permute-done | bytes 16416 | tf_op jit(solution)/shard_map/ppermute | solution.py:35
  22.3 1.9 %fusion.14 = (f32[4,4,128]{2,1,0:T(4,128)S(1)}, f32[4,1,4,128,256]{3,4,2,0,1:T(8,128)}) fusion(bf16[4,128,4,64]{3,2,1,0:T(4,128)(2,1)S(1)} %reshape.132, bf16[4,128,1,64]{1,3,0,2:T(8,128)(2,1)S(1)} %copy.38, bf16[4,128,1,64]{1,3,0,2:T(8,128)(2,1)S(1)} %copy.37, pred[4,128,256]{1,2,0:T(8,128)(4,1)S(1)} %fusion.5), kind=kOutput, calls=%fused_computation.44 | convolution fusion | flops 68941824 | bytes 2629632 | tf_op jit(solution)/shard_map/nqhgd,nkhd->nhgqk/dot_general | solution.py:79
  24.1 5.3 %all-to-all-done.4.refs_0_ = bf16[8,32,2176]{2,1,0:T(8,128)(2,1)S(1)} async-done(((bf16[8,32,2176]{2,1,0:T(8,128)(2,1)}), bf16[8,32,2176]{2,1,0:T(8,128)(2,1)S(1)}, u32[]{:S(2)}, u32[]{:S(2)}) %all-to-all-start.4) | async-done | bytes 1114144 | tf_op jit(solution)/shard_map/all_to_all | solution.py:219
  29.5 4.3 %collective-permute-start.3 = (bf16[8,32,2176]{2,1,0:T(8,128)(2,1)S(1)}, bf16[8,32,2176]{2,1,0:T(8,128)(2,1)S(1)}, u32[]{:S(2)}, u32[]{:S(2)}) collective-permute-start(bf16[8,32,2176]{2,1,0:T(8,128)(2,1)S(1)} %all-to-all-done.4.refs_0_), channel_id=1, source_target_pairs={{1,65},{0,8},{3,67},{2,10},{5,69},{4,12},{7,71},{6,14},{9,73},{8,1... | collective-permute-start | bytes 3342344 | tf_op jit(solution)/shard_map/ppermute | solution.py:214
  33.8 0.0 collective-permute-done
  33.8 0.0 copy-start.4
  33.9 0.1 broadcast_maximum_fusion
  33.9 2.0 %fusion = f32[4,4,128]{2,1,0:T(4,128)S(1)} fusion(f32[4,1,4,128,256]{3,4,2,0,1:T(8,128)} %get-tuple-element.6, f32[4,4,128]{2,1,0:T(4,128)S(1)} %broadcast_maximum_fusion), kind=kLoop, calls=%fused_computation.8 | loop fusion | flops 1046528 | bytes 2113536 | tf_op jit(solution)/shard_map/reduce_sum | solution.py:86
  36.0 0.1 exponential_add_fusion
  36.1 0.0 copy-done.4
  36.1 0.5 fusion.1
  36.6 0.2 copy.42
  36.8 8.4 %collective-permute-start.4 = (bf16[8,32,2176]{2,1,0:T(8,128)(2,1)S(1)}, bf16[8,32,2176]{2,1,0:T(8,128)(2,1)}, u32[]{:S(2)}, u32[]{:S(2)}) collective-permute-start(bf16[8,32,2176]{2,1,0:T(8,128)(2,1)S(1)} %all-to-all-done.4.refs_0_), channel_id=1, source_target_pairs={{1,449},{0,56},{3,451},{2,58},{5,453},{4,60},{7,455},{6,62},{9,457... | collective-permute-start | bytes 3342344 | tf_op jit(solution)/shard_map/ppermute | solution.py:214
  45.1 8.2 %collective-permute-done.3.refs_1_ = bf16[8,32,2176]{2,1,0:T(8,128)(2,1)S(1)} collective-permute-done((bf16[8,32,2176]{2,1,0:T(8,128)(2,1)S(1)}, bf16[8,32,2176]{2,1,0:T(8,128)(2,1)S(1)}, u32[]{:S(2)}, u32[]{:S(2)}) %collective-permute-start.3) | collective-permute-done | bytes 1114144 | tf_op jit(solution)/shard_map/ppermute | solution.py:214
  53.4 1.9 %collective-permute-start.5 = (bf16[8,32,2176]{2,1,0:T(8,128)(2,1)S(1)}, bf16[8,32,2176]{2,1,0:T(8,128)(2,1)}, u32[]{:S(2)}, u32[]{:S(2)}) collective-permute-start(bf16[8,32,2176]{2,1,0:T(8,128)(2,1)S(1)} %collective-permute-done.3.refs_1_), channel_id=1, source_target_pairs={{1,65},{0,8},{3,67},{2,10},{5,69},{4,12},{7,71},{6,14},{9,73},{8,1... | collective-permute-start | bytes 3342344 | tf_op jit(solution)/shard_map/ppermute | solution.py:214
  55.3 0.7 convolution_convert_fusion
  56.0 0.2 copy.60
  56.3 6.3 %all_to_all.35 = bf16[2,4,64,2048]{3,2,1,0:T(8,128)(2,1)} all-to-all(bf16[2,4,64,2048]{3,2,1,0:T(8,128)(2,1)S(1)} %bitcast.51), channel_id=1, replica_groups=mesh['z'=8,'y'=8,'x'=4,'c'=2] {'c'}, dimensions={0} | all-to-all | bytes 4194304 | tf_op jit(solution)/shard_map/all_to_all | solution.py:40
  62.6 3.3 %reduce_sum.79 = bf16[4,64,2048]{2,1,0:T(8,128)(2,1)} reduce(bf16[2,4,64,2048]{3,2,1,0:T(8,128)(2,1)} %all_to_all.35, bf16[]{:T(256)} %constant.39.clone.1), dimensions={0}, to_apply=%region_2.3 | reduce | flops 524288 | bytes 3145730 | tf_op jit(solution)/shard_map/reduce_sum | solution.py:39
  66.0 18.4 %all_to_all.36 = bf16[4,64,2048]{2,1,0:T(8,128)(2,1)S(1)} all-to-all(bf16[4,64,2048]{2,1,0:T(8,128)(2,1)} %reduce_sum.79), channel_id=1, replica_groups=mesh['z'=8,'y'=8,'x'=4,'c'=2] {'x'}, dimensions={0} | all-to-all | bytes 2097152 | tf_op jit(solution)/shard_map/all_to_all | solution.py:42
  84.3 0.2 convert_reduce_fusion.1
  84.5 0.1 multiply_reduce_fusion.2
  84.7 0.0 collective-permute-done.4.refs_2_
  84.7 4.2 %collective-permute-start.6 = (bf16[8,32,2176]{2,1,0:T(8,128)(2,1)}, bf16[8,32,2176]{2,1,0:T(8,128)(2,1)}, u32[]{:S(2)}, u32[]{:S(2)}) collective-permute-start(bf16[8,32,2176]{2,1,0:T(8,128)(2,1)} %collective-permute-done.4.refs_2_), channel_id=1, source_target_pairs={{1,449},{0,56},{3,451},{2,58},{5,453},{4,60},{7,455},{6,62},{9,457... | collective-permute-start | bytes 3342344 | tf_op jit(solution)/shard_map/ppermute | solution.py:214
  88.9 0.0 collective-permute-done.5.refs_3_
  88.9 1.9 %collective-permute-start.7 = (bf16[8,32,2176]{2,1,0:T(8,128)(2,1)}, bf16[8,32,2176]{2,1,0:T(8,128)(2,1)}, u32[]{:S(2)}, u32[]{:S(2)}) collective-permute-start(bf16[8,32,2176]{2,1,0:T(8,128)(2,1)} %collective-permute-done.5.refs_3_), channel_id=1, source_target_pairs={{1,65},{0,8},{3,67},{2,10},{5,69},{4,12},{7,71},{6,14},{9,73},{8,1... | collective-permute-start | bytes 3342344 | tf_op jit(solution)/shard_map/ppermute | solution.py:214
  90.9 0.3 multiply_reduce_fusion.1
  91.2 0.2 multiply_convert_fusion
  91.4 1.1 broadcast_in_dim.20
  92.5 4.2 %all-to-all-start.2 = ((bf16[4,64,2048]{2,1,0:T(8,128)(2,1)}), bf16[4,64,2048]{2,1,0:T(8,128)(2,1)}, u32[]{:S(2)}, u32[]{:S(2)}) async-start(bf16[4,64,2048]{2,1,0:T(8,128)(2,1)} %broadcast_in_dim.20), calls=%async_computation.2 | async-start | bytes 2097152 | tf_op jit(solution)/shard_map/all_to_all | solution.py:47
  96.7 4.9 %collective-permute-done.6.refs_4_ = bf16[8,32,2176]{2,1,0:T(8,128)(2,1)} collective-permute-done((bf16[8,32,2176]{2,1,0:T(8,128)(2,1)}, bf16[8,32,2176]{2,1,0:T(8,128)(2,1)}, u32[]{:S(2)}, u32[]{:S(2)}) %collective-permute-start.6) | collective-permute-done | bytes 1114144 | tf_op jit(solution)/shard_map/ppermute | solution.py:214
  101.6 5.3 %collective-permute-start.8 = (bf16[8,32,2176]{2,1,0:T(8,128)(2,1)}, bf16[8,32,2176]{2,1,0:T(8,128)(2,1)}, u32[]{:S(2)}, u32[]{:S(2)}) collective-permute-start(bf16[8,32,2176]{2,1,0:T(8,128)(2,1)} %collective-permute-done.6.refs_4_), channel_id=1, source_target_pairs={{1,449},{0,56},{3,451},{2,58},{5,453},{4,60},{7,455},{6,62},{9,457... | collective-permute-start | bytes 3342344 | tf_op jit(solution)/shard_map/ppermute | solution.py:214
  107.0 0.0 collective-permute-done.7.refs_5_
  107.0 1.9 %collective-permute-start.9 = (bf16[8,32,2176]{2,1,0:T(8,128)(2,1)}, bf16[8,32,2176]{2,1,0:T(8,128)(2,1)}, u32[]{:S(2)}, u32[]{:S(2)}) collective-permute-start(bf16[8,32,2176]{2,1,0:T(8,128)(2,1)} %collective-permute-done.7.refs_5_), channel_id=1, source_target_pairs={{1,65},{0,8},{3,67},{2,10},{5,69},{4,12},{7,71},{6,14},{9,73},{8,1... | collective-permute-start | bytes 3342344 | tf_op jit(solution)/shard_map/ppermute | solution.py:214
  108.9 0.1 all-to-all-done.2
  109.0 1.5 broadcast_in_dim.21
  110.5 8.9 %all_to_all.37 = bf16[2,4,64,2048]{3,2,1,0:T(8,128)(2,1)S(1)} all-to-all(bf16[2,4,64,2048]{3,2,1,0:T(8,128)(2,1)S(1)} %broadcast_in_dim.21), channel_id=1, replica_groups=mesh['z'=8,'y'=8,'x'=4,'c'=2] {'c'}, dimensions={0} | all-to-all | bytes 4194304 | tf_op jit(solution)/shard_map/all_to_all | solution.py:47
  119.5 0.2 copy.44
  119.7 2.0 %collective-permute-start.2 = (bf16[16,2048]{1,0:T(8,128)(2,1)S(1)}, bf16[16,2048]{1,0:T(8,128)(2,1)S(1)}, u32[]{:S(2)}, u32[]{:S(2)}) collective-permute-start(bf16[16,2048]{1,0:T(8,128)(2,1)S(1)} %slice.38), channel_id=1, source_target_pairs={{0,8},{8,16},{16,24},{24,32},{32,40},{40,48},{48,56},{56,64},{64,7... | collective-permute-start | bytes 196616 | tf_op jit(solution)/shard_map/ppermute | solution.py:35
  121.7 0.1 pad_maximum_fusion.3.taps_ref
  121.8 1.8 %collective-permute-done.2 = bf16[16,2048]{1,0:T(8,128)(2,1)S(1)} collective-permute-done((bf16[16,2048]{1,0:T(8,128)(2,1)S(1)}, bf16[16,2048]{1,0:T(8,128)(2,1)S(1)}, u32[]{:S(2)}, u32[]{:S(2)}) %collective-permute-start.2) | collective-permute-done | bytes 65568 | tf_op jit(solution)/shard_map/ppermute | solution.py:35
  123.6 1.5 pad_maximum_fusion.x_ref
  125.1 0.0 collective-permute-done.8.refs_6_
  125.1 0.0 collective-permute-done.9.refs_7_
  125.1 11.9 %feed_forward.1 = bf16[2,4,64,2048]{3,2,1,0:T(8,128)(2,1)} custom-call(bf16[528,2048]{1,0:T(8,128)(2,1)} %pad_maximum_fusion.x_ref, f32[3,1408]{1,0:T(4,128)S(1)} %pad_maximum_fusion.3.taps_ref, bf16[8,32,2176]{2,1,0:T(8,128)(2,1)S(1)} %all-to-all-done.4.refs_0_, bf16[8,32,2176]{2,1,0:T(8,128)(2,1)S(1)} %collective-permute-done.3.refs_1_, ...), custom_call_target="tpu_custom_call" | custom-call | flops 4429185024 | bytes 13107200 | tf_op jit(solution)/shard_map/feed_forward/pallas_call | solution.py:165
  137.0 11.3 %all_to_all.38 = bf16[2,4,64,2048]{3,2,1,0:T(8,128)(2,1)S(1)} all-to-all(bf16[2,4,64,2048]{3,2,1,0:T(8,128)(2,1)} %feed_forward.1), channel_id=1, replica_groups=mesh['z'=8,'y'=8,'x'=4,'c'=2] {'c'}, dimensions={0} | all-to-all | bytes 4194304 | tf_op jit(solution)/shard_map/all_to_all | solution.py:40
  148.3 1.7 %reduce_sum.83 = bf16[4,64,2048]{2,1,0:T(8,128)(2,1)} reduce(bf16[2,4,64,2048]{3,2,1,0:T(8,128)(2,1)S(1)} %all_to_all.38, bf16[]{:T(256)} %constant.39.clone.1), dimensions={0}, to_apply=%region_6.7 | reduce | flops 524288 | bytes 3145730 | tf_op jit(solution)/shard_map/reduce_sum | solution.py:39
  150.1 18.4 %all_to_all.39 = bf16[4,64,2048]{2,1,0:T(8,128)(2,1)S(1)} all-to-all(bf16[4,64,2048]{2,1,0:T(8,128)(2,1)} %reduce_sum.83), channel_id=1, replica_groups=mesh['z'=8,'y'=8,'x'=4,'c'=2] {'x'}, dimensions={0} | all-to-all | bytes 2097152 | tf_op jit(solution)/shard_map/all_to_all | solution.py:42
  168.5 0.2 convert_reduce_fusion
  168.7 0.1 multiply_reduce_fusion
  168.8 0.0 copy-done.12
  168.8 0.9 add_convert_fusion
  (41 shorter events, 0.3 us)
Async XLA Ops:
  0.0 55.3 %copy-start = (bf16[256,2048]{1,0:T(8,128)(2,1)S(1)}, bf16[256,2048]{1,0:T(8,128)(2,1)}, u32[]{:S(2)}) copy-start(bf16[256,2048]{1,0:T(8,128)(2,1)} %param.18) | copy-start | bytes 3145732
  0.0 10.6 %copy-start.5 = (bf16[512,64]{0,1:T(8,128)(2,1)S(1)}, bf16[512,64]{0,1:T(8,128)(2,1)}, u32[]{:S(2)}) copy-start(bf16[512,64]{0,1:T(8,128)(2,1)} %param.15) | copy-start | bytes 196612
  0.0 14.0 %copy-start.6 = (bf16[512,64]{0,1:T(8,128)(2,1)S(1)}, bf16[512,64]{0,1:T(8,128)(2,1)}, u32[]{:S(2)}) copy-start(bf16[512,64]{0,1:T(8,128)(2,1)} %param.16) | copy-start | bytes 196612
  0.9 16.7 %copy-start.7 = (bf16[512,256]{1,0:T(8,128)(2,1)S(1)}, bf16[512,256]{1,0:T(8,128)(2,1)}, u32[]{:S(2)}) copy-start(bf16[512,256]{1,0:T(8,128)(2,1)} %param.14) | copy-start | bytes 786436
  3.0 26.5 %all-to-all-start.4 = ((bf16[8,32,2176]{2,1,0:T(8,128)(2,1)}), bf16[8,32,2176]{2,1,0:T(8,128)(2,1)S(1)}, u32[]{:S(2)}, u32[]{:S(2)}) async-start(bf16[8,32,2176]{2,1,0:T(8,128)(2,1)} %broadcast_in_dim.22), calls=%async_computation.4 | async-start | bytes 2228224 | tf_op jit(solution)/shard_map/all_to_all | solution.py:219
  10.7 11.6 %collective-permute-start.1 = (bf16[128,64]{0,1:T(8,128)(2,1)S(1)}, bf16[128,64]{0,1:T(8,128)(2,1)S(1)}, u32[]{:S(2)}, u32[]{:S(2)}) collective-permute-start(bf16[128,64]{0,1:T(8,128)(2,1)S(1)} %slice.33), channel_id=1, source_target_pairs={{0,8},{8,16},{16,24},{24,32},{32,40},{40,48},{48,56},{56,64},{64,7... | collective-permute-start | bytes 49160 | tf_op jit(solution)/shard_map/ppermute | solution.py:35
  14.0 19.7 %collective-permute-start = (bf16[128,64]{0,1:T(8,128)(2,1)S(1)}, bf16[128,64]{0,1:T(8,128)(2,1)S(1)}, u32[]{:S(2)}, u32[]{:S(2)}) collective-permute-start(bf16[128,64]{0,1:T(8,128)(2,1)S(1)} %slice.29), channel_id=1, source_target_pairs={{0,8},{8,16},{16,24},{24,32},{32,40},{40,48},{48,56},{56,64},{64,7... | collective-permute-start | bytes 49160 | tf_op jit(solution)/shard_map/ppermute | solution.py:35
  17.9 16.0 %copy-start.13 = (f32[4]{0:T(128)S(1)}, f32[4]{0:T(128)}, u32[]{:S(2)}) copy-start(f32[4]{0:T(128)} %param.17) | copy-start | bytes 52
  29.5 23.9 %collective-permute-start.3 = (bf16[8,32,2176]{2,1,0:T(8,128)(2,1)S(1)}, bf16[8,32,2176]{2,1,0:T(8,128)(2,1)S(1)}, u32[]{:S(2)}, u32[]{:S(2)}) collective-permute-start(bf16[8,32,2176]{2,1,0:T(8,128)(2,1)S(1)} %all-to-all-done.4.refs_0_), channel_id=1, source_target_pairs={{1,65},{0,8},{3,67},{2,10},{5,69},{4,12},{7,71},{6,14},{9,73},{8,1... | collective-permute-start | bytes 3342344 | tf_op jit(solution)/shard_map/ppermute | solution.py:214
  33.8 2.2 %copy-start.4 = (f32[4,1,4,128,256]{3,4,2,0,1:T(8,128)S(1)}, f32[4,1,4,128,256]{3,4,2,0,1:T(8,128)}, u32[]{:S(2)}) copy-start(f32[4,1,4,128,256]{3,4,2,0,1:T(8,128)} %get-tuple-element.6) | copy-start | bytes 6291460
  36.8 47.9 %collective-permute-start.4 = (bf16[8,32,2176]{2,1,0:T(8,128)(2,1)S(1)}, bf16[8,32,2176]{2,1,0:T(8,128)(2,1)}, u32[]{:S(2)}, u32[]{:S(2)}) collective-permute-start(bf16[8,32,2176]{2,1,0:T(8,128)(2,1)S(1)} %all-to-all-done.4.refs_0_), channel_id=1, source_target_pairs={{1,449},{0,56},{3,451},{2,58},{5,453},{4,60},{7,455},{6,62},{9,457... | collective-permute-start | bytes 3342344 | tf_op jit(solution)/shard_map/ppermute | solution.py:214
  53.4 35.5 %collective-permute-start.5 = (bf16[8,32,2176]{2,1,0:T(8,128)(2,1)S(1)}, bf16[8,32,2176]{2,1,0:T(8,128)(2,1)}, u32[]{:S(2)}, u32[]{:S(2)}) collective-permute-start(bf16[8,32,2176]{2,1,0:T(8,128)(2,1)S(1)} %collective-permute-done.3.refs_1_), channel_id=1, source_target_pairs={{1,65},{0,8},{3,67},{2,10},{5,69},{4,12},{7,71},{6,14},{9,73},{8,1... | collective-permute-start | bytes 3342344 | tf_op jit(solution)/shard_map/ppermute | solution.py:214
  66.0 24.9 %copy-start.3 = (bf16[64,2048]{1,0:T(8,128)(2,1)S(1)}, bf16[64,2048]{1,0:T(8,128)(2,1)}, u32[]{:S(2)}) copy-start(bf16[64,2048]{1,0:T(8,128)(2,1)} %param.19) | copy-start | bytes 786436
  66.0 24.9 %copy-start.8 = (f32[2048]{0:T(1024)S(1)}, f32[2048]{0:T(1024)}, u32[]{:S(2)}) copy-start(f32[2048]{0:T(1024)} %param.20) | copy-start | bytes 24580
  66.0 25.2 %copy-start.11 = (f32[2048]{0:T(1024)S(1)}, f32[2048]{0:T(1024)}, u32[]{:S(2)}) copy-start(f32[2048]{0:T(1024)} %param.21) | copy-start | bytes 24580
  84.5 6.7 %copy-start.1 = (f32[64,2048]{1,0:T(8,128)}, f32[64,2048]{1,0:T(8,128)S(1)}, u32[]{:S(2)}) copy-start(f32[64,2048]{1,0:T(8,128)S(1)} %convert_reduce_fusion.1) | copy-start | bytes 1572868
  84.7 17.0 %collective-permute-start.6 = (bf16[8,32,2176]{2,1,0:T(8,128)(2,1)}, bf16[8,32,2176]{2,1,0:T(8,128)(2,1)}, u32[]{:S(2)}, u32[]{:S(2)}) collective-permute-start(bf16[8,32,2176]{2,1,0:T(8,128)(2,1)} %collective-permute-done.4.refs_2_), channel_id=1, source_target_pairs={{1,449},{0,56},{3,451},{2,58},{5,453},{4,60},{7,455},{6,62},{9,457... | collective-permute-start | bytes 3342344 | tf_op jit(solution)/shard_map/ppermute | solution.py:214
  88.9 18.1 %collective-permute-start.7 = (bf16[8,32,2176]{2,1,0:T(8,128)(2,1)}, bf16[8,32,2176]{2,1,0:T(8,128)(2,1)}, u32[]{:S(2)}, u32[]{:S(2)}) collective-permute-start(bf16[8,32,2176]{2,1,0:T(8,128)(2,1)} %collective-permute-done.5.refs_3_), channel_id=1, source_target_pairs={{1,65},{0,8},{3,67},{2,10},{5,69},{4,12},{7,71},{6,14},{9,73},{8,1... | collective-permute-start | bytes 3342344 | tf_op jit(solution)/shard_map/ppermute | solution.py:214
  92.5 16.5 %all-to-all-start.2 = ((bf16[4,64,2048]{2,1,0:T(8,128)(2,1)}), bf16[4,64,2048]{2,1,0:T(8,128)(2,1)}, u32[]{:S(2)}, u32[]{:S(2)}) async-start(bf16[4,64,2048]{2,1,0:T(8,128)(2,1)} %broadcast_in_dim.20), calls=%async_computation.2 | async-start | bytes 2097152 | tf_op jit(solution)/shard_map/all_to_all | solution.py:47
  101.6 23.5 %collective-permute-start.8 = (bf16[8,32,2176]{2,1,0:T(8,128)(2,1)}, bf16[8,32,2176]{2,1,0:T(8,128)(2,1)}, u32[]{:S(2)}, u32[]{:S(2)}) collective-permute-start(bf16[8,32,2176]{2,1,0:T(8,128)(2,1)} %collective-permute-done.6.refs_4_), channel_id=1, source_target_pairs={{1,449},{0,56},{3,451},{2,58},{5,453},{4,60},{7,455},{6,62},{9,457... | collective-permute-start | bytes 3342344 | tf_op jit(solution)/shard_map/ppermute | solution.py:214
  107.0 18.1 %collective-permute-start.9 = (bf16[8,32,2176]{2,1,0:T(8,128)(2,1)}, bf16[8,32,2176]{2,1,0:T(8,128)(2,1)}, u32[]{:S(2)}, u32[]{:S(2)}) collective-permute-start(bf16[8,32,2176]{2,1,0:T(8,128)(2,1)} %collective-permute-done.7.refs_5_), channel_id=1, source_target_pairs={{1,65},{0,8},{3,67},{2,10},{5,69},{4,12},{7,71},{6,14},{9,73},{8,1... | collective-permute-start | bytes 3342344 | tf_op jit(solution)/shard_map/ppermute | solution.py:214
  119.4 2.2 %copy-start.9 = (f32[3,704]{1,0:T(4,128)S(1)}, f32[3,704]{1,0:T(4,128)}, u32[]{:S(2)}) copy-start(f32[3,704]{1,0:T(4,128)} %param.26) | copy-start | bytes 25348
  119.4 2.3 %copy-start.10 = (f32[3,704]{1,0:T(4,128)S(1)}, f32[3,704]{1,0:T(4,128)}, u32[]{:S(2)}) copy-start(f32[3,704]{1,0:T(4,128)} %param.25) | copy-start | bytes 25348
  119.7 3.9 %collective-permute-start.2 = (bf16[16,2048]{1,0:T(8,128)(2,1)S(1)}, bf16[16,2048]{1,0:T(8,128)(2,1)S(1)}, u32[]{:S(2)}, u32[]{:S(2)}) collective-permute-start(bf16[16,2048]{1,0:T(8,128)(2,1)S(1)} %slice.38), channel_id=1, source_target_pairs={{0,8},{8,16},{16,24},{24,32},{32,40},{40,48},{48,56},{56,64},{64,7... | collective-permute-start | bytes 196616 | tf_op jit(solution)/shard_map/ppermute | solution.py:35
  150.0 18.8 %copy-start.2 = (f32[64,2048]{1,0:T(8,128)S(1)}, f32[64,2048]{1,0:T(8,128)}, u32[]{:S(2)}) copy-start(f32[64,2048]{1,0:T(8,128)} %copy-done.1) | copy-start | bytes 1572868
  150.1 18.8 %copy-start.12 = (f32[2048]{0:T(1024)S(1)}, f32[2048]{0:T(1024)}, u32[]{:S(2)}) copy-start(f32[2048]{0:T(1024)} %param.22) | copy-start | bytes 24580

commit v3 on v2

--- a/solution.py
+++ b/solution.py
@@ -35,11 +35,16 @@
     return lax.ppermute(block, axis, route)
 
 
-def summed_at_owner(shares):
-    pair = jnp.sum(
-        lax.all_to_all(shares, "c", 0, 0, tiled=True).astype(jnp.float32), axis=0
-    ).astype(jnp.bfloat16)
-    return jnp.sum(lax.all_to_all(pair, "x", 0, 0, tiled=True).astype(jnp.float32), axis=0)
+def swapped(block):
+    return lax.ppermute(block, "c", [(0, 1), (1, 0)])
+
+
+def projected(rows, weight):
+    return jnp.einsum("xrk,kd->xrd", rows, weight, preferred_element_type=jnp.float32)
+
+
+def summed_over_x(shares):
+    return jnp.sum(lax.all_to_all(shares, "x", 0, 0, tiled=True).astype(jnp.float32), axis=0)
 
 
 def sent_to_all(shard, axis):
@@ -51,49 +56,77 @@
     return matrix * lax.rsqrt(jnp.mean(matrix * matrix, axis=-1, keepdims=True) + 1e-06)
 
 
+def attention_kernel(q_ref, k_ref, v_ref, edge_ref, sink_ref, own_ref, other_ref):
+    core = lax.axis_index("c")
+    first = lax.axis_index("z") + lax.axis_index("y") == 0
+    row = lax.broadcasted_iota(jnp.int32, (WINDOW, 2 * WINDOW), 0)
+    key = lax.broadcasted_iota(jnp.int32, (WINDOW, 2 * WINDOW), 1)
+    inside = (key > row) & (key <= row + WINDOW)
+    none = jnp.zeros((HD, 2 * WINDOW), jnp.bfloat16)
+    for n in range(LOCAL // WINDOW):
+        if n == 0:
+            keys = jnp.concatenate([edge_ref[:HD], k_ref[:, :WINDOW]], axis=1)
+            values = jnp.concatenate([edge_ref[HD:], v_ref[:, :WINDOW]], axis=1)
+            seen = inside & ((key >= WINDOW) | jnp.logical_not(first))
+        else:
+            cols = pl.ds((n - 1) * WINDOW, 2 * WINDOW)
+            keys, values, seen = k_ref[:, cols], v_ref[:, cols], inside
+        for pair in range(2):
+            cols = pl.ds(pair * 2 * HD, 2 * HD)
+            query = q_ref[pl.ds(n * WINDOW, WINDOW), cols]
+            result = jnp.zeros((WINDOW, 2 * HD), jnp.float32)
+            for odd in range(2):
+                placed = lambda part: jnp.concatenate([none, part] if odd else [part, none], axis=0)
+                scores = jnp.dot(query, placed(keys), preferred_element_type=jnp.float32)
+                scores = jnp.where(seen, scores * HD ** (-0.5), NEG_FILL)
+                sink = sink_ref[2 * pair + odd]
+                top = jnp.maximum(jnp.max(scores, axis=-1, keepdims=True), sink)
+                expo = jnp.exp(scores - top)
+                total = jnp.sum(expo, axis=-1, keepdims=True) + jnp.exp(sink - top)
+                probs = (expo / total).astype(jnp.bfloat16)
+                result = result + lax.dot_general(
+                    probs,
+                    placed(values),
+                    (((1,), (1,)), ((), ())),
+                    preferred_element_type=jnp.float32,
+                )
+            result = result.astype(jnp.bfloat16)
+
+            @pl.when(core == 0)
+            def _():
+                own_ref[n, :, cols] = result[:OWN]
+                other_ref[n, :, cols] = result[OWN:]
+
+            @pl.when(core == 1)
+            def _():
+                own_ref[n, :, cols] = result[OWN:]
+                other_ref[n, :, cols] = result[:OWN]
+
+
 def attention_local(queries, key_states, value_states, sink_logits):
-    length = queries.shape[0]
-    blocks = length // WINDOW
-    kv_local = key_states.shape[1] // HD
-    grouping = queries.shape[1] // key_states.shape[1]
-    earlier_keys, earlier_values = passed_along(
-        (key_states[length - WINDOW :], value_states[length - WINDOW :]), SP, 1
-    )
-    keys_ext = jnp.concatenate([earlier_keys, key_states], axis=0).reshape(
-        blocks + 1, WINDOW, kv_local, HD
-    )
-    values_ext = jnp.concatenate([earlier_values, value_states], axis=0).reshape(
-        blocks + 1, WINDOW, kv_local, HD
-    )
-    key_blocks = jnp.concatenate([keys_ext[:-1], keys_ext[1:]], axis=1)
-    value_blocks = jnp.concatenate([values_ext[:-1], values_ext[1:]], axis=1)
-    query_blocks = queries.reshape(blocks, WINDOW, kv_local, grouping, HD)
-    offset = lax.axis_index(SP) * length
-    qpos = (offset + jnp.arange(length, dtype=jnp.int32)).reshape(blocks, WINDOW)
-    kpos = jnp.concatenate([qpos - WINDOW, qpos], axis=1)
-    visible = (
-        (kpos[:, None, :] <= qpos[:, :, None])
-        & (qpos[:, :, None] - kpos[:, None, :] < WINDOW)
-        & (kpos[:, None, :] >= 0)
-    )
-    scores = jnp.einsum(
-        "nqhgd,nkhd->nhgqk", query_blocks, key_blocks, preferred_element_type=jnp.float32
-    ) * HD ** (-0.5)
-    scores = jnp.where(visible[:, None, None], scores, NEG_FILL)
-    sink_col = sink_logits.reshape(kv_local, grouping)[None, :, :, None]
-    top = jnp.maximum(jnp.max(scores, axis=-1), sink_col)
-    expo = jnp.exp(scores - top[..., None])
-    total = jnp.sum(expo, axis=-1) + jnp.exp(sink_col - top)
-    probs = (expo / total[..., None]).astype(jnp.bfloat16)
-    result = jnp.einsum(
-        "nhgqk,nkhd->nqhgd", probs, value_blocks, preferred_element_type=jnp.float32
-    )
-    return result.astype(jnp.bfloat16).reshape(length, queries.shape[1])
-
-
-def feed_forward_kernel(x_ref, taps_ref, *refs):
+    keys, values = key_states.T, value_states.T
+    edge = jnp.concatenate([keys[:, LOCAL - WINDOW :], values[:, LOCAL - WINDOW :]], axis=0)
+    edge = passed_along(edge, SP, 1)
+    half = jax.ShapeDtypeStruct((LOCAL // OWN // 2, OWN, 4 * HD), jnp.bfloat16)
+    vmem = pl.BlockSpec(memory_space=pltpu.VMEM)
+    return pl.pallas_call(
+        attention_kernel,
+        out_shape=(half, half),
+        in_specs=[vmem] * 4 + [pl.BlockSpec(memory_space=pltpu.SMEM)],
+        out_specs=(vmem, vmem),
+        compiler_params=pltpu.CompilerParams(vmem_limit_bytes=16 * 1024 * 1024),
+        cost_estimate=pl.CostEstimate(
+            flops=8 * 4 * LOCAL * 2 * WINDOW * HD,
+            bytes_accessed=8 * LOCAL * 4 * HD,
+            transcendentals=4 * LOCAL * 2 * WINDOW,
+        ),
+        name="attention",
+    )(queries, keys, values, edge, sink_logits)
+
+
+def feed_forward_kernel(own_ref, other_ref, halo_0, halo_1, taps_ref, *refs):
     blocks = refs[:RING]
-    out_ref, weights, up, hidden, sems = refs[RING:]
+    out_own, out_other, weights, x_ref, up, hidden, sems, row_sems = refs[RING:]
     core = lax.axis_index("c")
     place = jnp.where(core == 1, lax.axis_index("z"), lax.axis_index("y"))
 
@@ -119,8 +152,25 @@
                     )
                 )
 
+    def on_rows(act):
+        for x in range(LOCAL // OWN // 2):
+            for k, (part, at) in enumerate(((own_ref, core), (other_ref, 1 - core))):
+                start = pl.multiple_of(HALO + OWN * (2 * x + at), HALO)
+                act(
+                    pltpu.make_async_copy(
+                        part.at[x], x_ref.at[pl.ds(start, OWN)], row_sems.at[2 * x + k]
+                    )
+                )
+        for k, halo in enumerate((halo_0, halo_1)):
+
+            @pl.when(core == k)
+            def _():
+                act(pltpu.make_async_copy(halo, x_ref.at[pl.ds(0, HALO)], row_sems.at[8]))
+
+    on_rows(lambda copy: copy.start())
     for chunk in range(len(CHUNKS)):
         on_copies(chunk, lambda copy: copy.start())
+    on_rows(lambda copy: copy.wait())
     for chunk, (at, width) in enumerate(CHUNKS[:-1]):
         on_copies(chunk, lambda copy: copy.wait())
         for sub in range(at, at + width, 256):
@@ -143,9 +193,9 @@
         return total + taps_ref[2:3, cols] * up[pl.ds(start + HALO, rows), cols]
 
     for start in range(0, LOCAL, rows):
-        gate = conv(start, 0)
+        gate = 0.5 * conv(start, 0)
         value = pltpu.roll(conv(start, 2 * UNITS - PADDED), UNITS, 1)
-        both = gate / (1.0 + jnp.exp(-gate)) * value
+        both = (gate + gate * jnp.tanh(gate)) * value
         both = jnp.where(lane < UNITS, both, 0.0)
         hidden[pl.ds(start, rows), :] = both.astype(jnp.bfloat16)
     on_copies(len(CHUNKS) - 1, lambda copy: copy.wait())
@@ -157,25 +207,31 @@
             preferred_element_type=jnp.float32,
         ).astype(jnp.bfloat16)
         cols = pl.ds(z * (D // RING), 2 * D // RING)
-        for block in range(LOCAL // OWN):
-            out_ref[block % 2, block // 2, :, cols] = part[block * OWN : (block + 1) * OWN]
-
-
-def feed_forward(rows, taps, blocks):
+        for owner, (even, odd) in enumerate(((out_own, out_other), (out_other, out_own))):
+
+            @pl.when(core == owner)
+            def _():
+                for x in range(LOCAL // OWN // 2):
+                    even[x, :, cols] = part[2 * x * OWN : (2 * x + 1) * OWN]
+                    odd[x, :, cols] = part[(2 * x + 1) * OWN : (2 * x + 2) * OWN]
+
+
+def feed_forward(own, other, halos, taps, blocks):
+    half = jax.ShapeDtypeStruct((LOCAL // OWN // 2, OWN, D), jnp.bfloat16)
     return pl.pallas_call(
         feed_forward_kernel,
-        out_shape=jax.ShapeDtypeStruct((2, LOCAL // OWN // 2, OWN, D), jnp.bfloat16),
-        in_specs=[
-            pl.BlockSpec(memory_space=pltpu.VMEM),
-            pl.BlockSpec(memory_space=pltpu.VMEM),
-        ]
+        out_shape=(half, half),
+        in_specs=[pl.BlockSpec(memory_space=pl.ANY)] * 4
+        + [pl.BlockSpec(memory_space=pltpu.VMEM)]
         + [pl.BlockSpec(memory_space=pl.ANY)] * RING,
-        out_specs=pl.BlockSpec(memory_space=pltpu.VMEM),
+        out_specs=[pl.BlockSpec(memory_space=pltpu.VMEM)] * 2,
         scratch_shapes=[
             pltpu.VMEM((RING, RING, D // RING // RING, WIDE), jnp.bfloat16),
+            pltpu.VMEM((HALO + LOCAL, D), jnp.bfloat16),
             pltpu.VMEM((HALO + LOCAL, 2 * UNITS), jnp.float32),
             pltpu.VMEM((LOCAL, PADDED), jnp.bfloat16),
             pltpu.SemaphoreType.DMA((len(CHUNKS), RING)),
+            pltpu.SemaphoreType.DMA((LOCAL // OWN + 1,)),
         ],
         compiler_params=pltpu.CompilerParams(vmem_limit_bytes=VMEM_LIMIT),
         cost_estimate=pl.CostEstimate(
@@ -184,7 +240,7 @@
             transcendentals=LOCAL * UNITS,
         ),
         name="feed_forward",
-    )(rows, taps, *blocks)
+    )(own, other, *halos, taps, *blocks)
 
 
 def device_at(z, y, x, c):
@@ -212,6 +268,14 @@
                     (device_at(z, y, x, 0), device_at(z, (y + distance) % RING, x, 0))
                 )
     return lax.ppermute(block, ALL, route)
+
+
+def halo_route(core):
+    route = []
+    for sp in range(RING * RING - 1):
+        for x in range(4):
+            route.append((device_at(0, sp, x, 1), device_at(0, sp + 1, x, core)))
+    return route
 
 
 def gathered_blocks(packed):
@@ -251,18 +315,21 @@
     )
     weights = gathered_blocks(packed)
     taps = jnp.concatenate([gate_taps, value_taps], axis=1)
-    attended = attention_local(queries, key_states, value_states, sink_logits)
-    shares = jnp.dot(attended, out_weight, preferred_element_type=jnp.float32)
-    shares = shares.astype(jnp.bfloat16).reshape(LOCAL // OWN // 2, 2, OWN, D)
-    attn_proj = summed_at_owner(jnp.moveaxis(shares, 1, 0))
+    other_weight = swapped(out_weight)
+    own, other = attention_local(queries, key_states, value_states, sink_logits)
+    other = swapped(other)
+    shares = projected(own, out_weight) + projected(other, other_weight)
+    attn_proj = summed_over_x(shares.astype(jnp.bfloat16))
     middle = residual.astype(jnp.float32) + rms_scale(attn_proj) * gain_attn
     normed = (rms_scale(middle) * gain_before).astype(jnp.bfloat16)
-    half = sent_to_all(normed, "x")
-    whole_rows = jnp.moveaxis(sent_to_all(half, "c"), 0, 1).reshape(LOCAL, D)
-    earlier = passed_along(whole_rows[LOCAL - HALO :], SP, 1)
-    rows = jnp.concatenate([earlier, whole_rows], axis=0)
-    shares = feed_forward(rows, taps, weights)
-    down = summed_at_owner(shares)
+    own_rows = sent_to_all(normed, "x")
+    other_rows = swapped(own_rows)
+    last = own_rows[-1, OWN - HALO :]
+    halos = [lax.ppermute(last, ALL, halo_route(core)) for core in range(2)]
+    own, other = feed_forward(own_rows, other_rows, halos, taps, weights)
+    other = swapped(other)
+    pair = (own.astype(jnp.float32) + other.astype(jnp.float32)).astype(jnp.bfloat16)
+    down = summed_over_x(pair)
     return (middle + rms_scale(down) * gain_after).astype(jnp.bfloat16)
 
 

time: 172 us -> 147 us (0.85)
  blocking collectives: 63.3 us -> 18.2 us
  starting transfers between devices: 48.2 us -> 69.1 us
  other arithmetic: 11.2 us -> 3.19 us
  waiting for transfers between devices: 24.7 us -> 31.8 us
  Pallas kernels: 11.9 us -> 14.9 us
  local copies, waits for them, and re-layouts: 6.78 us -> 4.05 us
    all_to_all x5 -> x1, blocking collectives: 63.3 us -> 18.2 us  [summed_over_x(): lax.all_to_all(shares, 'x', 0, 0, tiled=True).astype(jnp.float32)]
    ppermute x0 -> x6, starting transfers between devices: none -> 19.7 us  [the longest x4 16.2 us: swapped(): return lax.ppermute(block, 'c', [(0, 1), (1, 0)])]
    ppermute x7, waiting for transfers between devices: 13.2 us -> 22.9 us  [ring_step(): return lax.ppermute(block, ALL, route)]
    reduce_sum x5 -> x2, other arithmetic: 7.38 us -> 0.31 us  [summed_over_x(): jnp.sum(lax.all_to_all(shares, 'x', 0, 0, tiled=True).astype(jnp.float32)...]
    all_to_all x1, waiting for transfers between devices: 5.35 us -> 0.11 us  [gathered_blocks(): lax.all_to_all(copies, ALL, 0, 0, tiled=True, axis_index_groups=crossed_g...]
    ppermute x3 -> x1, starting transfers between devices: 8.42 us -> 3.2 us  [passed_along(): return lax.ppermute(block, axis, route)]
    all_to_all x0 -> x1, starting transfers between devices: none -> 4.15 us  [summed_over_x(): lax.all_to_all(shares, 'x', 0, 0, tiled=True).astype(jnp.float32)]
    ppermute x3 -> x1, waiting for transfers between devices: 6.12 us -> 2.56 us  [passed_along(): return lax.ppermute(block, axis, route)]
  transfers between devices with their start and end apart: 12 -> 17, of which waited for: 6 -> 12; matrix products, arithmetic and copies ran while one was open for 9% -> 5% of each run, Pallas kernels for 0% -> 3%
where the time goes in v3:
time: 147 us; the launch traced here: 146 us
  starting transfers between devices  69.1 us (47%)
  waiting for transfers between devices  31.8 us (22%)
  blocking collectives  18.2 us (12%)
  Pallas kernels  14.9 us (10%)
  local copies, waits for them, and re-layouts  4.05 us (3%)
  matrix products  4.04 us (3%)
  other arithmetic  3.19 us (2%)
    ppermute x7, starting transfers between devices, ring_step(): return lax.ppermute(block, ALL, route)  30.6 us
    ppermute x7, waiting for transfers between devices, ring_step(): return lax.ppermute(block, ALL, route)  22.9 us
    all_to_all x1, blocking collectives, summed_over_x(): lax.all_to_all(shares, 'x', 0, 0, tiled=True).astype(jnp.float32)  18.2 us
    ppermute x4, starting transfers between devices, swapped(): return lax.ppermute(block, 'c', [(0, 1), (1, 0)])  16.2 us
    pallas_call x1, Pallas kernels, feed_forward(): pl.pallas_call(feed_forward_kernel, out_shape=(half, half), in_specs=[pl....  10 us
    all_to_all x1, starting transfers between devices, gathered_blocks(): lax.all_to_all(copies, ALL, 0, 0, tiled=True, axis_index_groups=crossed_g...  7.64 us
    pallas_call x1, Pallas kernels, attention_local(): pl.pallas_call(attention_kernel, out_shape=(half, half), in_specs=[vmem]...  4.9 us
    all_to_all x1, starting transfers between devices, summed_over_x(): lax.all_to_all(shares, 'x', 0, 0, tiled=True).astype(jnp.float32)  4.15 us
  transfers between devices with their start and end apart: 17, of which 12 were waited for; matrix products, arithmetic and copies ran while one was open for 5% of the time, Pallas kernels for 3%

profile of v3, /device:TPU:1, one launch (start us, length us, event | category | flops | bytes accessed | tf_op | source)
XLA Modules:
  0.0 145.7 jit_solution(910284912842842336)
XLA Ops:
  0.0 0.0 copy-start.2
  0.0 0.9 pad.4
  0.9 0.9 concatenate.11
  1.8 1.1 broadcast_in_dim.5
  2.9 7.6 %all-to-all-start.2 = ((bf16[8,32,2176]{2,1,0:T(8,128)(2,1)}), bf16[8,32,2176]{2,1,0:T(8,128)(2,1)S(1)}, u32[]{:S(2)}, u32[]{:S(2)}) async-start(bf16[8,32,2176]{2,1,0:T(8,128)(2,1)} %broadcast_in_dim.5), calls=%async_computation.2 | async-start | bytes 2228224 | tf_op jit(solution)/shard_map/all_to_all | solution.py:283
  10.5 6.1 %collective-permute-start.2 = (bf16[256,2048]{1,0:T(8,128)(2,1)}, bf16[256,2048]{1,0:T(8,128)(2,1)S(1)}, u32[]{:S(2)}, u32[]{:S(2)}) collective-permute-start(bf16[256,2048]{1,0:T(8,128)(2,1)} %param.18), channel_id=1, source_target_pairs={{0,1},{1,0},{2,3},{3,2},{4,5},{5,4},{6,7},{7,6},{8,9},{9,8},{10,11... | collective-permute-start | bytes 3145736 | tf_op jit(solution)/shard_map/ppermute | solution.py:39
  16.6 0.0 copy-done
  16.6 0.0 copy-done.1
  16.7 3.2 %collective-permute-start = (bf16[128,128]{1,0:T(8,128)(2,1)S(1)}, bf16[128,128]{1,0:T(8,128)(2,1)S(1)}, u32[]{:S(2)}, u32[]{:S(2)}) collective-permute-start(bf16[128,128]{1,0:T(8,128)(2,1)S(1)} %pad_maximum_fusion), channel_id=1, source_target_pairs={{0,8},{8,16},{16,24},{24,32},{32,40},{40,48},{48,56},{56,64},{64,7... | collective-permute-start | bytes 98312 | tf_op jit(solution)/shard_map/ppermute | solution.py:35
  19.9 2.6 %collective-permute-done.edge_ref = bf16[128,128]{1,0:T(8,128)(2,1)S(1)} collective-permute-done((bf16[128,128]{1,0:T(8,128)(2,1)S(1)}, bf16[128,128]{1,0:T(8,128)(2,1)S(1)}, u32[]{:S(2)}, u32[]{:S(2)}) %collective-permute-start) | collective-permute-done | bytes 32800 | tf_op jit(solution)/shard_map/ppermute | solution.py:35
  22.4 0.0 copy-done.3
  22.5 0.0 copy-done.2
  22.5 4.9 %attention.1 = (bf16[4,64,256]{2,1,0:T(8,128)(2,1)S(1)}, bf16[4,64,256]{2,1,0:T(8,128)(2,1)S(1)}) custom-call(bf16[512,256]{1,0:T(8,128)(2,1)S(1)} %copy-done.2, bf16[64,512]{1,0:T(8,128)(2,1)S(1)} %bitcast.14, bf16[64,512]{1,0:T(8,128)(2,1)S(1)} %bitcast.16, bf16[128,128]{1,0:T(8,128)(2,1)S(1)} %collective-permute-done.edge_ref, f32[4]{0:T(128)S(1)} %copy-done.3), custom_call_target="tpu_custom_call" | custom-call | flops 268435456 | bytes 1048576 | tf_op jit(solution)/shard_map/attention/pallas_call | solution.py:112
  27.4 1.9 %collective-permute-start.1 = (bf16[4,64,256]{2,1,0:T(8,128)(2,1)S(1)}, bf16[4,64,256]{2,1,0:T(8,128)(2,1)}, u32[]{:S(2)}, u32[]{:S(2)}) collective-permute-start(bf16[4,64,256]{2,1,0:T(8,128)(2,1)S(1)} %get-tuple-element.10), channel_id=1, source_target_pairs={{0,1},{1,0},{2,3},{3,2},{4,5},{5,4},{6,7},{7,6},{8,9},{9,8},{10,11... | collective-permute-start | bytes 393224 | tf_op jit(solution)/shard_map/ppermute | solution.py:39
  29.3 0.1 all-to-all-done.2.refs_0_
  29.4 6.8 %collective-permute-start.6 = (bf16[8,32,2176]{2,1,0:T(8,128)(2,1)S(1)}, bf16[8,32,2176]{2,1,0:T(8,128)(2,1)S(1)}, u32[]{:S(2)}, u32[]{:S(2)}) collective-permute-start(bf16[8,32,2176]{2,1,0:T(8,128)(2,1)S(1)} %all-to-all-done.2.refs_0_), channel_id=1, source_target_pairs={{1,65},{0,8},{3,67},{2,10},{5,69},{4,12},{7,71},{6,14},{9,73},{8,1... | collective-permute-start | bytes 3342344 | tf_op jit(solution)/shard_map/ppermute | solution.py:270
  36.2 0.0 collective-permute-done.1
  36.2 0.0 collective-permute-done.2
  36.2 1.3 fusion.1
  37.5 2.7 %fusion = bf16[4,64,2048]{2,1,0:T(8,128)(2,1)} fusion(f32[4,64,2048]{2,1,0:T(8,128)S(1)} %fusion.1, bf16[4,64,256]{2,1,0:T(8,128)(2,1)S(1)} %get-tuple-element.9, bf16[256,2048]{1,0:T(8,128)(2,1)} %param.18), kind=kOutput, calls=%fused_computation.1 | convolution fusion | flops 269484032 | bytes 4325376 | tf_op jit(solution)/shard_map/xrk,kd->xrd/dot_general | solution.py:43
  40.2 4.1 %all-to-all-start = ((bf16[4,64,2048]{2,1,0:T(8,128)(2,1)}), bf16[4,64,2048]{2,1,0:T(8,128)(2,1)S(1)}, u32[]{:S(2)}, u32[]{:S(2)}) async-start(bf16[4,64,2048]{2,1,0:T(8,128)(2,1)} %fusion), calls=%async_computation | async-start | bytes 2097152 | tf_op jit(solution)/shard_map/all_to_all | solution.py:47
  44.4 7.4 %collective-permute-start.7 = (bf16[8,32,2176]{2,1,0:T(8,128)(2,1)S(1)}, bf16[8,32,2176]{2,1,0:T(8,128)(2,1)}, u32[]{:S(2)}, u32[]{:S(2)}) collective-permute-start(bf16[8,32,2176]{2,1,0:T(8,128)(2,1)S(1)} %all-to-all-done.2.refs_0_), channel_id=1, source_target_pairs={{1,449},{0,56},{3,451},{2,58},{5,453},{4,60},{7,455},{6,62},{9,457... | collective-permute-start | bytes 3342344 | tf_op jit(solution)/shard_map/ppermute | solution.py:270
  51.8 3.0 %collective-permute-done.6.refs_1_ = bf16[8,32,2176]{2,1,0:T(8,128)(2,1)S(1)} collective-permute-done((bf16[8,32,2176]{2,1,0:T(8,128)(2,1)S(1)}, bf16[8,32,2176]{2,1,0:T(8,128)(2,1)S(1)}, u32[]{:S(2)}, u32[]{:S(2)}) %collective-permute-start.6) | collective-permute-done | bytes 1114144 | tf_op jit(solution)/shard_map/ppermute | solution.py:270
  54.8 1.9 %collective-permute-start.8 = (bf16[8,32,2176]{2,1,0:T(8,128)(2,1)S(1)}, bf16[8,32,2176]{2,1,0:T(8,128)(2,1)}, u32[]{:S(2)}, u32[]{:S(2)}) collective-permute-start(bf16[8,32,2176]{2,1,0:T(8,128)(2,1)S(1)} %collective-permute-done.6.refs_1_), channel_id=1, source_target_pairs={{1,65},{0,8},{3,67},{2,10},{5,69},{4,12},{7,71},{6,14},{9,73},{8,1... | collective-permute-start | bytes 3342344 | tf_op jit(solution)/shard_map/ppermute | solution.py:270
  56.7 0.9 all-to-all-done
  57.6 0.2 convert_reduce_fusion.1
  57.8 0.0 copy-start.4
  57.8 0.1 multiply_reduce_fusion.2
  57.9 0.0 copy-done.6
  58.0 0.0 copy-done.7
  58.0 0.0 copy-start.10
  58.0 0.3 multiply_reduce_fusion.1
  58.3 5.9 %collective-permute-done.7.refs_2_ = bf16[8,32,2176]{2,1,0:T(8,128)(2,1)} collective-permute-done((bf16[8,32,2176]{2,1,0:T(8,128)(2,1)S(1)}, bf16[8,32,2176]{2,1,0:T(8,128)(2,1)}, u32[]{:S(2)}, u32[]{:S(2)}) %collective-permute-start.7) | collective-permute-done | bytes 1114144 | tf_op jit(solution)/shard_map/ppermute | solution.py:270
  64.2 5.4 %collective-permute-start.9 = (bf16[8,32,2176]{2,1,0:T(8,128)(2,1)}, bf16[8,32,2176]{2,1,0:T(8,128)(2,1)}, u32[]{:S(2)}, u32[]{:S(2)}) collective-permute-start(bf16[8,32,2176]{2,1,0:T(8,128)(2,1)} %collective-permute-done.7.refs_2_), channel_id=1, source_target_pairs={{1,449},{0,56},{3,451},{2,58},{5,453},{4,60},{7,455},{6,62},{9,457... | collective-permute-start | bytes 3342344 | tf_op jit(solution)/shard_map/ppermute | solution.py:270
  69.6 2.7 %collective-permute-done.8.refs_3_ = bf16[8,32,2176]{2,1,0:T(8,128)(2,1)} collective-permute-done((bf16[8,32,2176]{2,1,0:T(8,128)(2,1)S(1)}, bf16[8,32,2176]{2,1,0:T(8,128)(2,1)}, u32[]{:S(2)}, u32[]{:S(2)}) %collective-permute-start.8) | collective-permute-done | bytes 1114144 | tf_op jit(solution)/shard_map/ppermute | solution.py:270
  72.4 1.9 %collective-permute-start.10 = (bf16[8,32,2176]{2,1,0:T(8,128)(2,1)}, bf16[8,32,2176]{2,1,0:T(8,128)(2,1)}, u32[]{:S(2)}, u32[]{:S(2)}) collective-permute-start(bf16[8,32,2176]{2,1,0:T(8,128)(2,1)} %collective-permute-done.8.refs_3_), channel_id=1, source_target_pairs={{1,65},{0,8},{3,67},{2,10},{5,69},{4,12},{7,71},{6,14},{9,73},{8,1... | collective-permute-start | bytes 3342344 | tf_op jit(solution)/shard_map/ppermute | solution.py:270
  74.3 0.0 copy-done.4
  74.3 0.2 multiply_convert_fusion
  74.5 1.1 broadcast_in_dim.4
  75.6 3.9 %all-to-all-start.1 = ((bf16[4,64,2048]{2,1,0:T(8,128)(2,1)}), bf16[4,64,2048]{2,1,0:T(8,128)(2,1)S(1)}, u32[]{:S(2)}, u32[]{:S(2)}) async-start(bf16[4,64,2048]{2,1,0:T(8,128)(2,1)} %broadcast_in_dim.4), calls=%async_computation.1 | async-start | bytes 2097152 | tf_op jit(solution)/shard_map/all_to_all | solution.py:52
  79.5 2.9 %collective-permute-done.9.refs_4_ = bf16[8,32,2176]{2,1,0:T(8,128)(2,1)} collective-permute-done((bf16[8,32,2176]{2,1,0:T(8,128)(2,1)}, bf16[8,32,2176]{2,1,0:T(8,128)(2,1)}, u32[]{:S(2)}, u32[]{:S(2)}) %collective-permute-start.9) | collective-permute-done | bytes 1114144 | tf_op jit(solution)/shard_map/ppermute | solution.py:270
  82.4 5.3 %collective-permute-start.11 = (bf16[8,32,2176]{2,1,0:T(8,128)(2,1)}, bf16[8,32,2176]{2,1,0:T(8,128)(2,1)}, u32[]{:S(2)}, u32[]{:S(2)}) collective-permute-start(bf16[8,32,2176]{2,1,0:T(8,128)(2,1)} %collective-permute-done.9.refs_4_), channel_id=1, source_target_pairs={{1,449},{0,56},{3,451},{2,58},{5,453},{4,60},{7,455},{6,62},{9,457... | collective-permute-start | bytes 3342344 | tf_op jit(solution)/shard_map/ppermute | solution.py:270
  87.7 2.7 %collective-permute-done.10.refs_5_ = bf16[8,32,2176]{2,1,0:T(8,128)(2,1)} collective-permute-done((bf16[8,32,2176]{2,1,0:T(8,128)(2,1)}, bf16[8,32,2176]{2,1,0:T(8,128)(2,1)}, u32[]{:S(2)}, u32[]{:S(2)}) %collective-permute-start.10) | collective-permute-done | bytes 1114144 | tf_op jit(solution)/shard_map/ppermute | solution.py:270
  90.4 1.9 %collective-permute-start.12 = (bf16[8,32,2176]{2,1,0:T(8,128)(2,1)}, bf16[8,32,2176]{2,1,0:T(8,128)(2,1)}, u32[]{:S(2)}, u32[]{:S(2)}) collective-permute-start(bf16[8,32,2176]{2,1,0:T(8,128)(2,1)} %collective-permute-done.10.refs_5_), channel_id=1, source_target_pairs={{1,65},{0,8},{3,67},{2,10},{5,69},{4,12},{7,71},{6,14},{9,73},{8,1... | collective-permute-start | bytes 3342344 | tf_op jit(solution)/shard_map/ppermute | solution.py:270
  92.3 1.9 %all-to-all-done.1.own_ref = bf16[4,64,2048]{2,1,0:T(8,128)(2,1)S(1)} async-done(((bf16[4,64,2048]{2,1,0:T(8,128)(2,1)}), bf16[4,64,2048]{2,1,0:T(8,128)(2,1)S(1)}, u32[]{:S(2)}, u32[]{:S(2)}) %all-to-all-start.1) | async-done | bytes 1048608 | tf_op jit(solution)/shard_map/all_to_all | solution.py:52
  94.2 3.2 %collective-permute-start.3 = (bf16[4,64,2048]{2,1,0:T(8,128)(2,1)S(1)}, bf16[4,64,2048]{2,1,0:T(8,128)(2,1)S(1)}, u32[]{:S(2)}, u32[]{:S(2)}) collective-permute-start(bf16[4,64,2048]{2,1,0:T(8,128)(2,1)S(1)} %all-to-all-done.1.own_ref), channel_id=1, source_target_pairs={{0,1},{1,0},{2,3},{3,2},{4,5},{5,4},{6,7},{7,6},{8,9},{9,8},{10,11... | collective-permute-start | bytes 3145736 | tf_op jit(solution)/shard_map/ppermute | solution.py:39
  97.4 2.2 %collective-permute-start.5 = (bf16[16,2048]{1,0:T(8,128)(2,1)S(1)}, bf16[16,2048]{1,0:T(8,128)(2,1)S(1)}, u32[]{:S(2)}, u32[]{:S(2)}) collective-permute-start(bf16[16,2048]{1,0:T(8,128)(2,1)S(1)} %slice_bitcast_fusion), channel_id=1, source_target_pairs={{1,9},{3,11},{5,13},{7,15},{9,17},{11,19},{13,21},{15,23},{17,25},... | collective-permute-start | bytes 196616 | tf_op jit(solution)/shard_map/ppermute | solution.py:328
  99.6 1.3 collective-permute-start.4
  100.9 0.8 pad_maximum_fusion.1.taps_ref
  101.7 0.0 collective-permute-done.5.halo_1
  101.7 1.2 collective-permute-done.4.halo_0
  102.9 0.0 collective-permute-done.3.other_ref
  102.9 0.0 collective-permute-done.11.refs_6_
  102.9 5.5 %collective-permute-done.12.refs_7_ = bf16[8,32,2176]{2,1,0:T(8,128)(2,1)} collective-permute-done((bf16[8,32,2176]{2,1,0:T(8,128)(2,1)}, bf16[8,32,2176]{2,1,0:T(8,128)(2,1)}, u32[]{:S(2)}, u32[]{:S(2)}) %collective-permute-start.12) | collective-permute-done | bytes 1114144 | tf_op jit(solution)/shard_map/ppermute | solution.py:270
  108.5 10.0 %feed_forward.1 = (bf16[4,64,2048]{2,1,0:T(8,128)(2,1)S(1)}, bf16[4,64,2048]{2,1,0:T(8,128)(2,1)S(1)}) custom-call(bf16[4,64,2048]{2,1,0:T(8,128)(2,1)S(1)} %all-to-all-done.1.own_ref, bf16[4,64,2048]{2,1,0:T(8,128)(2,1)S(1)} %collective-permute-done.3.other_ref, bf16[16,2048]{1,0:T(8,128)(2,1)S(1)} %collective-permute-done.4.halo_0, ...), custom_call_target="tpu_custom_call" | custom-call | flops 4429185024 | bytes 13107200 | tf_op jit(solution)/shard_map/feed_forward/pallas_call | solution.py:221
  118.5 5.0 %collective-permute-start.13 = (bf16[4,64,2048]{2,1,0:T(8,128)(2,1)S(1)}, bf16[4,64,2048]{2,1,0:T(8,128)(2,1)S(1)}, u32[]{:S(2)}, u32[]{:S(2)}) collective-permute-start(bf16[4,64,2048]{2,1,0:T(8,128)(2,1)S(1)} %get-tuple-element.12), channel_id=1, source_target_pairs={{0,1},{1,0},{2,3},{3,2},{4,5},{5,4},{6,7},{7,6},{8,9},{9,8},{10,11... | collective-permute-start | bytes 3145736 | tf_op jit(solution)/shard_map/ppermute | solution.py:39
  123.6 2.3 %collective-permute-done.13 = bf16[4,64,2048]{2,1,0:T(8,128)(2,1)S(1)} collective-permute-done((bf16[4,64,2048]{2,1,0:T(8,128)(2,1)S(1)}, bf16[4,64,2048]{2,1,0:T(8,128)(2,1)S(1)}, u32[]{:S(2)}, u32[]{:S(2)}) %collective-permute-start.13) | collective-permute-done | bytes 1048608 | tf_op jit(solution)/shard_map/ppermute | solution.py:39
  125.8 0.4 add_convert_fusion
  126.2 0.0 copy-start.9
  126.2 0.0 copy-start.11
  126.3 18.2 %all_to_all.20 = bf16[4,64,2048]{2,1,0:T(8,128)(2,1)S(1)} all-to-all(bf16[4,64,2048]{2,1,0:T(8,128)(2,1)S(1)} %add_convert_fusion), channel_id=1, replica_groups=mesh['z'=8,'y'=8,'x'=4,'c'=2] {'x'}, dimensions={0} | all-to-all | bytes 2097152 | tf_op jit(solution)/shard_map/all_to_all | solution.py:47
  144.4 0.2 convert_reduce_fusion
  144.6 0.1 multiply_reduce_fusion
  144.8 0.9 add_convert_fusion.1
  (19 shorter events, 0.1 us)
Async XLA Ops:
  0.0 16.6 %copy-start = (bf16[512,64]{0,1:T(8,128)(2,1)S(1)}, bf16[512,64]{0,1:T(8,128)(2,1)}, u32[]{:S(2)}) copy-start(bf16[512,64]{0,1:T(8,128)(2,1)} %param.15) | copy-start | bytes 196612
  0.0 16.6 %copy-start.1 = (bf16[512,64]{0,1:T(8,128)(2,1)S(1)}, bf16[512,64]{0,1:T(8,128)(2,1)}, u32[]{:S(2)}) copy-start(bf16[512,64]{0,1:T(8,128)(2,1)} %param.16) | copy-start | bytes 196612
  0.0 22.4 %copy-start.3 = (f32[4]{0:T(128)S(1)}, f32[4]{0:T(128)}, u32[]{:S(2)}) copy-start(f32[4]{0:T(128)} %sink_ref.1) | copy-start | bytes 52
  0.0 22.4 %copy-start.2 = (bf16[512,256]{1,0:T(8,128)(2,1)S(1)}, bf16[512,256]{1,0:T(8,128)(2,1)}, u32[]{:S(2)}) copy-start(bf16[512,256]{1,0:T(8,128)(2,1)} %q_ref.1) | copy-start | bytes 786436
  2.9 26.5 %all-to-all-start.2 = ((bf16[8,32,2176]{2,1,0:T(8,128)(2,1)}), bf16[8,32,2176]{2,1,0:T(8,128)(2,1)S(1)}, u32[]{:S(2)}, u32[]{:S(2)}) async-start(bf16[8,32,2176]{2,1,0:T(8,128)(2,1)} %broadcast_in_dim.5), calls=%async_computation.2 | async-start | bytes 2228224 | tf_op jit(solution)/shard_map/all_to_all | solution.py:283
  10.5 25.6 %collective-permute-start.2 = (bf16[256,2048]{1,0:T(8,128)(2,1)}, bf16[256,2048]{1,0:T(8,128)(2,1)S(1)}, u32[]{:S(2)}, u32[]{:S(2)}) collective-permute-start(bf16[256,2048]{1,0:T(8,128)(2,1)} %param.18), channel_id=1, source_target_pairs={{0,1},{1,0},{2,3},{3,2},{4,5},{5,4},{6,7},{7,6},{8,9},{9,8},{10,11... | collective-permute-start | bytes 3145736 | tf_op jit(solution)/shard_map/ppermute | solution.py:39
  16.7 5.8 %collective-permute-start = (bf16[128,128]{1,0:T(8,128)(2,1)S(1)}, bf16[128,128]{1,0:T(8,128)(2,1)S(1)}, u32[]{:S(2)}, u32[]{:S(2)}) collective-permute-start(bf16[128,128]{1,0:T(8,128)(2,1)S(1)} %pad_maximum_fusion), channel_id=1, source_target_pairs={{0,8},{8,16},{16,24},{24,32},{32,40},{40,48},{48,56},{56,64},{64,7... | collective-permute-start | bytes 98312 | tf_op jit(solution)/shard_map/ppermute | solution.py:35
  27.4 8.8 %collective-permute-start.1 = (bf16[4,64,256]{2,1,0:T(8,128)(2,1)S(1)}, bf16[4,64,256]{2,1,0:T(8,128)(2,1)}, u32[]{:S(2)}, u32[]{:S(2)}) collective-permute-start(bf16[4,64,256]{2,1,0:T(8,128)(2,1)S(1)} %get-tuple-element.10), channel_id=1, source_target_pairs={{0,1},{1,0},{2,3},{3,2},{4,5},{5,4},{6,7},{7,6},{8,9},{9,8},{10,11... | collective-permute-start | bytes 393224 | tf_op jit(solution)/shard_map/ppermute | solution.py:39
  29.4 25.4 %collective-permute-start.6 = (bf16[8,32,2176]{2,1,0:T(8,128)(2,1)S(1)}, bf16[8,32,2176]{2,1,0:T(8,128)(2,1)S(1)}, u32[]{:S(2)}, u32[]{:S(2)}) collective-permute-start(bf16[8,32,2176]{2,1,0:T(8,128)(2,1)S(1)} %all-to-all-done.2.refs_0_), channel_id=1, source_target_pairs={{1,65},{0,8},{3,67},{2,10},{5,69},{4,12},{7,71},{6,14},{9,73},{8,1... | collective-permute-start | bytes 3342344 | tf_op jit(solution)/shard_map/ppermute | solution.py:270
  40.2 17.7 %copy-start.6 = (bf16[64,2048]{1,0:T(8,128)(2,1)S(1)}, bf16[64,2048]{1,0:T(8,128)(2,1)}, u32[]{:S(2)}) copy-start(bf16[64,2048]{1,0:T(8,128)(2,1)} %param.19) | copy-start | bytes 786436
  40.2 17.7 %copy-start.7 = (f32[2048]{0:T(1024)S(1)}, f32[2048]{0:T(1024)}, u32[]{:S(2)}) copy-start(f32[2048]{0:T(1024)} %param.20) | copy-start | bytes 24580
  40.2 34.1 %copy-start.8 = (f32[2048]{0:T(1024)S(1)}, f32[2048]{0:T(1024)}, u32[]{:S(2)}) copy-start(f32[2048]{0:T(1024)} %param.21) | copy-start | bytes 24580
  40.2 17.4 %all-to-all-start = ((bf16[4,64,2048]{2,1,0:T(8,128)(2,1)}), bf16[4,64,2048]{2,1,0:T(8,128)(2,1)S(1)}, u32[]{:S(2)}, u32[]{:S(2)}) async-start(bf16[4,64,2048]{2,1,0:T(8,128)(2,1)} %fusion), calls=%async_computation | async-start | bytes 2097152 | tf_op jit(solution)/shard_map/all_to_all | solution.py:47
  44.4 19.8 %collective-permute-start.7 = (bf16[8,32,2176]{2,1,0:T(8,128)(2,1)S(1)}, bf16[8,32,2176]{2,1,0:T(8,128)(2,1)}, u32[]{:S(2)}, u32[]{:S(2)}) collective-permute-start(bf16[8,32,2176]{2,1,0:T(8,128)(2,1)S(1)} %all-to-all-done.2.refs_0_), channel_id=1, source_target_pairs={{1,449},{0,56},{3,451},{2,58},{5,453},{4,60},{7,455},{6,62},{9,457... | collective-permute-start | bytes 3342344 | tf_op jit(solution)/shard_map/ppermute | solution.py:270
  54.8 17.6 %collective-permute-start.8 = (bf16[8,32,2176]{2,1,0:T(8,128)(2,1)S(1)}, bf16[8,32,2176]{2,1,0:T(8,128)(2,1)}, u32[]{:S(2)}, u32[]{:S(2)}) collective-permute-start(bf16[8,32,2176]{2,1,0:T(8,128)(2,1)S(1)} %collective-permute-done.6.refs_1_), channel_id=1, source_target_pairs={{1,65},{0,8},{3,67},{2,10},{5,69},{4,12},{7,71},{6,14},{9,73},{8,1... | collective-permute-start | bytes 3342344 | tf_op jit(solution)/shard_map/ppermute | solution.py:270
  57.8 16.5 %copy-start.4 = (f32[64,2048]{1,0:T(8,128)}, f32[64,2048]{1,0:T(8,128)S(1)}, u32[]{:S(2)}) copy-start(f32[64,2048]{1,0:T(8,128)S(1)} %convert_reduce_fusion.1) | copy-start | bytes 1572868
  58.0 17.6 %copy-start.10 = (f32[64]{0:T(128)}, f32[64]{0:T(128)S(1)}, u32[]{:S(2)}) copy-start(f32[64]{0:T(128)S(1)} %add_rsqrt_fusion.2) | copy-start | bytes 772
  64.2 18.2 %collective-permute-start.9 = (bf16[8,32,2176]{2,1,0:T(8,128)(2,1)}, bf16[8,32,2176]{2,1,0:T(8,128)(2,1)}, u32[]{:S(2)}, u32[]{:S(2)}) collective-permute-start(bf16[8,32,2176]{2,1,0:T(8,128)(2,1)} %collective-permute-done.7.refs_2_), channel_id=1, source_target_pairs={{1,449},{0,56},{3,451},{2,58},{5,453},{4,60},{7,455},{6,62},{9,457... | collective-permute-start | bytes 3342344 | tf_op jit(solution)/shard_map/ppermute | solution.py:270
  72.4 18.1 %collective-permute-start.10 = (bf16[8,32,2176]{2,1,0:T(8,128)(2,1)}, bf16[8,32,2176]{2,1,0:T(8,128)(2,1)}, u32[]{:S(2)}, u32[]{:S(2)}) collective-permute-start(bf16[8,32,2176]{2,1,0:T(8,128)(2,1)} %collective-permute-done.8.refs_3_), channel_id=1, source_target_pairs={{1,65},{0,8},{3,67},{2,10},{5,69},{4,12},{7,71},{6,14},{9,73},{8,1... | collective-permute-start | bytes 3342344 | tf_op jit(solution)/shard_map/ppermute | solution.py:270
  75.6 18.6 %all-to-all-start.1 = ((bf16[4,64,2048]{2,1,0:T(8,128)(2,1)}), bf16[4,64,2048]{2,1,0:T(8,128)(2,1)S(1)}, u32[]{:S(2)}, u32[]{:S(2)}) async-start(bf16[4,64,2048]{2,1,0:T(8,128)(2,1)} %broadcast_in_dim.4), calls=%async_computation.1 | async-start | bytes 2097152 | tf_op jit(solution)/shard_map/all_to_all | solution.py:52
  82.4 20.6 %collective-permute-start.11 = (bf16[8,32,2176]{2,1,0:T(8,128)(2,1)}, bf16[8,32,2176]{2,1,0:T(8,128)(2,1)}, u32[]{:S(2)}, u32[]{:S(2)}) collective-permute-start(bf16[8,32,2176]{2,1,0:T(8,128)(2,1)} %collective-permute-done.9.refs_4_), channel_id=1, source_target_pairs={{1,449},{0,56},{3,451},{2,58},{5,453},{4,60},{7,455},{6,62},{9,457... | collective-permute-start | bytes 3342344 | tf_op jit(solution)/shard_map/ppermute | solution.py:270
  90.4 18.1 %collective-permute-start.12 = (bf16[8,32,2176]{2,1,0:T(8,128)(2,1)}, bf16[8,32,2176]{2,1,0:T(8,128)(2,1)}, u32[]{:S(2)}, u32[]{:S(2)}) collective-permute-start(bf16[8,32,2176]{2,1,0:T(8,128)(2,1)} %collective-permute-done.10.refs_5_), channel_id=1, source_target_pairs={{1,65},{0,8},{3,67},{2,10},{5,69},{4,12},{7,71},{6,14},{9,73},{8,1... | collective-permute-start | bytes 3342344 | tf_op jit(solution)/shard_map/ppermute | solution.py:270
  94.2 8.7 %collective-permute-start.3 = (bf16[4,64,2048]{2,1,0:T(8,128)(2,1)S(1)}, bf16[4,64,2048]{2,1,0:T(8,128)(2,1)S(1)}, u32[]{:S(2)}, u32[]{:S(2)}) collective-permute-start(bf16[4,64,2048]{2,1,0:T(8,128)(2,1)S(1)} %all-to-all-done.1.own_ref), channel_id=1, source_target_pairs={{0,1},{1,0},{2,3},{3,2},{4,5},{5,4},{6,7},{7,6},{8,9},{9,8},{10,11... | collective-permute-start | bytes 3145736 | tf_op jit(solution)/shard_map/ppermute | solution.py:39
  97.4 4.3 %collective-permute-start.5 = (bf16[16,2048]{1,0:T(8,128)(2,1)S(1)}, bf16[16,2048]{1,0:T(8,128)(2,1)S(1)}, u32[]{:S(2)}, u32[]{:S(2)}) collective-permute-start(bf16[16,2048]{1,0:T(8,128)(2,1)S(1)} %slice_bitcast_fusion), channel_id=1, source_target_pairs={{1,9},{3,11},{5,13},{7,15},{9,17},{11,19},{13,21},{15,23},{17,25},... | collective-permute-start | bytes 196616 | tf_op jit(solution)/shard_map/ppermute | solution.py:328
  99.6 3.3 %collective-permute-start.4 = (bf16[16,2048]{1,0:T(8,128)(2,1)S(1)}, bf16[16,2048]{1,0:T(8,128)(2,1)S(1)}, u32[]{:S(2)}, u32[]{:S(2)}) collective-permute-start(bf16[16,2048]{1,0:T(8,128)(2,1)S(1)} %slice_bitcast_fusion), channel_id=1, source_target_pairs={{1,8},{3,10},{5,12},{7,14},{9,16},{11,18},{13,20},{15,22},{17,24},... | collective-permute-start | bytes 196616 | tf_op jit(solution)/shard_map/ppermute | solution.py:328
  118.5 7.3 %collective-permute-start.13 = (bf16[4,64,2048]{2,1,0:T(8,128)(2,1)S(1)}, bf16[4,64,2048]{2,1,0:T(8,128)(2,1)S(1)}, u32[]{:S(2)}, u32[]{:S(2)}) collective-permute-start(bf16[4,64,2048]{2,1,0:T(8,128)(2,1)S(1)} %get-tuple-element.12), channel_id=1, source_target_pairs={{0,1},{1,0},{2,3},{3,2},{4,5},{5,4},{6,7},{7,6},{8,9},{9,8},{10,11... | collective-permute-start | bytes 3145736 | tf_op jit(solution)/shard_map/ppermute | solution.py:39
  126.2 18.5 %copy-start.5 = (f32[64,2048]{1,0:T(8,128)S(1)}, f32[64,2048]{1,0:T(8,128)}, u32[]{:S(2)}) copy-start(f32[64,2048]{1,0:T(8,128)} %copy-done.4) | copy-start | bytes 1572868
  126.2 18.5 %copy-start.9 = (f32[2048]{0:T(1024)S(1)}, f32[2048]{0:T(1024)}, u32[]{:S(2)}) copy-start(f32[2048]{0:T(1024)} %param.22) | copy-start | bytes 24580
  126.2 18.5 %copy-start.11 = (f32[64]{0:T(128)S(1)}, f32[64]{0:T(128)}, u32[]{:S(2)}) copy-start(f32[64]{0:T(128)} %copy-done.10) | copy-start | bytes 772

commit v4 on v3

--- a/solution.py
+++ b/solution.py
@@ -25,7 +25,6 @@
 ALL = (*SP, *TP)
 RING = 8
 STEPS = (0, 1, -1, 2, -2, 3, -3, 4)
-CHUNKS = ((UP_AT, 512), (UP_AT + 512, 512), (UP_AT + 1024, 384), (0, PADDED))
 VMEM_LIMIT = 44 * 1024 * 1024
 
 
@@ -130,27 +129,18 @@
     core = lax.axis_index("c")
     place = jnp.where(core == 1, lax.axis_index("z"), lax.axis_index("y"))
 
-    def on_copies(chunk, act):
-        cols = pl.ds(*CHUNKS[chunk])
+    def on_copies(act):
         for k, (block, step) in enumerate(zip(blocks, STEPS)):
             source = lax.rem(place - step + RING, RING)
-            sem = sems.at[chunk, k]
+            sem = sems.at[k]
 
             @pl.when(core == 1)
             def _():
-                act(
-                    pltpu.make_async_copy(
-                        block.at[:, :, cols], weights.at[source, :, :, cols], sem
-                    )
-                )
+                act(pltpu.make_async_copy(block, weights.at[source], sem))
 
             @pl.when(core == 0)
             def _():
-                act(
-                    pltpu.make_async_copy(
-                        block.at[:, :, cols], weights.at[:, source, :, cols], sem
-                    )
-                )
+                act(pltpu.make_async_copy(block, weights.at[:, source], sem))
 
     def on_rows(act):
         for x in range(LOCAL // OWN // 2):
@@ -168,21 +158,17 @@
                 act(pltpu.make_async_copy(halo, x_ref.at[pl.ds(0, HALO)], row_sems.at[8]))
 
     on_rows(lambda copy: copy.start())
-    for chunk in range(len(CHUNKS)):
-        on_copies(chunk, lambda copy: copy.start())
+    on_copies(lambda copy: copy.start())
     on_rows(lambda copy: copy.wait())
-    for chunk, (at, width) in enumerate(CHUNKS[:-1]):
-        on_copies(chunk, lambda copy: copy.wait())
-        for sub in range(at, at + width, 256):
-            wide = min(256, at + width - sub)
-            part = jnp.dot(
-                x_ref[...],
-                weights[:, :, :, sub : sub + wide].reshape(D, wide),
-                preferred_element_type=jnp.float32,
-            )
-            up[:, sub - UP_AT : sub - UP_AT + wide] = part.astype(jnp.bfloat16).astype(
-                jnp.float32
-            )
+    on_copies(lambda copy: copy.wait())
+    for at in range(0, 2 * UNITS, 256):
+        width = min(256, 2 * UNITS - at)
+        part = jnp.dot(
+            x_ref[...],
+            weights[:, :, :, UP_AT + at : UP_AT + at + width].reshape(D, width),
+            preferred_element_type=jnp.float32,
+        )
+        up[:, at : at + width] = part.astype(jnp.bfloat16).astype(jnp.float32)
     rows = 64
     lane = lax.broadcasted_iota(jnp.int32, (rows, PADDED), 1)
 
@@ -198,7 +184,6 @@
         both = (gate + gate * jnp.tanh(gate)) * value
         both = jnp.where(lane < UNITS, both, 0.0)
         hidden[pl.ds(start, rows), :] = both.astype(jnp.bfloat16)
-    on_copies(len(CHUNKS) - 1, lambda copy: copy.wait())
     for z in range(0, RING, 2):
         part = lax.dot_general(
             hidden[...],
@@ -230,7 +215,7 @@
             pltpu.VMEM((HALO + LOCAL, D), jnp.bfloat16),
             pltpu.VMEM((HALO + LOCAL, 2 * UNITS), jnp.float32),
             pltpu.VMEM((LOCAL, PADDED), jnp.bfloat16),
-            pltpu.SemaphoreType.DMA((len(CHUNKS), RING)),
+            pltpu.SemaphoreType.DMA((RING,)),
             pltpu.SemaphoreType.DMA((LOCAL // OWN + 1,)),
         ],
         compiler_params=pltpu.CompilerParams(vmem_limit_bytes=VMEM_LIMIT),
@@ -278,8 +263,7 @@
     return route
 
 
-def gathered_blocks(packed):
-    copies = jnp.broadcast_to(packed, (RING, *packed.shape))
+def gathered_blocks(copies):
     own = lax.all_to_all(copies, ALL, 0, 0, tiled=True, axis_index_groups=crossed_groups())
     held = {0: own}
     for step in range(1, RING // 2 + 1):
@@ -287,6 +271,38 @@
         if step < RING // 2:
             held[-step] = ring_step(held[1 - step], -1)
     return [held[step] for step in STEPS]
+
+
+def pack_kernel(down_hbm, gate_hbm, value_hbm, out_ref, down, gate, value, sems):
+    pairs = ((down_hbm, down), (gate_hbm, gate), (value_hbm, value))
+    copies = [
+        pltpu.make_async_copy(source, target, sems.at[k]) for k, (source, target) in enumerate(pairs)
+    ]
+    for copy in copies:
+        copy.start()
+    for copy in copies:
+        copy.wait()
+    for k in range(RING):
+        out_ref[k, :, :UNITS] = down[...]
+        out_ref[k, :, UNITS:PADDED] = jnp.zeros((OWN // 2, PADDED - UNITS), jnp.bfloat16)
+        out_ref[k, :, PADDED : PADDED + UNITS] = gate[...]
+        out_ref[k, :, PADDED + UNITS :] = value[...]
+
+
+def packed_copies(down_weight, gate_weight, value_weight):
+    part = pltpu.VMEM((OWN // 2, UNITS), jnp.bfloat16)
+    return pl.pallas_call(
+        pack_kernel,
+        out_shape=jax.ShapeDtypeStruct((RING, OWN // 2, WIDE), jnp.bfloat16),
+        in_specs=[pl.BlockSpec(memory_space=pl.ANY)] * 3,
+        out_specs=pl.BlockSpec(memory_space=pltpu.VMEM),
+        scratch_shapes=[part, part, part, pltpu.SemaphoreType.DMA((3,))],
+        compiler_params=pltpu.CompilerParams(vmem_limit_bytes=60 * 1024 * 1024),
+        cost_estimate=pl.CostEstimate(
+            flops=0, bytes_accessed=2 * RING * OWN // 2 * WIDE, transcendentals=0
+        ),
+        name="pack",
+    )(down_weight.T, gate_weight, value_weight)
 
 
 def on_device(
@@ -305,15 +321,9 @@
     value_taps,
     down_weight,
 ):
-    packed = jnp.concatenate(
-        [
-            jnp.pad(down_weight.T, ((0, 0), (0, PADDED - UNITS))),
-            gate_weight,
-            value_weight,
-        ],
-        axis=1,
-    )
-    weights = gathered_blocks(packed)
+    copies = packed_copies(down_weight, gate_weight, value_weight)
+    copies, out_weight, key_states = lax.optimization_barrier((copies, out_weight, key_states))
+    weights = gathered_blocks(copies)
     taps = jnp.concatenate([gate_taps, value_taps], axis=1)
     other_weight = swapped(out_weight)
     own, other = attention_local(queries, key_states, value_states, sink_logits)

time: 147 us -> 146 us (level)
  local copies, waits for them, and re-layouts: 4.05 us -> 1.17 us
  Pallas kernels: 14.9 us -> 17.3 us
    pallas_call x0 -> x1, Pallas kernels: none -> 2.12 us  [packed_copies(): pl.pallas_call(pack_kernel, out_shape=jax.ShapeDtypeStruct((RING, OWN //...]
where the time goes in v4:
time: 146 us; the launch traced here: 145 us
  starting transfers between devices  69 us (47%)
  waiting for transfers between devices  31.8 us (22%)
  blocking collectives  18.2 us (12%)
  Pallas kernels  17.3 us (12%)
  matrix products  4.04 us (3%)
  other arithmetic  3.19 us (2%)
    ppermute x7, starting transfers between devices, ring_step(): return lax.ppermute(block, ALL, route)  30.6 us
    ppermute x7, waiting for transfers between devices, ring_step(): return lax.ppermute(block, ALL, route)  22.9 us
    all_to_all x1, blocking collectives, summed_over_x(): lax.all_to_all(shares, 'x', 0, 0, tiled=True).astype(jnp.float32)  18.2 us
    ppermute x4, starting transfers between devices, swapped(): return lax.ppermute(block, 'c', [(0, 1), (1, 0)])  16.1 us
    pallas_call x1, Pallas kernels, feed_forward(): pl.pallas_call(feed_forward_kernel, out_shape=(half, half), in_specs=[pl....  10.3 us
    all_to_all x1, starting transfers between devices, gathered_blocks(): lax.all_to_all(copies, ALL, 0, 0, tiled=True, axis_index_groups=crossed_g...  7.65 us
    pallas_call x1, Pallas kernels, attention_local(): pl.pallas_call(attention_kernel, out_shape=(half, half), in_specs=[vmem]...  4.9 us
    all_to_all x1, starting transfers between devices, summed_over_x(): lax.all_to_all(shares, 'x', 0, 0, tiled=True).astype(jnp.float32)  4.15 us
  transfers between devices with their start and end apart: 17, of which 12 were waited for; matrix products, arithmetic and copies ran while one was open for 5% of the time, Pallas kernels for 3%

profile of v4, /device:TPU:1, one launch (start us, length us, event | category | flops | bytes accessed | tf_op | source)
XLA Modules:
  0.0 145.0 jit_solution(3964030924031152118)
XLA Ops:
  0.0 0.0 copy-start.2
  0.0 2.1 %pack.1 = bf16[8,32,2176]{2,1,0:T(8,128)(2,1)} custom-call(bf16[32,704]{1,0:T(8,128)(2,1)} %bitcast.17, bf16[32,704]{1,0:T(8,128)(2,1)} %gate_hbm.1, bf16[32,704]{1,0:T(8,128)(2,1)} %value_hbm.1), custom_call_target="tpu_custom_call" | custom-call | bytes 1114112 | tf_op jit(solution)/shard_map/pack/pallas_call | solution.py:294
  2.1 7.7 %all-to-all-start.2 = ((bf16[8,32,2176]{2,1,0:T(8,128)(2,1)}), bf16[8,32,2176]{2,1,0:T(8,128)(2,1)S(1)}, u32[]{:S(2)}, u32[]{:S(2)}) async-start(bf16[8,32,2176]{2,1,0:T(8,128)(2,1)} %pack.1), calls=%async_computation.2 | async-start | bytes 2228224 | tf_op jit(solution)/shard_map/all_to_all | solution.py:267
  9.8 6.1 %collective-permute-start.2 = (bf16[256,2048]{1,0:T(8,128)(2,1)}, bf16[256,2048]{1,0:T(8,128)(2,1)S(1)}, u32[]{:S(2)}, u32[]{:S(2)}) collective-permute-start(bf16[256,2048]{1,0:T(8,128)(2,1)} %param.18), channel_id=1, source_target_pairs={{0,1},{1,0},{2,3},{3,2},{4,5},{5,4},{6,7},{7,6},{8,9},{9,8},{10,11... | collective-permute-start | bytes 3145736 | tf_op jit(solution)/shard_map/ppermute | solution.py:38
  15.9 0.0 copy-done.1
  15.9 0.0 copy-done
  15.9 3.2 %collective-permute-start = (bf16[128,128]{1,0:T(8,128)(2,1)S(1)}, bf16[128,128]{1,0:T(8,128)(2,1)S(1)}, u32[]{:S(2)}, u32[]{:S(2)}) collective-permute-start(bf16[128,128]{1,0:T(8,128)(2,1)S(1)} %pad_maximum_fusion), channel_id=1, source_target_pairs={{0,8},{8,16},{16,24},{24,32},{32,40},{40,48},{48,56},{56,64},{64,7... | collective-permute-start | bytes 98312 | tf_op jit(solution)/shard_map/ppermute | solution.py:34
  19.1 2.6 %collective-permute-done.edge_ref = bf16[128,128]{1,0:T(8,128)(2,1)S(1)} collective-permute-done((bf16[128,128]{1,0:T(8,128)(2,1)S(1)}, bf16[128,128]{1,0:T(8,128)(2,1)S(1)}, u32[]{:S(2)}, u32[]{:S(2)}) %collective-permute-start) | collective-permute-done | bytes 32800 | tf_op jit(solution)/shard_map/ppermute | solution.py:34
  21.7 0.0 copy-done.3
  21.7 0.0 copy-done.2
  21.7 4.9 %attention.1 = (bf16[4,64,256]{2,1,0:T(8,128)(2,1)S(1)}, bf16[4,64,256]{2,1,0:T(8,128)(2,1)S(1)}) custom-call(bf16[512,256]{1,0:T(8,128)(2,1)S(1)} %copy-done.2, bf16[64,512]{1,0:T(8,128)(2,1)S(1)} %bitcast.14, bf16[64,512]{1,0:T(8,128)(2,1)S(1)} %bitcast.16, bf16[128,128]{1,0:T(8,128)(2,1)S(1)} %collective-permute-done.edge_ref, f32[4]{0:T(128)S(1)} %copy-done.3), custom_call_target="tpu_custom_call" | custom-call | flops 268435456 | bytes 1048576 | tf_op jit(solution)/shard_map/attention/pallas_call | solution.py:111
  26.6 1.9 %collective-permute-start.1 = (bf16[4,64,256]{2,1,0:T(8,128)(2,1)S(1)}, bf16[4,64,256]{2,1,0:T(8,128)(2,1)}, u32[]{:S(2)}, u32[]{:S(2)}) collective-permute-start(bf16[4,64,256]{2,1,0:T(8,128)(2,1)S(1)} %get-tuple-element.15), channel_id=1, source_target_pairs={{0,1},{1,0},{2,3},{3,2},{4,5},{5,4},{6,7},{7,6},{8,9},{9,8},{10,11... | collective-permute-start | bytes 393224 | tf_op jit(solution)/shard_map/ppermute | solution.py:38
  28.6 0.1 all-to-all-done.2.refs_0_
  28.7 6.8 %collective-permute-start.6 = (bf16[8,32,2176]{2,1,0:T(8,128)(2,1)S(1)}, bf16[8,32,2176]{2,1,0:T(8,128)(2,1)S(1)}, u32[]{:S(2)}, u32[]{:S(2)}) collective-permute-start(bf16[8,32,2176]{2,1,0:T(8,128)(2,1)S(1)} %all-to-all-done.2.refs_0_), channel_id=1, source_target_pairs={{1,65},{0,8},{3,67},{2,10},{5,69},{4,12},{7,71},{6,14},{9,73},{8,1... | collective-permute-start | bytes 3342344 | tf_op jit(solution)/shard_map/ppermute | solution.py:255
  35.4 0.0 collective-permute-done.1
  35.4 0.0 collective-permute-done.2
  35.4 1.3 fusion.1
  36.8 2.7 %fusion = bf16[4,64,2048]{2,1,0:T(8,128)(2,1)} fusion(f32[4,64,2048]{2,1,0:T(8,128)S(1)} %fusion.1, bf16[4,64,256]{2,1,0:T(8,128)(2,1)S(1)} %get-tuple-element.13, bf16[256,2048]{1,0:T(8,128)(2,1)} %param.18), kind=kOutput, calls=%fused_computation.1 | convolution fusion | flops 269484032 | bytes 4325376 | tf_op jit(solution)/shard_map/xrk,kd->xrd/dot_general | solution.py:42
  39.5 4.1 %all-to-all-start = ((bf16[4,64,2048]{2,1,0:T(8,128)(2,1)}), bf16[4,64,2048]{2,1,0:T(8,128)(2,1)S(1)}, u32[]{:S(2)}, u32[]{:S(2)}) async-start(bf16[4,64,2048]{2,1,0:T(8,128)(2,1)} %fusion), calls=%async_computation | async-start | bytes 2097152 | tf_op jit(solution)/shard_map/all_to_all | solution.py:46
  43.6 7.4 %collective-permute-start.7 = (bf16[8,32,2176]{2,1,0:T(8,128)(2,1)S(1)}, bf16[8,32,2176]{2,1,0:T(8,128)(2,1)}, u32[]{:S(2)}, u32[]{:S(2)}) collective-permute-start(bf16[8,32,2176]{2,1,0:T(8,128)(2,1)S(1)} %all-to-all-done.2.refs_0_), channel_id=1, source_target_pairs={{1,449},{0,56},{3,451},{2,58},{5,453},{4,60},{7,455},{6,62},{9,457... | collective-permute-start | bytes 3342344 | tf_op jit(solution)/shard_map/ppermute | solution.py:255
  51.0 3.0 %collective-permute-done.6.refs_1_ = bf16[8,32,2176]{2,1,0:T(8,128)(2,1)S(1)} collective-permute-done((bf16[8,32,2176]{2,1,0:T(8,128)(2,1)S(1)}, bf16[8,32,2176]{2,1,0:T(8,128)(2,1)S(1)}, u32[]{:S(2)}, u32[]{:S(2)}) %collective-permute-start.6) | collective-permute-done | bytes 1114144 | tf_op jit(solution)/shard_map/ppermute | solution.py:255
  54.1 1.9 %collective-permute-start.8 = (bf16[8,32,2176]{2,1,0:T(8,128)(2,1)S(1)}, bf16[8,32,2176]{2,1,0:T(8,128)(2,1)}, u32[]{:S(2)}, u32[]{:S(2)}) collective-permute-start(bf16[8,32,2176]{2,1,0:T(8,128)(2,1)S(1)} %collective-permute-done.6.refs_1_), channel_id=1, source_target_pairs={{1,65},{0,8},{3,67},{2,10},{5,69},{4,12},{7,71},{6,14},{9,73},{8,1... | collective-permute-start | bytes 3342344 | tf_op jit(solution)/shard_map/ppermute | solution.py:255
  56.0 0.9 all-to-all-done
  56.9 0.2 convert_reduce_fusion.1
  57.0 0.0 copy-start.4
  57.1 0.1 multiply_reduce_fusion.2
  57.2 0.0 copy-done.6
  57.2 0.0 copy-done.7
  57.2 0.0 copy-start.10
  57.2 0.3 multiply_reduce_fusion.1
  57.5 5.9 %collective-permute-done.7.refs_2_ = bf16[8,32,2176]{2,1,0:T(8,128)(2,1)} collective-permute-done((bf16[8,32,2176]{2,1,0:T(8,128)(2,1)S(1)}, bf16[8,32,2176]{2,1,0:T(8,128)(2,1)}, u32[]{:S(2)}, u32[]{:S(2)}) %collective-permute-start.7) | collective-permute-done | bytes 1114144 | tf_op jit(solution)/shard_map/ppermute | solution.py:255
  63.5 5.4 %collective-permute-start.9 = (bf16[8,32,2176]{2,1,0:T(8,128)(2,1)}, bf16[8,32,2176]{2,1,0:T(8,128)(2,1)}, u32[]{:S(2)}, u32[]{:S(2)}) collective-permute-start(bf16[8,32,2176]{2,1,0:T(8,128)(2,1)} %collective-permute-done.7.refs_2_), channel_id=1, source_target_pairs={{1,449},{0,56},{3,451},{2,58},{5,453},{4,60},{7,455},{6,62},{9,457... | collective-permute-start | bytes 3342344 | tf_op jit(solution)/shard_map/ppermute | solution.py:255
  68.9 2.7 %collective-permute-done.8.refs_3_ = bf16[8,32,2176]{2,1,0:T(8,128)(2,1)} collective-permute-done((bf16[8,32,2176]{2,1,0:T(8,128)(2,1)S(1)}, bf16[8,32,2176]{2,1,0:T(8,128)(2,1)}, u32[]{:S(2)}, u32[]{:S(2)}) %collective-permute-start.8) | collective-permute-done | bytes 1114144 | tf_op jit(solution)/shard_map/ppermute | solution.py:255
  71.6 1.9 %collective-permute-start.10 = (bf16[8,32,2176]{2,1,0:T(8,128)(2,1)}, bf16[8,32,2176]{2,1,0:T(8,128)(2,1)}, u32[]{:S(2)}, u32[]{:S(2)}) collective-permute-start(bf16[8,32,2176]{2,1,0:T(8,128)(2,1)} %collective-permute-done.8.refs_3_), channel_id=1, source_target_pairs={{1,65},{0,8},{3,67},{2,10},{5,69},{4,12},{7,71},{6,14},{9,73},{8,1... | collective-permute-start | bytes 3342344 | tf_op jit(solution)/shard_map/ppermute | solution.py:255
  73.5 0.0 copy-done.4
  73.6 0.2 multiply_convert_fusion
  73.8 1.1 broadcast_in_dim.2
  74.9 3.9 %all-to-all-start.1 = ((bf16[4,64,2048]{2,1,0:T(8,128)(2,1)}), bf16[4,64,2048]{2,1,0:T(8,128)(2,1)S(1)}, u32[]{:S(2)}, u32[]{:S(2)}) async-start(bf16[4,64,2048]{2,1,0:T(8,128)(2,1)} %broadcast_in_dim.2), calls=%async_computation.1 | async-start | bytes 2097152 | tf_op jit(solution)/shard_map/all_to_all | solution.py:51
  78.7 2.9 %collective-permute-done.9.refs_4_ = bf16[8,32,2176]{2,1,0:T(8,128)(2,1)} collective-permute-done((bf16[8,32,2176]{2,1,0:T(8,128)(2,1)}, bf16[8,32,2176]{2,1,0:T(8,128)(2,1)}, u32[]{:S(2)}, u32[]{:S(2)}) %collective-permute-start.9) | collective-permute-done | bytes 1114144 | tf_op jit(solution)/shard_map/ppermute | solution.py:255
  81.6 5.3 %collective-permute-start.11 = (bf16[8,32,2176]{2,1,0:T(8,128)(2,1)}, bf16[8,32,2176]{2,1,0:T(8,128)(2,1)}, u32[]{:S(2)}, u32[]{:S(2)}) collective-permute-start(bf16[8,32,2176]{2,1,0:T(8,128)(2,1)} %collective-permute-done.9.refs_4_), channel_id=1, source_target_pairs={{1,449},{0,56},{3,451},{2,58},{5,453},{4,60},{7,455},{6,62},{9,457... | collective-permute-start | bytes 3342344 | tf_op jit(solution)/shard_map/ppermute | solution.py:255
  86.9 2.7 %collective-permute-done.10.refs_5_ = bf16[8,32,2176]{2,1,0:T(8,128)(2,1)} collective-permute-done((bf16[8,32,2176]{2,1,0:T(8,128)(2,1)}, bf16[8,32,2176]{2,1,0:T(8,128)(2,1)}, u32[]{:S(2)}, u32[]{:S(2)}) %collective-permute-start.10) | collective-permute-done | bytes 1114144 | tf_op jit(solution)/shard_map/ppermute | solution.py:255
  89.7 1.9 %collective-permute-start.12 = (bf16[8,32,2176]{2,1,0:T(8,128)(2,1)}, bf16[8,32,2176]{2,1,0:T(8,128)(2,1)}, u32[]{:S(2)}, u32[]{:S(2)}) collective-permute-start(bf16[8,32,2176]{2,1,0:T(8,128)(2,1)} %collective-permute-done.10.refs_5_), channel_id=1, source_target_pairs={{1,65},{0,8},{3,67},{2,10},{5,69},{4,12},{7,71},{6,14},{9,73},{8,1... | collective-permute-start | bytes 3342344 | tf_op jit(solution)/shard_map/ppermute | solution.py:255
  91.6 1.9 %all-to-all-done.1.own_ref = bf16[4,64,2048]{2,1,0:T(8,128)(2,1)S(1)} async-done(((bf16[4,64,2048]{2,1,0:T(8,128)(2,1)}), bf16[4,64,2048]{2,1,0:T(8,128)(2,1)S(1)}, u32[]{:S(2)}, u32[]{:S(2)}) %all-to-all-start.1) | async-done | bytes 1048608 | tf_op jit(solution)/shard_map/all_to_all | solution.py:51
  93.5 3.2 %collective-permute-start.3 = (bf16[4,64,2048]{2,1,0:T(8,128)(2,1)S(1)}, bf16[4,64,2048]{2,1,0:T(8,128)(2,1)S(1)}, u32[]{:S(2)}, u32[]{:S(2)}) collective-permute-start(bf16[4,64,2048]{2,1,0:T(8,128)(2,1)S(1)} %all-to-all-done.1.own_ref), channel_id=1, source_target_pairs={{0,1},{1,0},{2,3},{3,2},{4,5},{5,4},{6,7},{7,6},{8,9},{9,8},{10,11... | collective-permute-start | bytes 3145736 | tf_op jit(solution)/shard_map/ppermute | solution.py:38
  96.7 2.2 %collective-permute-start.5 = (bf16[16,2048]{1,0:T(8,128)(2,1)S(1)}, bf16[16,2048]{1,0:T(8,128)(2,1)S(1)}, u32[]{:S(2)}, u32[]{:S(2)}) collective-permute-start(bf16[16,2048]{1,0:T(8,128)(2,1)S(1)} %slice_bitcast_fusion), channel_id=1, source_target_pairs={{1,9},{3,11},{5,13},{7,15},{9,17},{11,19},{13,21},{15,23},{17,25},... | collective-permute-start | bytes 196616 | tf_op jit(solution)/shard_map/ppermute | solution.py:338
  98.9 1.3 collective-permute-start.4
  100.2 0.8 pad_maximum_fusion.1.taps_ref
  101.0 0.0 collective-permute-done.5.halo_1
  101.0 1.2 collective-permute-done.4.halo_0
  102.2 0.0 collective-permute-done.3.other_ref
  102.2 0.0 collective-permute-done.11.refs_6_
  102.2 5.5 %collective-permute-done.12.refs_7_ = bf16[8,32,2176]{2,1,0:T(8,128)(2,1)} collective-permute-done((bf16[8,32,2176]{2,1,0:T(8,128)(2,1)}, bf16[8,32,2176]{2,1,0:T(8,128)(2,1)}, u32[]{:S(2)}, u32[]{:S(2)}) %collective-permute-start.12) | collective-permute-done | bytes 1114144 | tf_op jit(solution)/shard_map/ppermute | solution.py:255
  107.7 10.3 %feed_forward.1 = (bf16[4,64,2048]{2,1,0:T(8,128)(2,1)S(1)}, bf16[4,64,2048]{2,1,0:T(8,128)(2,1)S(1)}) custom-call(bf16[4,64,2048]{2,1,0:T(8,128)(2,1)S(1)} %all-to-all-done.1.own_ref, bf16[4,64,2048]{2,1,0:T(8,128)(2,1)S(1)} %collective-permute-done.3.other_ref, bf16[16,2048]{1,0:T(8,128)(2,1)S(1)} %collective-permute-done.4.halo_0, ...), custom_call_target="tpu_custom_call" | custom-call | flops 4429185024 | bytes 13107200 | tf_op jit(solution)/shard_map/feed_forward/pallas_call | solution.py:206
  118.0 4.9 %collective-permute-start.13 = (bf16[4,64,2048]{2,1,0:T(8,128)(2,1)S(1)}, bf16[4,64,2048]{2,1,0:T(8,128)(2,1)S(1)}, u32[]{:S(2)}, u32[]{:S(2)}) collective-permute-start(bf16[4,64,2048]{2,1,0:T(8,128)(2,1)S(1)} %get-tuple-element.18), channel_id=1, source_target_pairs={{0,1},{1,0},{2,3},{3,2},{4,5},{5,4},{6,7},{7,6},{8,9},{9,8},{10,11... | collective-permute-start | bytes 3145736 | tf_op jit(solution)/shard_map/ppermute | solution.py:38
  122.9 2.3 %collective-permute-done.13 = bf16[4,64,2048]{2,1,0:T(8,128)(2,1)S(1)} collective-permute-done((bf16[4,64,2048]{2,1,0:T(8,128)(2,1)S(1)}, bf16[4,64,2048]{2,1,0:T(8,128)(2,1)S(1)}, u32[]{:S(2)}, u32[]{:S(2)}) %collective-permute-start.13) | collective-permute-done | bytes 1048608 | tf_op jit(solution)/shard_map/ppermute | solution.py:38
  125.2 0.4 add_convert_fusion
  125.6 0.0 copy-start.5
  125.6 0.0 copy-start.9
  125.6 0.0 copy-start.11
  125.6 18.2 %all_to_all.20 = bf16[4,64,2048]{2,1,0:T(8,128)(2,1)S(1)} all-to-all(bf16[4,64,2048]{2,1,0:T(8,128)(2,1)S(1)} %add_convert_fusion), channel_id=1, replica_groups=mesh['z'=8,'y'=8,'x'=4,'c'=2] {'x'}, dimensions={0} | all-to-all | bytes 2097152 | tf_op jit(solution)/shard_map/all_to_all | solution.py:46
  143.8 0.2 convert_reduce_fusion
  144.0 0.1 multiply_reduce_fusion
  144.1 0.0 copy-done.5
  144.1 0.9 add_convert_fusion.1
  (17 shorter events, 0.1 us)
Async XLA Ops:
  0.0 15.9 %copy-start = (bf16[512,64]{0,1:T(8,128)(2,1)S(1)}, bf16[512,64]{0,1:T(8,128)(2,1)}, u32[]{:S(2)}) copy-start(bf16[512,64]{0,1:T(8,128)(2,1)} %param.15) | copy-start | bytes 196612
  0.0 15.9 %copy-start.1 = (bf16[512,64]{0,1:T(8,128)(2,1)S(1)}, bf16[512,64]{0,1:T(8,128)(2,1)}, u32[]{:S(2)}) copy-start(bf16[512,64]{0,1:T(8,128)(2,1)} %param.16) | copy-start | bytes 196612
  0.0 21.7 %copy-start.3 = (f32[4]{0:T(128)S(1)}, f32[4]{0:T(128)}, u32[]{:S(2)}) copy-start(f32[4]{0:T(128)} %sink_ref.1) | copy-start | bytes 52
  0.0 21.7 %copy-start.2 = (bf16[512,256]{1,0:T(8,128)(2,1)S(1)}, bf16[512,256]{1,0:T(8,128)(2,1)}, u32[]{:S(2)}) copy-start(bf16[512,256]{1,0:T(8,128)(2,1)} %q_ref.1) | copy-start | bytes 786436
  2.1 26.5 %all-to-all-start.2 = ((bf16[8,32,2176]{2,1,0:T(8,128)(2,1)}), bf16[8,32,2176]{2,1,0:T(8,128)(2,1)S(1)}, u32[]{:S(2)}, u32[]{:S(2)}) async-start(bf16[8,32,2176]{2,1,0:T(8,128)(2,1)} %pack.1), calls=%async_computation.2 | async-start | bytes 2228224 | tf_op jit(solution)/shard_map/all_to_all | solution.py:267
  9.8 25.6 %collective-permute-start.2 = (bf16[256,2048]{1,0:T(8,128)(2,1)}, bf16[256,2048]{1,0:T(8,128)(2,1)S(1)}, u32[]{:S(2)}, u32[]{:S(2)}) collective-permute-start(bf16[256,2048]{1,0:T(8,128)(2,1)} %param.18), channel_id=1, source_target_pairs={{0,1},{1,0},{2,3},{3,2},{4,5},{5,4},{6,7},{7,6},{8,9},{9,8},{10,11... | collective-permute-start | bytes 3145736 | tf_op jit(solution)/shard_map/ppermute | solution.py:38
  15.9 5.8 %collective-permute-start = (bf16[128,128]{1,0:T(8,128)(2,1)S(1)}, bf16[128,128]{1,0:T(8,128)(2,1)S(1)}, u32[]{:S(2)}, u32[]{:S(2)}) collective-permute-start(bf16[128,128]{1,0:T(8,128)(2,1)S(1)} %pad_maximum_fusion), channel_id=1, source_target_pairs={{0,8},{8,16},{16,24},{24,32},{32,40},{40,48},{48,56},{56,64},{64,7... | collective-permute-start | bytes 98312 | tf_op jit(solution)/shard_map/ppermute | solution.py:34
  26.6 8.8 %collective-permute-start.1 = (bf16[4,64,256]{2,1,0:T(8,128)(2,1)S(1)}, bf16[4,64,256]{2,1,0:T(8,128)(2,1)}, u32[]{:S(2)}, u32[]{:S(2)}) collective-permute-start(bf16[4,64,256]{2,1,0:T(8,128)(2,1)S(1)} %get-tuple-element.15), channel_id=1, source_target_pairs={{0,1},{1,0},{2,3},{3,2},{4,5},{5,4},{6,7},{7,6},{8,9},{9,8},{10,11... | collective-permute-start | bytes 393224 | tf_op jit(solution)/shard_map/ppermute | solution.py:38
  28.7 25.4 %collective-permute-start.6 = (bf16[8,32,2176]{2,1,0:T(8,128)(2,1)S(1)}, bf16[8,32,2176]{2,1,0:T(8,128)(2,1)S(1)}, u32[]{:S(2)}, u32[]{:S(2)}) collective-permute-start(bf16[8,32,2176]{2,1,0:T(8,128)(2,1)S(1)} %all-to-all-done.2.refs_0_), channel_id=1, source_target_pairs={{1,65},{0,8},{3,67},{2,10},{5,69},{4,12},{7,71},{6,14},{9,73},{8,1... | collective-permute-start | bytes 3342344 | tf_op jit(solution)/shard_map/ppermute | solution.py:255
  39.5 17.7 %copy-start.6 = (bf16[64,2048]{1,0:T(8,128)(2,1)S(1)}, bf16[64,2048]{1,0:T(8,128)(2,1)}, u32[]{:S(2)}) copy-start(bf16[64,2048]{1,0:T(8,128)(2,1)} %param.19) | copy-start | bytes 786436
  39.5 17.7 %copy-start.7 = (f32[2048]{0:T(1024)S(1)}, f32[2048]{0:T(1024)}, u32[]{:S(2)}) copy-start(f32[2048]{0:T(1024)} %param.20) | copy-start | bytes 24580
  39.5 34.1 %copy-start.8 = (f32[2048]{0:T(1024)S(1)}, f32[2048]{0:T(1024)}, u32[]{:S(2)}) copy-start(f32[2048]{0:T(1024)} %param.21) | copy-start | bytes 24580
  39.5 17.4 %all-to-all-start = ((bf16[4,64,2048]{2,1,0:T(8,128)(2,1)}), bf16[4,64,2048]{2,1,0:T(8,128)(2,1)S(1)}, u32[]{:S(2)}, u32[]{:S(2)}) async-start(bf16[4,64,2048]{2,1,0:T(8,128)(2,1)} %fusion), calls=%async_computation | async-start | bytes 2097152 | tf_op jit(solution)/shard_map/all_to_all | solution.py:46
  43.6 19.8 %collective-permute-start.7 = (bf16[8,32,2176]{2,1,0:T(8,128)(2,1)S(1)}, bf16[8,32,2176]{2,1,0:T(8,128)(2,1)}, u32[]{:S(2)}, u32[]{:S(2)}) collective-permute-start(bf16[8,32,2176]{2,1,0:T(8,128)(2,1)S(1)} %all-to-all-done.2.refs_0_), channel_id=1, source_target_pairs={{1,449},{0,56},{3,451},{2,58},{5,453},{4,60},{7,455},{6,62},{9,457... | collective-permute-start | bytes 3342344 | tf_op jit(solution)/shard_map/ppermute | solution.py:255
  54.1 17.6 %collective-permute-start.8 = (bf16[8,32,2176]{2,1,0:T(8,128)(2,1)S(1)}, bf16[8,32,2176]{2,1,0:T(8,128)(2,1)}, u32[]{:S(2)}, u32[]{:S(2)}) collective-permute-start(bf16[8,32,2176]{2,1,0:T(8,128)(2,1)S(1)} %collective-permute-done.6.refs_1_), channel_id=1, source_target_pairs={{1,65},{0,8},{3,67},{2,10},{5,69},{4,12},{7,71},{6,14},{9,73},{8,1... | collective-permute-start | bytes 3342344 | tf_op jit(solution)/shard_map/ppermute | solution.py:255
  57.0 16.5 %copy-start.4 = (f32[64,2048]{1,0:T(8,128)}, f32[64,2048]{1,0:T(8,128)S(1)}, u32[]{:S(2)}) copy-start(f32[64,2048]{1,0:T(8,128)S(1)} %convert_reduce_fusion.1) | copy-start | bytes 1572868
  57.2 16.3 %copy-start.10 = (f32[64]{0:T(128)}, f32[64]{0:T(128)S(1)}, u32[]{:S(2)}) copy-start(f32[64]{0:T(128)S(1)} %add_rsqrt_fusion.2) | copy-start | bytes 772
  63.5 18.2 %collective-permute-start.9 = (bf16[8,32,2176]{2,1,0:T(8,128)(2,1)}, bf16[8,32,2176]{2,1,0:T(8,128)(2,1)}, u32[]{:S(2)}, u32[]{:S(2)}) collective-permute-start(bf16[8,32,2176]{2,1,0:T(8,128)(2,1)} %collective-permute-done.7.refs_2_), channel_id=1, source_target_pairs={{1,449},{0,56},{3,451},{2,58},{5,453},{4,60},{7,455},{6,62},{9,457... | collective-permute-start | bytes 3342344 | tf_op jit(solution)/shard_map/ppermute | solution.py:255
  71.6 18.1 %collective-permute-start.10 = (bf16[8,32,2176]{2,1,0:T(8,128)(2,1)}, bf16[8,32,2176]{2,1,0:T(8,128)(2,1)}, u32[]{:S(2)}, u32[]{:S(2)}) collective-permute-start(bf16[8,32,2176]{2,1,0:T(8,128)(2,1)} %collective-permute-done.8.refs_3_), channel_id=1, source_target_pairs={{1,65},{0,8},{3,67},{2,10},{5,69},{4,12},{7,71},{6,14},{9,73},{8,1... | collective-permute-start | bytes 3342344 | tf_op jit(solution)/shard_map/ppermute | solution.py:255
  74.9 18.6 %all-to-all-start.1 = ((bf16[4,64,2048]{2,1,0:T(8,128)(2,1)}), bf16[4,64,2048]{2,1,0:T(8,128)(2,1)S(1)}, u32[]{:S(2)}, u32[]{:S(2)}) async-start(bf16[4,64,2048]{2,1,0:T(8,128)(2,1)} %broadcast_in_dim.2), calls=%async_computation.1 | async-start | bytes 2097152 | tf_op jit(solution)/shard_map/all_to_all | solution.py:51
  81.6 20.6 %collective-permute-start.11 = (bf16[8,32,2176]{2,1,0:T(8,128)(2,1)}, bf16[8,32,2176]{2,1,0:T(8,128)(2,1)}, u32[]{:S(2)}, u32[]{:S(2)}) collective-permute-start(bf16[8,32,2176]{2,1,0:T(8,128)(2,1)} %collective-permute-done.9.refs_4_), channel_id=1, source_target_pairs={{1,449},{0,56},{3,451},{2,58},{5,453},{4,60},{7,455},{6,62},{9,457... | collective-permute-start | bytes 3342344 | tf_op jit(solution)/shard_map/ppermute | solution.py:255
  89.7 18.1 %collective-permute-start.12 = (bf16[8,32,2176]{2,1,0:T(8,128)(2,1)}, bf16[8,32,2176]{2,1,0:T(8,128)(2,1)}, u32[]{:S(2)}, u32[]{:S(2)}) collective-permute-start(bf16[8,32,2176]{2,1,0:T(8,128)(2,1)} %collective-permute-done.10.refs_5_), channel_id=1, source_target_pairs={{1,65},{0,8},{3,67},{2,10},{5,69},{4,12},{7,71},{6,14},{9,73},{8,1... | collective-permute-start | bytes 3342344 | tf_op jit(solution)/shard_map/ppermute | solution.py:255
  93.5 8.7 %collective-permute-start.3 = (bf16[4,64,2048]{2,1,0:T(8,128)(2,1)S(1)}, bf16[4,64,2048]{2,1,0:T(8,128)(2,1)S(1)}, u32[]{:S(2)}, u32[]{:S(2)}) collective-permute-start(bf16[4,64,2048]{2,1,0:T(8,128)(2,1)S(1)} %all-to-all-done.1.own_ref), channel_id=1, source_target_pairs={{0,1},{1,0},{2,3},{3,2},{4,5},{5,4},{6,7},{7,6},{8,9},{9,8},{10,11... | collective-permute-start | bytes 3145736 | tf_op jit(solution)/shard_map/ppermute | solution.py:38
  96.7 4.3 %collective-permute-start.5 = (bf16[16,2048]{1,0:T(8,128)(2,1)S(1)}, bf16[16,2048]{1,0:T(8,128)(2,1)S(1)}, u32[]{:S(2)}, u32[]{:S(2)}) collective-permute-start(bf16[16,2048]{1,0:T(8,128)(2,1)S(1)} %slice_bitcast_fusion), channel_id=1, source_target_pairs={{1,9},{3,11},{5,13},{7,15},{9,17},{11,19},{13,21},{15,23},{17,25},... | collective-permute-start | bytes 196616 | tf_op jit(solution)/shard_map/ppermute | solution.py:338
  98.9 3.3 %collective-permute-start.4 = (bf16[16,2048]{1,0:T(8,128)(2,1)S(1)}, bf16[16,2048]{1,0:T(8,128)(2,1)S(1)}, u32[]{:S(2)}, u32[]{:S(2)}) collective-permute-start(bf16[16,2048]{1,0:T(8,128)(2,1)S(1)} %slice_bitcast_fusion), channel_id=1, source_target_pairs={{1,8},{3,10},{5,12},{7,14},{9,16},{11,18},{13,20},{15,22},{17,24},... | collective-permute-start | bytes 196616 | tf_op jit(solution)/shard_map/ppermute | solution.py:338
  118.0 7.1 %collective-permute-start.13 = (bf16[4,64,2048]{2,1,0:T(8,128)(2,1)S(1)}, bf16[4,64,2048]{2,1,0:T(8,128)(2,1)S(1)}, u32[]{:S(2)}, u32[]{:S(2)}) collective-permute-start(bf16[4,64,2048]{2,1,0:T(8,128)(2,1)S(1)} %get-tuple-element.18), channel_id=1, source_target_pairs={{0,1},{1,0},{2,3},{3,2},{4,5},{5,4},{6,7},{7,6},{8,9},{9,8},{10,11... | collective-permute-start | bytes 3145736 | tf_op jit(solution)/shard_map/ppermute | solution.py:38
  125.6 18.5 %copy-start.5 = (f32[64,2048]{1,0:T(8,128)S(1)}, f32[64,2048]{1,0:T(8,128)}, u32[]{:S(2)}) copy-start(f32[64,2048]{1,0:T(8,128)} %copy-done.4) | copy-start | bytes 1572868
  125.6 18.5 %copy-start.9 = (f32[2048]{0:T(1024)S(1)}, f32[2048]{0:T(1024)}, u32[]{:S(2)}) copy-start(f32[2048]{0:T(1024)} %param.22) | copy-start | bytes 24580
  125.6 18.5 %copy-start.11 = (f32[64]{0:T(128)S(1)}, f32[64]{0:T(128)}, u32[]{:S(2)}) copy-start(f32[64]{0:T(128)} %copy-done.10) | copy-start | bytes 772

commit v5 on v4

--- a/solution.py
+++ b/solution.py
@@ -25,6 +25,7 @@
 ALL = (*SP, *TP)
 RING = 8
 STEPS = (0, 1, -1, 2, -2, 3, -3, 4)
+CHUNKS = ((UP_AT, 2 * UNITS), (0, PADDED))
 VMEM_LIMIT = 44 * 1024 * 1024
 
 
@@ -129,18 +130,27 @@
     core = lax.axis_index("c")
     place = jnp.where(core == 1, lax.axis_index("z"), lax.axis_index("y"))
 
-    def on_copies(act):
+    def on_copies(chunk, act):
+        cols = pl.ds(*CHUNKS[chunk])
         for k, (block, step) in enumerate(zip(blocks, STEPS)):
             source = lax.rem(place - step + RING, RING)
-            sem = sems.at[k]
+            sem = sems.at[chunk, k]
 
             @pl.when(core == 1)
             def _():
-                act(pltpu.make_async_copy(block, weights.at[source], sem))
+                act(
+                    pltpu.make_async_copy(
+                        block.at[:, :, cols], weights.at[source, :, :, cols], sem
+                    )
+                )
 
             @pl.when(core == 0)
             def _():
-                act(pltpu.make_async_copy(block, weights.at[:, source], sem))
+                act(
+                    pltpu.make_async_copy(
+                        block.at[:, :, cols], weights.at[:, source, :, cols], sem
+                    )
+                )
 
     def on_rows(act):
         for x in range(LOCAL // OWN // 2):
@@ -158,17 +168,21 @@
                 act(pltpu.make_async_copy(halo, x_ref.at[pl.ds(0, HALO)], row_sems.at[8]))
 
     on_rows(lambda copy: copy.start())
-    on_copies(lambda copy: copy.start())
+    for chunk in range(len(CHUNKS)):
+        on_copies(chunk, lambda copy: copy.start())
     on_rows(lambda copy: copy.wait())
-    on_copies(lambda copy: copy.wait())
-    for at in range(0, 2 * UNITS, 256):
-        width = min(256, 2 * UNITS - at)
-        part = jnp.dot(
-            x_ref[...],
-            weights[:, :, :, UP_AT + at : UP_AT + at + width].reshape(D, width),
-            preferred_element_type=jnp.float32,
-        )
-        up[:, at : at + width] = part.astype(jnp.bfloat16).astype(jnp.float32)
+    for chunk, (at, width) in enumerate(CHUNKS[:-1]):
+        on_copies(chunk, lambda copy: copy.wait())
+        for sub in range(at, at + width, 256):
+            wide = min(256, at + width - sub)
+            part = jnp.dot(
+                x_ref[...],
+                weights[:, :, :, sub : sub + wide].reshape(D, wide),
+                preferred_element_type=jnp.float32,
+            )
+            up[:, sub - UP_AT : sub - UP_AT + wide] = part.astype(jnp.bfloat16).astype(
+                jnp.float32
+            )
     rows = 64
     lane = lax.broadcasted_iota(jnp.int32, (rows, PADDED), 1)
 
@@ -184,6 +198,7 @@
         both = (gate + gate * jnp.tanh(gate)) * value
         both = jnp.where(lane < UNITS, both, 0.0)
         hidden[pl.ds(start, rows), :] = both.astype(jnp.bfloat16)
+    on_copies(len(CHUNKS) - 1, lambda copy: copy.wait())
     for z in range(0, RING, 2):
         part = lax.dot_general(
             hidden[...],
@@ -215,7 +230,7 @@
             pltpu.VMEM((HALO + LOCAL, D), jnp.bfloat16),
             pltpu.VMEM((HALO + LOCAL, 2 * UNITS), jnp.float32),
             pltpu.VMEM((LOCAL, PADDED), jnp.bfloat16),
-            pltpu.SemaphoreType.DMA((RING,)),
+            pltpu.SemaphoreType.DMA((len(CHUNKS), RING)),
             pltpu.SemaphoreType.DMA((LOCAL // OWN + 1,)),
         ],
         compiler_params=pltpu.CompilerParams(vmem_limit_bytes=VMEM_LIMIT),

time: 146 us -> 146 us (level)
  no operation moved by 1% of the time
where the time goes in v5:
time: 146 us; the launch traced here: 145 us
  starting transfers between devices  69.2 us (47%)
  waiting for transfers between devices  31.8 us (22%)
  blocking collectives  18.2 us (12%)
  Pallas kernels  16.9 us (12%)
  matrix products  4.04 us (3%)
  other arithmetic  3.19 us (2%)
    ppermute x7, starting transfers between devices, ring_step(): return lax.ppermute(block, ALL, route)  30.6 us
    ppermute x7, waiting for transfers between devices, ring_step(): return lax.ppermute(block, ALL, route)  22.9 us
    all_to_all x1, blocking collectives, summed_over_x(): lax.all_to_all(shares, 'x', 0, 0, tiled=True).astype(jnp.float32)  18.2 us
    ppermute x4, starting transfers between devices, swapped(): return lax.ppermute(block, 'c', [(0, 1), (1, 0)])  16.2 us
    pallas_call x1, Pallas kernels, feed_forward(): pl.pallas_call(feed_forward_kernel, out_shape=(half, half), in_specs=[pl....  9.9 us
    all_to_all x1, starting transfers between devices, gathered_blocks(): lax.all_to_all(copies, ALL, 0, 0, tiled=True, axis_index_groups=crossed_g...  7.65 us
    pallas_call x1, Pallas kernels, attention_local(): pl.pallas_call(attention_kernel, out_shape=(half, half), in_specs=[vmem]...  4.9 us
    all_to_all x1, starting transfers between devices, summed_over_x(): lax.all_to_all(shares, 'x', 0, 0, tiled=True).astype(jnp.float32)  4.15 us
  transfers between devices with their start and end apart: 17, of which 12 were waited for; matrix products, arithmetic and copies ran while one was open for 5% of the time, Pallas kernels for 3%

profile of v5, /device:TPU:1, one launch (start us, length us, event | category | flops | bytes accessed | tf_op | source)
XLA Modules:
  0.0 144.8 jit_solution(11453851874701143906)
XLA Ops:
  0.0 0.0 copy-start.2
  0.0 2.1 %pack.1 = bf16[8,32,2176]{2,1,0:T(8,128)(2,1)} custom-call(bf16[32,704]{1,0:T(8,128)(2,1)} %bitcast.17, bf16[32,704]{1,0:T(8,128)(2,1)} %gate_hbm.1, bf16[32,704]{1,0:T(8,128)(2,1)} %value_hbm.1), custom_call_target="tpu_custom_call" | custom-call | bytes 1114112 | tf_op jit(solution)/shard_map/pack/pallas_call | solution.py:309
  2.1 7.7 %all-to-all-start.2 = ((bf16[8,32,2176]{2,1,0:T(8,128)(2,1)}), bf16[8,32,2176]{2,1,0:T(8,128)(2,1)S(1)}, u32[]{:S(2)}, u32[]{:S(2)}) async-start(bf16[8,32,2176]{2,1,0:T(8,128)(2,1)} %pack.1), calls=%async_computation.2 | async-start | bytes 2228224 | tf_op jit(solution)/shard_map/all_to_all | solution.py:282
  9.8 6.1 %collective-permute-start.2 = (bf16[256,2048]{1,0:T(8,128)(2,1)}, bf16[256,2048]{1,0:T(8,128)(2,1)S(1)}, u32[]{:S(2)}, u32[]{:S(2)}) collective-permute-start(bf16[256,2048]{1,0:T(8,128)(2,1)} %param.18), channel_id=1, source_target_pairs={{0,1},{1,0},{2,3},{3,2},{4,5},{5,4},{6,7},{7,6},{8,9},{9,8},{10,11... | collective-permute-start | bytes 3145736 | tf_op jit(solution)/shard_map/ppermute | solution.py:39
  15.9 0.0 copy-done.1
  15.9 0.0 copy-done
  15.9 3.2 %collective-permute-start = (bf16[128,128]{1,0:T(8,128)(2,1)S(1)}, bf16[128,128]{1,0:T(8,128)(2,1)S(1)}, u32[]{:S(2)}, u32[]{:S(2)}) collective-permute-start(bf16[128,128]{1,0:T(8,128)(2,1)S(1)} %pad_maximum_fusion), channel_id=1, source_target_pairs={{0,8},{8,16},{16,24},{24,32},{32,40},{40,48},{48,56},{56,64},{64,7... | collective-permute-start | bytes 98312 | tf_op jit(solution)/shard_map/ppermute | solution.py:35
  19.1 2.6 %collective-permute-done.edge_ref = bf16[128,128]{1,0:T(8,128)(2,1)S(1)} collective-permute-done((bf16[128,128]{1,0:T(8,128)(2,1)S(1)}, bf16[128,128]{1,0:T(8,128)(2,1)S(1)}, u32[]{:S(2)}, u32[]{:S(2)}) %collective-permute-start) | collective-permute-done | bytes 32800 | tf_op jit(solution)/shard_map/ppermute | solution.py:35
  21.7 0.0 copy-done.3
  21.7 0.0 copy-done.2
  21.7 4.9 %attention.1 = (bf16[4,64,256]{2,1,0:T(8,128)(2,1)S(1)}, bf16[4,64,256]{2,1,0:T(8,128)(2,1)S(1)}) custom-call(bf16[512,256]{1,0:T(8,128)(2,1)S(1)} %copy-done.2, bf16[64,512]{1,0:T(8,128)(2,1)S(1)} %bitcast.14, bf16[64,512]{1,0:T(8,128)(2,1)S(1)} %bitcast.16, bf16[128,128]{1,0:T(8,128)(2,1)S(1)} %collective-permute-done.edge_ref, f32[4]{0:T(128)S(1)} %copy-done.3), custom_call_target="tpu_custom_call" | custom-call | flops 268435456 | bytes 1048576 | tf_op jit(solution)/shard_map/attention/pallas_call | solution.py:112
  26.6 1.9 %collective-permute-start.1 = (bf16[4,64,256]{2,1,0:T(8,128)(2,1)S(1)}, bf16[4,64,256]{2,1,0:T(8,128)(2,1)}, u32[]{:S(2)}, u32[]{:S(2)}) collective-permute-start(bf16[4,64,256]{2,1,0:T(8,128)(2,1)S(1)} %get-tuple-element.15), channel_id=1, source_target_pairs={{0,1},{1,0},{2,3},{3,2},{4,5},{5,4},{6,7},{7,6},{8,9},{9,8},{10,11... | collective-permute-start | bytes 393224 | tf_op jit(solution)/shard_map/ppermute | solution.py:39
  28.6 0.1 all-to-all-done.2.refs_0_
  28.7 6.8 %collective-permute-start.6 = (bf16[8,32,2176]{2,1,0:T(8,128)(2,1)S(1)}, bf16[8,32,2176]{2,1,0:T(8,128)(2,1)S(1)}, u32[]{:S(2)}, u32[]{:S(2)}) collective-permute-start(bf16[8,32,2176]{2,1,0:T(8,128)(2,1)S(1)} %all-to-all-done.2.refs_0_), channel_id=1, source_target_pairs={{1,65},{0,8},{3,67},{2,10},{5,69},{4,12},{7,71},{6,14},{9,73},{8,1... | collective-permute-start | bytes 3342344 | tf_op jit(solution)/shard_map/ppermute | solution.py:270
  35.4 0.0 collective-permute-done.1
  35.4 0.0 collective-permute-done.2
  35.4 1.3 fusion.1
  36.8 2.7 %fusion = bf16[4,64,2048]{2,1,0:T(8,128)(2,1)} fusion(f32[4,64,2048]{2,1,0:T(8,128)S(1)} %fusion.1, bf16[4,64,256]{2,1,0:T(8,128)(2,1)S(1)} %get-tuple-element.13, bf16[256,2048]{1,0:T(8,128)(2,1)} %param.18), kind=kOutput, calls=%fused_computation.1 | convolution fusion | flops 269484032 | bytes 4325376 | tf_op jit(solution)/shard_map/xrk,kd->xrd/dot_general | solution.py:43
  39.5 4.1 %all-to-all-start = ((bf16[4,64,2048]{2,1,0:T(8,128)(2,1)}), bf16[4,64,2048]{2,1,0:T(8,128)(2,1)S(1)}, u32[]{:S(2)}, u32[]{:S(2)}) async-start(bf16[4,64,2048]{2,1,0:T(8,128)(2,1)} %fusion), calls=%async_computation | async-start | bytes 2097152 | tf_op jit(solution)/shard_map/all_to_all | solution.py:47
  43.6 7.4 %collective-permute-start.7 = (bf16[8,32,2176]{2,1,0:T(8,128)(2,1)S(1)}, bf16[8,32,2176]{2,1,0:T(8,128)(2,1)}, u32[]{:S(2)}, u32[]{:S(2)}) collective-permute-start(bf16[8,32,2176]{2,1,0:T(8,128)(2,1)S(1)} %all-to-all-done.2.refs_0_), channel_id=1, source_target_pairs={{1,449},{0,56},{3,451},{2,58},{5,453},{4,60},{7,455},{6,62},{9,457... | collective-permute-start | bytes 3342344 | tf_op jit(solution)/shard_map/ppermute | solution.py:270
  51.0 3.0 %collective-permute-done.6.refs_1_ = bf16[8,32,2176]{2,1,0:T(8,128)(2,1)S(1)} collective-permute-done((bf16[8,32,2176]{2,1,0:T(8,128)(2,1)S(1)}, bf16[8,32,2176]{2,1,0:T(8,128)(2,1)S(1)}, u32[]{:S(2)}, u32[]{:S(2)}) %collective-permute-start.6) | collective-permute-done | bytes 1114144 | tf_op jit(solution)/shard_map/ppermute | solution.py:270
  54.1 1.9 %collective-permute-start.8 = (bf16[8,32,2176]{2,1,0:T(8,128)(2,1)S(1)}, bf16[8,32,2176]{2,1,0:T(8,128)(2,1)}, u32[]{:S(2)}, u32[]{:S(2)}) collective-permute-start(bf16[8,32,2176]{2,1,0:T(8,128)(2,1)S(1)} %collective-permute-done.6.refs_1_), channel_id=1, source_target_pairs={{1,65},{0,8},{3,67},{2,10},{5,69},{4,12},{7,71},{6,14},{9,73},{8,1... | collective-permute-start | bytes 3342344 | tf_op jit(solution)/shard_map/ppermute | solution.py:270
  56.0 0.9 all-to-all-done
  56.9 0.2 convert_reduce_fusion.1
  57.0 0.0 copy-start.4
  57.1 0.1 multiply_reduce_fusion.2
  57.2 0.0 copy-done.6
  57.2 0.0 copy-done.7
  57.2 0.0 copy-start.10
  57.2 0.3 multiply_reduce_fusion.1
  57.5 5.9 %collective-permute-done.7.refs_2_ = bf16[8,32,2176]{2,1,0:T(8,128)(2,1)} collective-permute-done((bf16[8,32,2176]{2,1,0:T(8,128)(2,1)S(1)}, bf16[8,32,2176]{2,1,0:T(8,128)(2,1)}, u32[]{:S(2)}, u32[]{:S(2)}) %collective-permute-start.7) | collective-permute-done | bytes 1114144 | tf_op jit(solution)/shard_map/ppermute | solution.py:270
  63.5 5.4 %collective-permute-start.9 = (bf16[8,32,2176]{2,1,0:T(8,128)(2,1)}, bf16[8,32,2176]{2,1,0:T(8,128)(2,1)}, u32[]{:S(2)}, u32[]{:S(2)}) collective-permute-start(bf16[8,32,2176]{2,1,0:T(8,128)(2,1)} %collective-permute-done.7.refs_2_), channel_id=1, source_target_pairs={{1,449},{0,56},{3,451},{2,58},{5,453},{4,60},{7,455},{6,62},{9,457... | collective-permute-start | bytes 3342344 | tf_op jit(solution)/shard_map/ppermute | solution.py:270
  68.9 2.7 %collective-permute-done.8.refs_3_ = bf16[8,32,2176]{2,1,0:T(8,128)(2,1)} collective-permute-done((bf16[8,32,2176]{2,1,0:T(8,128)(2,1)S(1)}, bf16[8,32,2176]{2,1,0:T(8,128)(2,1)}, u32[]{:S(2)}, u32[]{:S(2)}) %collective-permute-start.8) | collective-permute-done | bytes 1114144 | tf_op jit(solution)/shard_map/ppermute | solution.py:270
  71.6 1.9 %collective-permute-start.10 = (bf16[8,32,2176]{2,1,0:T(8,128)(2,1)}, bf16[8,32,2176]{2,1,0:T(8,128)(2,1)}, u32[]{:S(2)}, u32[]{:S(2)}) collective-permute-start(bf16[8,32,2176]{2,1,0:T(8,128)(2,1)} %collective-permute-done.8.refs_3_), channel_id=1, source_target_pairs={{1,65},{0,8},{3,67},{2,10},{5,69},{4,12},{7,71},{6,14},{9,73},{8,1... | collective-permute-start | bytes 3342344 | tf_op jit(solution)/shard_map/ppermute | solution.py:270
  73.6 0.2 multiply_convert_fusion
  73.8 1.1 broadcast_in_dim.2
  74.9 3.9 %all-to-all-start.1 = ((bf16[4,64,2048]{2,1,0:T(8,128)(2,1)}), bf16[4,64,2048]{2,1,0:T(8,128)(2,1)S(1)}, u32[]{:S(2)}, u32[]{:S(2)}) async-start(bf16[4,64,2048]{2,1,0:T(8,128)(2,1)} %broadcast_in_dim.2), calls=%async_computation.1 | async-start | bytes 2097152 | tf_op jit(solution)/shard_map/all_to_all | solution.py:52
  78.7 2.9 %collective-permute-done.9.refs_4_ = bf16[8,32,2176]{2,1,0:T(8,128)(2,1)} collective-permute-done((bf16[8,32,2176]{2,1,0:T(8,128)(2,1)}, bf16[8,32,2176]{2,1,0:T(8,128)(2,1)}, u32[]{:S(2)}, u32[]{:S(2)}) %collective-permute-start.9) | collective-permute-done | bytes 1114144 | tf_op jit(solution)/shard_map/ppermute | solution.py:270
  81.6 5.3 %collective-permute-start.11 = (bf16[8,32,2176]{2,1,0:T(8,128)(2,1)}, bf16[8,32,2176]{2,1,0:T(8,128)(2,1)}, u32[]{:S(2)}, u32[]{:S(2)}) collective-permute-start(bf16[8,32,2176]{2,1,0:T(8,128)(2,1)} %collective-permute-done.9.refs_4_), channel_id=1, source_target_pairs={{1,449},{0,56},{3,451},{2,58},{5,453},{4,60},{7,455},{6,62},{9,457... | collective-permute-start | bytes 3342344 | tf_op jit(solution)/shard_map/ppermute | solution.py:270
  86.9 2.7 %collective-permute-done.10.refs_5_ = bf16[8,32,2176]{2,1,0:T(8,128)(2,1)} collective-permute-done((bf16[8,32,2176]{2,1,0:T(8,128)(2,1)}, bf16[8,32,2176]{2,1,0:T(8,128)(2,1)}, u32[]{:S(2)}, u32[]{:S(2)}) %collective-permute-start.10) | collective-permute-done | bytes 1114144 | tf_op jit(solution)/shard_map/ppermute | solution.py:270
  89.7 1.9 %collective-permute-start.12 = (bf16[8,32,2176]{2,1,0:T(8,128)(2,1)}, bf16[8,32,2176]{2,1,0:T(8,128)(2,1)}, u32[]{:S(2)}, u32[]{:S(2)}) collective-permute-start(bf16[8,32,2176]{2,1,0:T(8,128)(2,1)} %collective-permute-done.10.refs_5_), channel_id=1, source_target_pairs={{1,65},{0,8},{3,67},{2,10},{5,69},{4,12},{7,71},{6,14},{9,73},{8,1... | collective-permute-start | bytes 3342344 | tf_op jit(solution)/shard_map/ppermute | solution.py:270
  91.6 1.9 %all-to-all-done.1.own_ref = bf16[4,64,2048]{2,1,0:T(8,128)(2,1)S(1)} async-done(((bf16[4,64,2048]{2,1,0:T(8,128)(2,1)}), bf16[4,64,2048]{2,1,0:T(8,128)(2,1)S(1)}, u32[]{:S(2)}, u32[]{:S(2)}) %all-to-all-start.1) | async-done | bytes 1048608 | tf_op jit(solution)/shard_map/all_to_all | solution.py:52
  93.5 3.2 %collective-permute-start.3 = (bf16[4,64,2048]{2,1,0:T(8,128)(2,1)S(1)}, bf16[4,64,2048]{2,1,0:T(8,128)(2,1)S(1)}, u32[]{:S(2)}, u32[]{:S(2)}) collective-permute-start(bf16[4,64,2048]{2,1,0:T(8,128)(2,1)S(1)} %all-to-all-done.1.own_ref), channel_id=1, source_target_pairs={{0,1},{1,0},{2,3},{3,2},{4,5},{5,4},{6,7},{7,6},{8,9},{9,8},{10,11... | collective-permute-start | bytes 3145736 | tf_op jit(solution)/shard_map/ppermute | solution.py:39
  96.7 2.2 %collective-permute-start.5 = (bf16[16,2048]{1,0:T(8,128)(2,1)S(1)}, bf16[16,2048]{1,0:T(8,128)(2,1)S(1)}, u32[]{:S(2)}, u32[]{:S(2)}) collective-permute-start(bf16[16,2048]{1,0:T(8,128)(2,1)S(1)} %slice_bitcast_fusion), channel_id=1, source_target_pairs={{1,9},{3,11},{5,13},{7,15},{9,17},{11,19},{13,21},{15,23},{17,25},... | collective-permute-start | bytes 196616 | tf_op jit(solution)/shard_map/ppermute | solution.py:353
  98.9 1.3 collective-permute-start.4
  100.2 0.8 pad_maximum_fusion.1.taps_ref
  101.0 0.0 collective-permute-done.5.halo_1
  101.0 1.2 collective-permute-done.4.halo_0
  102.2 0.0 collective-permute-done.3.other_ref
  102.2 0.0 collective-permute-done.11.refs_6_
  102.2 5.5 %collective-permute-done.12.refs_7_ = bf16[8,32,2176]{2,1,0:T(8,128)(2,1)} collective-permute-done((bf16[8,32,2176]{2,1,0:T(8,128)(2,1)}, bf16[8,32,2176]{2,1,0:T(8,128)(2,1)}, u32[]{:S(2)}, u32[]{:S(2)}) %collective-permute-start.12) | collective-permute-done | bytes 1114144 | tf_op jit(solution)/shard_map/ppermute | solution.py:270
  107.7 9.9 %feed_forward.1 = (bf16[4,64,2048]{2,1,0:T(8,128)(2,1)S(1)}, bf16[4,64,2048]{2,1,0:T(8,128)(2,1)S(1)}) custom-call(bf16[4,64,2048]{2,1,0:T(8,128)(2,1)S(1)} %all-to-all-done.1.own_ref, bf16[4,64,2048]{2,1,0:T(8,128)(2,1)S(1)} %collective-permute-done.3.other_ref, bf16[16,2048]{1,0:T(8,128)(2,1)S(1)} %collective-permute-done.4.halo_0, ...), custom_call_target="tpu_custom_call" | custom-call | flops 4429185024 | bytes 13107200 | tf_op jit(solution)/shard_map/feed_forward/pallas_call | solution.py:221
  117.6 5.1 %collective-permute-start.13 = (bf16[4,64,2048]{2,1,0:T(8,128)(2,1)S(1)}, bf16[4,64,2048]{2,1,0:T(8,128)(2,1)S(1)}, u32[]{:S(2)}, u32[]{:S(2)}) collective-permute-start(bf16[4,64,2048]{2,1,0:T(8,128)(2,1)S(1)} %get-tuple-element.18), channel_id=1, source_target_pairs={{0,1},{1,0},{2,3},{3,2},{4,5},{5,4},{6,7},{7,6},{8,9},{9,8},{10,11... | collective-permute-start | bytes 3145736 | tf_op jit(solution)/shard_map/ppermute | solution.py:39
  122.7 2.3 %collective-permute-done.13 = bf16[4,64,2048]{2,1,0:T(8,128)(2,1)S(1)} collective-permute-done((bf16[4,64,2048]{2,1,0:T(8,128)(2,1)S(1)}, bf16[4,64,2048]{2,1,0:T(8,128)(2,1)S(1)}, u32[]{:S(2)}, u32[]{:S(2)}) %collective-permute-start.13) | collective-permute-done | bytes 1048608 | tf_op jit(solution)/shard_map/ppermute | solution.py:39
  125.0 0.4 add_convert_fusion
  125.4 0.0 copy-start.5
  125.4 0.0 copy-start.9
  125.4 0.0 copy-start.11
  125.4 18.2 %all_to_all.20 = bf16[4,64,2048]{2,1,0:T(8,128)(2,1)S(1)} all-to-all(bf16[4,64,2048]{2,1,0:T(8,128)(2,1)S(1)} %add_convert_fusion), channel_id=1, replica_groups=mesh['z'=8,'y'=8,'x'=4,'c'=2] {'x'}, dimensions={0} | all-to-all | bytes 2097152 | tf_op jit(solution)/shard_map/all_to_all | solution.py:47
  143.6 0.2 convert_reduce_fusion
  143.7 0.1 multiply_reduce_fusion
  143.9 0.0 copy-done.9
  143.9 0.0 copy-done.11
  143.9 0.9 add_convert_fusion.1
  (17 shorter events, 0.1 us)
Async XLA Ops:
  0.0 15.9 %copy-start = (bf16[512,64]{0,1:T(8,128)(2,1)S(1)}, bf16[512,64]{0,1:T(8,128)(2,1)}, u32[]{:S(2)}) copy-start(bf16[512,64]{0,1:T(8,128)(2,1)} %param.15) | copy-start | bytes 196612
  0.0 15.9 %copy-start.1 = (bf16[512,64]{0,1:T(8,128)(2,1)S(1)}, bf16[512,64]{0,1:T(8,128)(2,1)}, u32[]{:S(2)}) copy-start(bf16[512,64]{0,1:T(8,128)(2,1)} %param.16) | copy-start | bytes 196612
  0.0 21.7 %copy-start.3 = (f32[4]{0:T(128)S(1)}, f32[4]{0:T(128)}, u32[]{:S(2)}) copy-start(f32[4]{0:T(128)} %sink_ref.1) | copy-start | bytes 52
  0.0 21.7 %copy-start.2 = (bf16[512,256]{1,0:T(8,128)(2,1)S(1)}, bf16[512,256]{1,0:T(8,128)(2,1)}, u32[]{:S(2)}) copy-start(bf16[512,256]{1,0:T(8,128)(2,1)} %q_ref.1) | copy-start | bytes 786436
  2.1 26.5 %all-to-all-start.2 = ((bf16[8,32,2176]{2,1,0:T(8,128)(2,1)}), bf16[8,32,2176]{2,1,0:T(8,128)(2,1)S(1)}, u32[]{:S(2)}, u32[]{:S(2)}) async-start(bf16[8,32,2176]{2,1,0:T(8,128)(2,1)} %pack.1), calls=%async_computation.2 | async-start | bytes 2228224 | tf_op jit(solution)/shard_map/all_to_all | solution.py:282
  9.8 25.6 %collective-permute-start.2 = (bf16[256,2048]{1,0:T(8,128)(2,1)}, bf16[256,2048]{1,0:T(8,128)(2,1)S(1)}, u32[]{:S(2)}, u32[]{:S(2)}) collective-permute-start(bf16[256,2048]{1,0:T(8,128)(2,1)} %param.18), channel_id=1, source_target_pairs={{0,1},{1,0},{2,3},{3,2},{4,5},{5,4},{6,7},{7,6},{8,9},{9,8},{10,11... | collective-permute-start | bytes 3145736 | tf_op jit(solution)/shard_map/ppermute | solution.py:39
  15.9 5.8 %collective-permute-start = (bf16[128,128]{1,0:T(8,128)(2,1)S(1)}, bf16[128,128]{1,0:T(8,128)(2,1)S(1)}, u32[]{:S(2)}, u32[]{:S(2)}) collective-permute-start(bf16[128,128]{1,0:T(8,128)(2,1)S(1)} %pad_maximum_fusion), channel_id=1, source_target_pairs={{0,8},{8,16},{16,24},{24,32},{32,40},{40,48},{48,56},{56,64},{64,7... | collective-permute-start | bytes 98312 | tf_op jit(solution)/shard_map/ppermute | solution.py:35
  26.6 8.8 %collective-permute-start.1 = (bf16[4,64,256]{2,1,0:T(8,128)(2,1)S(1)}, bf16[4,64,256]{2,1,0:T(8,128)(2,1)}, u32[]{:S(2)}, u32[]{:S(2)}) collective-permute-start(bf16[4,64,256]{2,1,0:T(8,128)(2,1)S(1)} %get-tuple-element.15), channel_id=1, source_target_pairs={{0,1},{1,0},{2,3},{3,2},{4,5},{5,4},{6,7},{7,6},{8,9},{9,8},{10,11... | collective-permute-start | bytes 393224 | tf_op jit(solution)/shard_map/ppermute | solution.py:39
  28.7 25.4 %collective-permute-start.6 = (bf16[8,32,2176]{2,1,0:T(8,128)(2,1)S(1)}, bf16[8,32,2176]{2,1,0:T(8,128)(2,1)S(1)}, u32[]{:S(2)}, u32[]{:S(2)}) collective-permute-start(bf16[8,32,2176]{2,1,0:T(8,128)(2,1)S(1)} %all-to-all-done.2.refs_0_), channel_id=1, source_target_pairs={{1,65},{0,8},{3,67},{2,10},{5,69},{4,12},{7,71},{6,14},{9,73},{8,1... | collective-permute-start | bytes 3342344 | tf_op jit(solution)/shard_map/ppermute | solution.py:270
  39.5 17.7 %copy-start.6 = (bf16[64,2048]{1,0:T(8,128)(2,1)S(1)}, bf16[64,2048]{1,0:T(8,128)(2,1)}, u32[]{:S(2)}) copy-start(bf16[64,2048]{1,0:T(8,128)(2,1)} %param.19) | copy-start | bytes 786436
  39.5 17.7 %copy-start.7 = (f32[2048]{0:T(1024)S(1)}, f32[2048]{0:T(1024)}, u32[]{:S(2)}) copy-start(f32[2048]{0:T(1024)} %param.20) | copy-start | bytes 24580
  39.5 34.1 %copy-start.8 = (f32[2048]{0:T(1024)S(1)}, f32[2048]{0:T(1024)}, u32[]{:S(2)}) copy-start(f32[2048]{0:T(1024)} %param.21) | copy-start | bytes 24580
  39.5 17.4 %all-to-all-start = ((bf16[4,64,2048]{2,1,0:T(8,128)(2,1)}), bf16[4,64,2048]{2,1,0:T(8,128)(2,1)S(1)}, u32[]{:S(2)}, u32[]{:S(2)}) async-start(bf16[4,64,2048]{2,1,0:T(8,128)(2,1)} %fusion), calls=%async_computation | async-start | bytes 2097152 | tf_op jit(solution)/shard_map/all_to_all | solution.py:47
  43.6 19.8 %collective-permute-start.7 = (bf16[8,32,2176]{2,1,0:T(8,128)(2,1)S(1)}, bf16[8,32,2176]{2,1,0:T(8,128)(2,1)}, u32[]{:S(2)}, u32[]{:S(2)}) collective-permute-start(bf16[8,32,2176]{2,1,0:T(8,128)(2,1)S(1)} %all-to-all-done.2.refs_0_), channel_id=1, source_target_pairs={{1,449},{0,56},{3,451},{2,58},{5,453},{4,60},{7,455},{6,62},{9,457... | collective-permute-start | bytes 3342344 | tf_op jit(solution)/shard_map/ppermute | solution.py:270
  54.1 17.6 %collective-permute-start.8 = (bf16[8,32,2176]{2,1,0:T(8,128)(2,1)S(1)}, bf16[8,32,2176]{2,1,0:T(8,128)(2,1)}, u32[]{:S(2)}, u32[]{:S(2)}) collective-permute-start(bf16[8,32,2176]{2,1,0:T(8,128)(2,1)S(1)} %collective-permute-done.6.refs_1_), channel_id=1, source_target_pairs={{1,65},{0,8},{3,67},{2,10},{5,69},{4,12},{7,71},{6,14},{9,73},{8,1... | collective-permute-start | bytes 3342344 | tf_op jit(solution)/shard_map/ppermute | solution.py:270
  57.0 16.5 %copy-start.4 = (f32[64,2048]{1,0:T(8,128)}, f32[64,2048]{1,0:T(8,128)S(1)}, u32[]{:S(2)}) copy-start(f32[64,2048]{1,0:T(8,128)S(1)} %convert_reduce_fusion.1) | copy-start | bytes 1572868
  57.2 16.3 %copy-start.10 = (f32[64]{0:T(128)}, f32[64]{0:T(128)S(1)}, u32[]{:S(2)}) copy-start(f32[64]{0:T(128)S(1)} %add_rsqrt_fusion.2) | copy-start | bytes 772
  63.5 18.2 %collective-permute-start.9 = (bf16[8,32,2176]{2,1,0:T(8,128)(2,1)}, bf16[8,32,2176]{2,1,0:T(8,128)(2,1)}, u32[]{:S(2)}, u32[]{:S(2)}) collective-permute-start(bf16[8,32,2176]{2,1,0:T(8,128)(2,1)} %collective-permute-done.7.refs_2_), channel_id=1, source_target_pairs={{1,449},{0,56},{3,451},{2,58},{5,453},{4,60},{7,455},{6,62},{9,457... | collective-permute-start | bytes 3342344 | tf_op jit(solution)/shard_map/ppermute | solution.py:270
  71.6 18.1 %collective-permute-start.10 = (bf16[8,32,2176]{2,1,0:T(8,128)(2,1)}, bf16[8,32,2176]{2,1,0:T(8,128)(2,1)}, u32[]{:S(2)}, u32[]{:S(2)}) collective-permute-start(bf16[8,32,2176]{2,1,0:T(8,128)(2,1)} %collective-permute-done.8.refs_3_), channel_id=1, source_target_pairs={{1,65},{0,8},{3,67},{2,10},{5,69},{4,12},{7,71},{6,14},{9,73},{8,1... | collective-permute-start | bytes 3342344 | tf_op jit(solution)/shard_map/ppermute | solution.py:270
  74.9 18.6 %all-to-all-start.1 = ((bf16[4,64,2048]{2,1,0:T(8,128)(2,1)}), bf16[4,64,2048]{2,1,0:T(8,128)(2,1)S(1)}, u32[]{:S(2)}, u32[]{:S(2)}) async-start(bf16[4,64,2048]{2,1,0:T(8,128)(2,1)} %broadcast_in_dim.2), calls=%async_computation.1 | async-start | bytes 2097152 | tf_op jit(solution)/shard_map/all_to_all | solution.py:52
  81.6 20.6 %collective-permute-start.11 = (bf16[8,32,2176]{2,1,0:T(8,128)(2,1)}, bf16[8,32,2176]{2,1,0:T(8,128)(2,1)}, u32[]{:S(2)}, u32[]{:S(2)}) collective-permute-start(bf16[8,32,2176]{2,1,0:T(8,128)(2,1)} %collective-permute-done.9.refs_4_), channel_id=1, source_target_pairs={{1,449},{0,56},{3,451},{2,58},{5,453},{4,60},{7,455},{6,62},{9,457... | collective-permute-start | bytes 3342344 | tf_op jit(solution)/shard_map/ppermute | solution.py:270
  89.7 18.1 %collective-permute-start.12 = (bf16[8,32,2176]{2,1,0:T(8,128)(2,1)}, bf16[8,32,2176]{2,1,0:T(8,128)(2,1)}, u32[]{:S(2)}, u32[]{:S(2)}) collective-permute-start(bf16[8,32,2176]{2,1,0:T(8,128)(2,1)} %collective-permute-done.10.refs_5_), channel_id=1, source_target_pairs={{1,65},{0,8},{3,67},{2,10},{5,69},{4,12},{7,71},{6,14},{9,73},{8,1... | collective-permute-start | bytes 3342344 | tf_op jit(solution)/shard_map/ppermute | solution.py:270
  93.5 8.7 %collective-permute-start.3 = (bf16[4,64,2048]{2,1,0:T(8,128)(2,1)S(1)}, bf16[4,64,2048]{2,1,0:T(8,128)(2,1)S(1)}, u32[]{:S(2)}, u32[]{:S(2)}) collective-permute-start(bf16[4,64,2048]{2,1,0:T(8,128)(2,1)S(1)} %all-to-all-done.1.own_ref), channel_id=1, source_target_pairs={{0,1},{1,0},{2,3},{3,2},{4,5},{5,4},{6,7},{7,6},{8,9},{9,8},{10,11... | collective-permute-start | bytes 3145736 | tf_op jit(solution)/shard_map/ppermute | solution.py:39
  96.7 4.3 %collective-permute-start.5 = (bf16[16,2048]{1,0:T(8,128)(2,1)S(1)}, bf16[16,2048]{1,0:T(8,128)(2,1)S(1)}, u32[]{:S(2)}, u32[]{:S(2)}) collective-permute-start(bf16[16,2048]{1,0:T(8,128)(2,1)S(1)} %slice_bitcast_fusion), channel_id=1, source_target_pairs={{1,9},{3,11},{5,13},{7,15},{9,17},{11,19},{13,21},{15,23},{17,25},... | collective-permute-start | bytes 196616 | tf_op jit(solution)/shard_map/ppermute | solution.py:353
  98.9 3.3 %collective-permute-start.4 = (bf16[16,2048]{1,0:T(8,128)(2,1)S(1)}, bf16[16,2048]{1,0:T(8,128)(2,1)S(1)}, u32[]{:S(2)}, u32[]{:S(2)}) collective-permute-start(bf16[16,2048]{1,0:T(8,128)(2,1)S(1)} %slice_bitcast_fusion), channel_id=1, source_target_pairs={{1,8},{3,10},{5,12},{7,14},{9,16},{11,18},{13,20},{15,22},{17,24},... | collective-permute-start | bytes 196616 | tf_op jit(solution)/shard_map/ppermute | solution.py:353
  117.6 7.3 %collective-permute-start.13 = (bf16[4,64,2048]{2,1,0:T(8,128)(2,1)S(1)}, bf16[4,64,2048]{2,1,0:T(8,128)(2,1)S(1)}, u32[]{:S(2)}, u32[]{:S(2)}) collective-permute-start(bf16[4,64,2048]{2,1,0:T(8,128)(2,1)S(1)} %get-tuple-element.18), channel_id=1, source_target_pairs={{0,1},{1,0},{2,3},{3,2},{4,5},{5,4},{6,7},{7,6},{8,9},{9,8},{10,11... | collective-permute-start | bytes 3145736 | tf_op jit(solution)/shard_map/ppermute | solution.py:39
  125.4 18.5 %copy-start.5 = (f32[64,2048]{1,0:T(8,128)S(1)}, f32[64,2048]{1,0:T(8,128)}, u32[]{:S(2)}) copy-start(f32[64,2048]{1,0:T(8,128)} %copy-done.4) | copy-start | bytes 1572868
  125.4 18.5 %copy-start.9 = (f32[2048]{0:T(1024)S(1)}, f32[2048]{0:T(1024)}, u32[]{:S(2)}) copy-start(f32[2048]{0:T(1024)} %param.22) | copy-start | bytes 24580
  125.4 18.5 %copy-start.11 = (f32[64]{0:T(128)S(1)}, f32[64]{0:T(128)}, u32[]{:S(2)}) copy-start(f32[64]{0:T(128)} %copy-done.10) | copy-start | bytes 772
